TPU v7x, 512 devices: a whole 4x4x16 slice. The times are simulated.
512 devices in a mesh: sp: 32 (over z, core), tp: 16 (over y, x).
Axes of the slice: x: 4, y: 4, z: 16, core: 2. Of those that a mesh axis runs over, the one named last changes fastest.
Arguments:
- moe_input: bfloat16 [8192, 2048], P('sp'), may hold values from -6 to 6
- out_grad: bfloat16 [8192, 2048], P('sp'), may hold values from -0.29882812 to 0.29882812
- route_ids: int32 [8192, 2], P('sp'), may hold values from 0 to 31, all different within a row; in each aligned block of 256 rows (0 to 255, 256 to 511, ...) at most 20 rows name the same one
- route_weights: float32 [8192, 2], P('sp'), may hold values from 0.2 to 1
- gate_weight: bfloat16 [32, 1024, 2048], P('sp', 'tp'), may hold values from -0.1875 to 0.1875
- lin_weight: bfloat16 [32, 1024, 2048], P('sp', 'tp'), may hold values from -0.1875 to 0.1875
- down_weight: bfloat16 [32, 1024, 2048], P('sp', 'tp'), may hold values from -0.1875 to 0.1875
- outer_gate: bfloat16 [8192, 2048], P('sp', 'tp'), may hold values from -6 to 6
- inner_gate: bfloat16 [8192, 2048], P('sp', 'tp'), may hold values from -6 to 6
- conv_input: bfloat16 [8192, 2048], P('sp', 'tp'), may hold values from -6 to 6
- conv_taps: float32 [3, 2048], P(None, 'tp'), may hold values from -3.5 to 3.5
- out_proj: bfloat16 [2048, 2048], P('tp', 'sp'), may hold values from -0.125 to 0.125
Outputs:
- gate_weight_grad: bfloat16 [32, 1024, 2048], P('sp', 'tp')
- lin_weight_grad: bfloat16 [32, 1024, 2048], P('sp', 'tp')
- down_weight_grad: bfloat16 [32, 1024, 2048], P('sp', 'tp')
- out_proj_grad: float32 [2048, 2048], P('sp', 'tp')
- outer_gate_grad: bfloat16 [8192, 2048], P('sp', 'tp')
- inner_gate_grad: bfloat16 [8192, 2048], P('sp', 'tp')
- conv_input_grad: bfloat16 [8192, 2048], P('sp', 'tp')
Inputs may be any that keep to these rules, and one draw needn't show every extreme that they name: `route_ids`: each row names 2 different experts. Among the rows of one device no expert is named more than 20 times, a bound that some block reaches.
All inputs are finite; a program needn't handle non-finite values.
Results may differ from a plain program's by a relative error of at most 0.015.
Values may be sent and summed in bfloat16 or wider, within the bound.
No kernel may reach another device: no remote copies, remote signals or barrier semaphores. Data moves between devices by JAX's collectives and lax.ppermute only.
A program may use at most 64 MiB of HBM per device.

v0:
```python
import jax
import jax.numpy as jnp
from jax import lax
from jax.sharding import Mesh
from jax.sharding import PartitionSpec as P

SP = ("sp_0", "sp_1")


LIMIT = 7.0
ALPHA = 1.702


def in_one_piece(arrays, axis, split_dim, concat_dim, along):
    widths = [a.shape[along] for a in arrays]
    both = jnp.concatenate(arrays, axis=along)
    filled = lax.all_to_all(both, axis, split_axis=split_dim, concat_axis=concat_dim, tiled=True)
    return tuple(jnp.split(filled, [sum(widths[:k]) for k in range(1, len(widths))], axis=along))


def sent_together(arrays, axis, dim, along):
    ends, at = ([], 0)
    for a in arrays[:-1]:
        at += a.shape[along]
        ends.append(at)
    both = jnp.concatenate(arrays, axis=along)
    return tuple(jnp.split(lax.all_gather(both, axis, axis=dim, tiled=True), ends, axis=along))


def from_everyone(value, axis):
    copies = jnp.broadcast_to(value, (lax.axis_size(axis), *value.shape))
    return lax.all_to_all(copies, axis, split_axis=0, concat_axis=0, tiled=True)


def laid_out(blocks, dim):
    dims = list(blocks.shape[1:])
    dims[dim] *= blocks.shape[0]
    return jnp.moveaxis(blocks, 0, dim).reshape(dims)


def gather_directly(value, axis, dim):
    blocks = from_everyone(value, axis)
    return laid_out(blocks, dim)


def from_behind(value, axis, by):
    count = lax.axis_size(axis)
    pairs = [(i, i + by) for i in range(count) if 0 <= i + by < count]
    return lax.ppermute(value, axis, pairs)


def all_blocks(value, axes, sequence):
    blocks = value[None]
    for k in sequence:
        blocks = lax.all_gather(blocks, axes[k], axis=0, tiled=True)
    block = [lax.axis_size(axes[k]) for k in reversed(sequence)]
    blocks = blocks.reshape(*block, *value.shape)
    turned = sorted(range(len(sequence)), key=lambda place: sequence[len(sequence) - 1 - place])
    return blocks.transpose(*turned, *range(len(sequence), blocks.ndim)).reshape(-1, *value.shape)


def whole_of(value, axes, sequence, dim):
    return laid_out(all_blocks(value, axes, sequence), dim)


def split_up(value, dim, count):
    dims = value.shape
    blocks = value.reshape(*dims[:dim], count, dims[dim] // count, *dims[dim + 1 :])
    return jnp.moveaxis(blocks, dim, 0)


def sum_at_owner(value, axis, dim):
    count = lax.axis_size(axis)
    blocks = lax.all_to_all(split_up(value, dim, count), axis, 0, 0, tiled=True)
    return jnp.sum(blocks, axis=0)


def slot_layout(flat_ids, experts, capacity):
    onehot = (flat_ids[:, None] == jnp.arange(experts, dtype=jnp.int32)[None, :]).astype(jnp.int32)
    before = jnp.cumsum(onehot, axis=0) - onehot
    slot_rank = jnp.sum(before * onehot, axis=1)
    position = flat_ids * capacity + slot_rank
    pair_index = jnp.arange(flat_ids.shape[0], dtype=jnp.int32)
    source = jnp.full((experts * capacity,), -1, jnp.int32).at[position].set(pair_index)
    return (position, source)


def expert_terms(routed, cotan, gate_w, lin_w, down_w):
    gate_pre = jnp.einsum("xfd,xrd->xfr", gate_w, routed, preferred_element_type=jnp.float32)
    lin_pre = jnp.einsum("xfd,xrd->xfr", lin_w, routed, preferred_element_type=jnp.float32)
    gate_cut = jnp.minimum(gate_pre, LIMIT)
    lin_cut = jnp.clip(lin_pre, -LIMIT, LIMIT)
    sigma = jax.nn.sigmoid(ALPHA * gate_cut)
    act = (gate_cut * sigma * (lin_cut + 1.0)).astype(jnp.bfloat16)
    act_grad = jnp.einsum("xfd,xrd->xfr", down_w, cotan, preferred_element_type=jnp.float32)
    down_grad = jnp.einsum("xfr,xrd->xfd", act, cotan, preferred_element_type=jnp.float32)
    slope = sigma * (1.0 + ALPHA * gate_cut * (1.0 - sigma))
    gate_cot = jnp.where(gate_pre < LIMIT, act_grad * (lin_cut + 1.0) * slope, 0.0).astype(
        jnp.bfloat16
    )
    lin_cot = jnp.where(jnp.abs(lin_pre) < LIMIT, act_grad * gate_cut * sigma, 0.0).astype(
        jnp.bfloat16
    )
    gate_grad = jnp.einsum("xfr,xrd->xfd", gate_cot, routed, preferred_element_type=jnp.float32)
    lin_grad = jnp.einsum("xfr,xrd->xfd", lin_cot, routed, preferred_element_type=jnp.float32)
    input_part = jnp.einsum("xfr,xfd->xrd", gate_cot, gate_w, preferred_element_type=jnp.float32)
    input_part = input_part + jnp.einsum(
        "xfr,xfd->xrd", lin_cot, lin_w, preferred_element_type=jnp.float32
    )
    return (gate_grad, lin_grad, down_grad, input_part.astype(jnp.bfloat16))


def local(
    moe_input,
    out_grad,
    route_ids,
    route_weights,
    gate_weight,
    lin_weight,
    down_weight,
    outer_gate,
    inner_gate,
    conv_input,
    conv_taps,
    out_proj,
):
    sp_count = lax.axis_size(SP)
    tp_count = lax.axis_size("tp")
    local_experts = gate_weight.shape[0]
    experts = local_experts * sp_count
    tokens, top_count = route_ids.shape
    width = moe_input.shape[1]
    width_dev = width // tp_count
    capacity = 5 * tokens // (2 * experts)
    position, source = slot_layout(route_ids.reshape(-1), experts, capacity)
    filled = source >= 0
    picked = jnp.maximum(source, 0)
    token_row = picked // top_count
    send_rows = jnp.where(filled[:, None], moe_input[token_row], jnp.zeros((), jnp.bfloat16))
    send_rows = send_rows.reshape(experts, capacity, width)
    slot_weight = jnp.where(filled, route_weights.reshape(-1)[picked], 0.0)
    send_grads = (
        (slot_weight[:, None] * out_grad[token_row])
        .astype(jnp.bfloat16)
        .reshape(experts, capacity, width)
    )
    column_start = lax.axis_index("tp") * width_dev
    part_rows = lax.dynamic_slice_in_dim(send_rows, column_start, width_dev, 2)
    part_grads = lax.dynamic_slice_in_dim(send_grads, column_start, width_dev, 2)
    routed_part, cotan_part = in_one_piece((part_rows, part_grads), SP, 0, 1, 2)
    routed, cotan = sent_together((routed_part, cotan_part), "tp", 2, 0)
    expert_out = expert_terms(routed, cotan, gate_weight, lin_weight, down_weight)
    totals = expert_out[:3]
    input_part = expert_out[3]
    slot_count = input_part.shape[1]
    exchanged = lax.all_to_all(
        input_part.reshape(local_experts * slot_count, tp_count, width_dev),
        "tp",
        split_axis=1,
        concat_axis=1,
        tiled=True,
    )
    slot_sums = jnp.sum(exchanged.astype(jnp.float32), axis=1).astype(jnp.bfloat16)
    slot_sums = slot_sums.reshape(local_experts, slot_count, width_dev)
    returned = lax.all_to_all(slot_sums, SP, split_axis=1, concat_axis=0, tiled=True)
    pair_grads = returned.reshape(experts * capacity, width_dev)[position].astype(jnp.float32)
    row_grads = jnp.sum(pair_grads.reshape(tokens, top_count, width_dev), axis=1).astype(
        jnp.bfloat16
    )
    full_rows = gather_directly(row_grads, "tp", 1)
    stream_grad = (out_grad.astype(jnp.float32) + full_rows.astype(jnp.float32)).astype(
        jnp.bfloat16
    )
    tap_count = conv_taps.shape[0]
    conv_values = (inner_gate.astype(jnp.float32) * conv_input.astype(jnp.float32)).astype(
        jnp.bfloat16
    )
    prior_rows = from_behind(conv_values[tokens - (tap_count - 1) :], SP, 1)
    extended = jnp.concatenate([prior_rows, conv_values], axis=0).astype(jnp.float32)
    convolved = jnp.zeros((tokens, width_dev), jnp.float32)
    for tap_index in range(tap_count):
        convolved = (
            convolved + conv_taps[tap_index][None, :] * extended[tap_index : tap_index + tokens]
        )
    mixed = (outer_gate.astype(jnp.float32) * convolved).astype(jnp.bfloat16)
    columns = stream_grad
    mixed_grad = lax.dot_general(
        columns,
        whole_of(out_proj, SP, (0, 1), 1),
        (((1,), (1,)), ((), ())),
        preferred_element_type=jnp.float32,
    )
    columns = stream_grad
    out_proj_grad = sum_at_owner(
        lax.dot_general(
            columns, mixed, (((0,), (0,)), ((), ())), preferred_element_type=jnp.float32
        ),
        SP,
        0,
    )
    outer_gate_grad = (mixed_grad * convolved).astype(jnp.bfloat16)
    conv_cot = (mixed_grad * outer_gate.astype(jnp.float32)).astype(jnp.bfloat16)
    later_rows = from_behind(conv_cot[: tap_count - 1], SP, -1)
    extended_cot = jnp.concatenate([conv_cot, later_rows], axis=0).astype(jnp.float32)
    value_grad = jnp.zeros((tokens, width_dev), jnp.float32)
    for tap_index in range(tap_count):
        first_row = tap_count - 1 - tap_index
        value_grad = (
            value_grad
            + conv_taps[tap_index][None, :] * extended_cot[first_row : first_row + tokens]
        )
    inner_gate_grad = (value_grad * conv_input.astype(jnp.float32)).astype(jnp.bfloat16)
    conv_input_grad = (value_grad * inner_gate.astype(jnp.float32)).astype(jnp.bfloat16)
    return (
        totals[0].astype(jnp.bfloat16),
        totals[1].astype(jnp.bfloat16),
        totals[2].astype(jnp.bfloat16),
        out_proj_grad,
        outer_gate_grad,
        inner_gate_grad,
        conv_input_grad,
    )


def solution(mesh):
    torus = Mesh(mesh.devices.reshape(16, 2, mesh.shape["tp"]), ("sp_0", "sp_1", "tp"))
    placed = (
        P(SP, None),
        P(SP, None),
        P(SP, None),
        P(SP, None),
        P(SP, "tp", None),
        P(SP, "tp", None),
        P(SP, "tp", None),
        P(SP, "tp"),
        P(SP, "tp"),
        P(SP, "tp"),
        P(None, "tp"),
        P("tp", SP),
    )
    return jax.shard_map(
        local,
        mesh=torus,
        in_specs=placed,
        out_specs=(
            P(SP, "tp", None),
            P(SP, "tp", None),
            P(SP, "tp", None),
            P(SP, "tp"),
            P(SP, "tp"),
            P(SP, "tp"),
            P(SP, "tp"),
        ),
        check_vma=False,
    )
```

profile of v0, /device:TPU:1, one launch (start us, length us, event | category | flops | bytes accessed | tf_op | source)
XLA Modules:
  0.0 355.5 jit_solution(17896420848058425541)
XLA Ops:
  7.2 0.8 broadcast_multiply_fusion
  8.1 0.8 copy.46
  9.5 1.2 reduce-window.6
  11.0 2.4 scatter_custom_fusion
  13.5 4.1 %gather_fusion.2 = bf16[640,2048]{1,0:T(8,128)(2,1)} fusion(bf16[256,2048]{1,0:T(8,128)(2,1)S(1)} %copy-done.1, s32[1024]{0:T(1024)S(1)} %get-tuple-element.24), kind=kCustom, calls=%fused_computation.2 | custom fusion | bytes 5245440 | tf_op jit(solution)/shard_map/gather | solution.py:143
  17.7 5.5 %reshape.199 = f32[32,20,2048]{2,1,0:T(8,128)} reshape(bf16[640,2048]{1,0:T(8,128)(2,1)} %gather_fusion.2) | data formatting | bytes 7864320 | tf_op jit(solution)/shard_map/convert_element_type | solution.py:143
  23.4 4.3 %gather_fusion.1 = f32[640]{0:T(1024)S(1)} fusion(f32[512]{0:T(512)S(1)} %reshape.186, s32[1024]{0:T(1024)S(1)} %get-tuple-element.23), kind=kCustom, calls=%fused_computation.1 | custom fusion | bytes 7680 | tf_op jit(solution)/shard_map/gather | solution.py:141
  27.9 4.1 %gather_fusion = bf16[640,2048]{1,0:T(8,128)(2,1)} fusion(bf16[256,2048]{1,0:T(8,128)(2,1)S(1)} %copy-done, s32[1024]{0:T(1024)S(1)} %get-tuple-element.24), kind=kCustom, calls=%fused_computation | custom fusion | bytes 5245440 | tf_op jit(solution)/shard_map/gather | solution.py:139
  31.9 5.1 %gather.17 = bf16[32,20,2048]{2,1,0:T(8,128)(2,1)} reshape(bf16[640,2048]{1,0:T(8,128)(2,1)} %gather_fusion) | data formatting | bytes 5242880 | tf_op jit(solution)/shard_map/gather | solution.py:139
  37.2 1.2 fusion.11
  38.4 1.1 dynamic-slice_select_fusion
  39.5 44.3 %all_to_all.36 = bf16[32,20,256]{2,1,0:T(8,128)(2,1)S(1)} all-to-all(bf16[32,20,256]{2,1,0:T(8,128)(2,1)S(1)} %pad_maximum_fusion), channel_id=1, replica_groups=mesh['sp_0'=16,'sp_1'=2,'tp'=16] {'sp_0','sp_1'}, dimensions={0} | all-to-all | bytes 655360 | tf_op jit(solution)/shard_map/all_to_all | solution.py:17
  83.9 0.8 pad_maximum_fusion.1
  84.7 67.3 %all-gather.3.cloned.1.call-done = bf16[2,640,2048]{2,1,0:T(8,128)(2,1)} async-done(((bf16[2,640,128]{2,1,0:T(8,128)(2,1)}), bf16[2,640,2048]{2,1,0:T(8,128)(2,1)}) %all-gather.3.cloned.1.call-update) | async-done | bytes 5242896 | tf_op jit(solution)/shard_map/all_gather | solution.py:27
  152.1 2.8 fusion.8
  154.9 2.7 fusion.9
  157.7 0.9 fusion.20
  158.7 0.9 fusion.15
  159.5 0.9 fusion.7
  160.4 0.7 copy.65
  161.1 37.5 %all_to_all.37 = bf16[640,16,128]{2,0,1:T(8,128)(2,1)} all-to-all(bf16[640,16,128]{2,0,1:T(8,128)(2,1)S(1)} %bitcast.149), channel_id=1, replica_groups=mesh['sp_0'=16,'sp_1'=2,'tp'=16] {'tp'}, dimensions={1} | all-to-all | bytes 5242880 | tf_op jit(solution)/shard_map/all_to_all | solution.py:156
  198.6 2.1 reduce_sum.46
  201.4 1.6 reduce.4
  203.1 0.7 reshape.248
  203.8 15.4 %all-to-all-start.2 = ((bf16[32,2,1280]{2,1,0:T(2,128)(2,1)}), bf16[32,2,1280]{2,1,0:T(2,128)(2,1)S(1)}, u32[]{:S(2)}, u32[]{:S(2)}) async-start(bf16[32,2,1280]{2,1,0:T(2,128)(2,1)} %reshape.248), calls=%async_computation.2 | async-start | bytes 327680 | tf_op jit(solution)/shard_map/all_to_all | solution.py:165
  219.2 17.1 %all-to-all-done.2 = bf16[32,2,1280]{2,1,0:T(2,128)(2,1)S(1)} async-done(((bf16[32,2,1280]{2,1,0:T(2,128)(2,1)}), bf16[32,2,1280]{2,1,0:T(2,128)(2,1)S(1)}, u32[]{:S(2)}, u32[]{:S(2)}) %all-to-all-start.2) | async-done | bytes 163872 | tf_op jit(solution)/shard_map/all_to_all | solution.py:165
  236.6 1.3 gather_fusion.3
  238.2 1.2 broadcast_in_dim.52
  239.4 4.3 %all-to-all-start.3 = ((bf16[16,256,128]{2,1,0:T(8,128)(2,1)}), bf16[16,256,128]{2,1,0:T(8,128)(2,1)}, u32[]{:S(2)}, u32[]{:S(2)}) async-start(bf16[16,256,128]{2,1,0:T(8,128)(2,1)} %broadcast_in_dim.52), calls=%async_computation.3 | async-start | bytes 2097152 | tf_op jit(solution)/shard_map/all_to_all | solution.py:32
  243.9 3.5 collective-permute-start
  247.4 21.5 %all-gather = bf16[2048,64]{0,1:T(8,128)(2,1)S(1)} all-gather(bf16[128,64]{0,1:T(8,128)(2,1)S(1)} %copy-done.11), channel_id=2, replica_groups=mesh['sp_0'=16,'sp_1'=2,'tp'=16] {'sp_0'}, dimensions={0}, use_global_device_ids=true | all-gather | bytes 278528 | tf_op jit(solution)/shard_map/all_gather | solution.py:55
  269.0 8.1 %all_gather.11 = bf16[32,128,64]{1,0,2:T(8,128)(2,1)} all-gather(bf16[16,128,64]{1,0,2:T(8,128)(2,1)S(1)} %bitcast.155), channel_id=1, replica_groups=mesh['sp_0'=16,'sp_1'=2,'tp'=16] {'sp_1'}, dimensions={0}, use_global_device_ids=true | all-gather | bytes 786432 | tf_op jit(solution)/shard_map/all_gather | solution.py:55
  277.1 0.5 copy.50
  277.6 2.0 copy.55
  279.7 2.3 copy.53
  282.0 1.5 fusion.6
  283.5 2.2 multiply_convert_fusion
  285.7 1.4 fusion.42
  287.1 5.2 %all-to-all-start.4 = ((f32[32,64,128]{2,1,0:T(8,128)}), f32[32,64,128]{2,1,0:T(8,128)S(1)}, u32[]{:S(2)}, u32[]{:S(2)}) async-start(f32[32,64,128]{2,1,0:T(8,128)} %bitcast.23), calls=%async_computation.4 | async-start | bytes 2097152 | tf_op jit(solution)/shard_map/all_to_all | solution.py:74
  292.3 3.0 fusion.3
  295.3 3.1 fusion.5
  298.4 2.1 collective-permute-start.1
  300.5 3.0 fusion.4
  303.6 34.1 %collective-permute-done.1 = bf16[2,128]{1,0:T(2,128)(2,1)S(1)} collective-permute-done((bf16[2,128]{1,0:T(2,128)(2,1)S(1)}, bf16[2,128]{1,0:T(2,128)(2,1)S(1)}, u32[]{:S(2)}, u32[]{:S(2)}) %collective-permute-start.1) | collective-permute-done | bytes 544 | tf_op jit(solution)/shard_map/ppermute | solution.py:49
  337.6 0.7 fusion.29
  338.3 0.7 fusion.31
  339.0 9.0 %all-to-all-done.4 = f32[32,64,128]{2,1,0:T(8,128)S(1)} async-done(((f32[32,64,128]{2,1,0:T(8,128)}), f32[32,64,128]{2,1,0:T(8,128)S(1)}, u32[]{:S(2)}, u32[]{:S(2)}) %all-to-all-start.4) | async-done | bytes 1048608 | tf_op jit(solution)/shard_map/all_to_all | solution.py:74
  348.0 0.7 reduce_sum.48
  (78 shorter events, 3.1 us)
Async XLA Ops:
  7.2 20.7 %copy-start = (bf16[256,2048]{1,0:T(8,128)(2,1)S(1)}, bf16[256,2048]{1,0:T(8,128)(2,1)}, u32[]{:S(2)}) copy-start(bf16[256,2048]{1,0:T(8,128)(2,1)} %param.12) | copy-start | bytes 3145732
  7.2 6.3 %copy-start.1 = (bf16[256,2048]{1,0:T(8,128)(2,1)S(1)}, bf16[256,2048]{1,0:T(8,128)(2,1)}, u32[]{:S(2)}) copy-start(bf16[256,2048]{1,0:T(8,128)(2,1)} %param.13) | copy-start | bytes 3145732
  7.2 144.9 %all-gather.3.cloned.1.call-start = ((), (), s32[]{:S(2)}) async-start(), calls=%async_computation.5 | async-start | bytes 5570560 | tf_op jit(solution)/shard_map/all_gather | solution.py:27
  17.7 5.5 %copy-start.12 = (f32[256,2]{0,1:T(2,128)S(1)}, f32[256,2]{0,1:T(2,128)}, u32[]{:S(2)}) copy-start(f32[256,2]{0,1:T(2,128)} %param.15) | copy-start | bytes 6148
  37.1 115.0 %copy-start.3 = (bf16[1,64,2048]{2,1,0:T(8,128)(2,1)S(1)}, bf16[1,64,2048]{2,1,0:T(8,128)(2,1)}, u32[]{:S(2)}) copy-start(bf16[1,64,2048]{2,1,0:T(8,128)(2,1)} %param.17) | copy-start | bytes 786436
  83.9 71.0 %copy-start.2 = (bf16[1,64,2048]{2,1,0:T(8,128)(2,1)S(1)}, bf16[1,64,2048]{2,1,0:T(8,128)(2,1)}, u32[]{:S(2)}) copy-start(bf16[1,64,2048]{2,1,0:T(8,128)(2,1)} %param.16) | copy-start | bytes 786436
  152.1 5.6 %copy-start.14 = (bf16[2,640,2048]{2,1,0:T(8,128)(2,1)S(1)}, bf16[2,640,2048]{2,1,0:T(8,128)(2,1)}, u32[]{:S(2)}) copy-start(bf16[2,640,2048]{2,1,0:T(8,128)(2,1)} %all-gather.3.cloned.1.call-done) | copy-start | bytes 15728644
  154.9 3.7 %copy-start.16 = (f32[640,64]{0,1:T(8,128)}, f32[640,64]{0,1:T(8,128)S(1)}, u32[]{:S(2)}) copy-start(f32[640,64]{0,1:T(8,128)S(1)} %fusion.8) | copy-start | bytes 491524
  154.9 2.7 copy-start.15
  157.7 1.0 copy-start.18
  158.6 0.9 copy-start.9
  158.7 0.9 copy-start.7
  203.8 32.6 %all-to-all-start.2 = ((bf16[32,2,1280]{2,1,0:T(2,128)(2,1)}), bf16[32,2,1280]{2,1,0:T(2,128)(2,1)S(1)}, u32[]{:S(2)}, u32[]{:S(2)}) async-start(bf16[32,2,1280]{2,1,0:T(2,128)(2,1)} %reshape.248), calls=%async_computation.2 | async-start | bytes 327680 | tf_op jit(solution)/shard_map/all_to_all | solution.py:165
  236.5 7.3 %copy-start.5 = (bf16[256,128]{1,0:T(8,128)(2,1)S(1)}, bf16[256,128]{1,0:T(8,128)(2,1)}, u32[]{:S(2)}) copy-start(bf16[256,128]{1,0:T(8,128)(2,1)} %param.20) | copy-start | bytes 196612
  236.5 7.3 %copy-start.6 = (bf16[256,128]{1,0:T(8,128)(2,1)S(1)}, bf16[256,128]{1,0:T(8,128)(2,1)}, u32[]{:S(2)}) copy-start(bf16[256,128]{1,0:T(8,128)(2,1)} %param.21) | copy-start | bytes 196612
  236.5 10.9 %copy-start.11 = (bf16[128,64]{0,1:T(8,128)(2,1)S(1)}, bf16[128,64]{0,1:T(8,128)(2,1)}, u32[]{:S(2)}) copy-start(bf16[128,64]{0,1:T(8,128)(2,1)} %param.23) | copy-start | bytes 49156
  236.6 32.4 %copy-start.13 = (f32[3,128]{1,0:T(4,128)S(1)}, f32[3,128]{1,0:T(4,128)}, u32[]{:S(2)}) copy-start(f32[3,128]{1,0:T(4,128)} %param.22) | copy-start | bytes 4612
  239.4 40.2 %all-to-all-start.3 = ((bf16[16,256,128]{2,1,0:T(8,128)(2,1)}), bf16[16,256,128]{2,1,0:T(8,128)(2,1)}, u32[]{:S(2)}, u32[]{:S(2)}) async-start(bf16[16,256,128]{2,1,0:T(8,128)(2,1)} %broadcast_in_dim.52), calls=%async_computation.3 | async-start | bytes 2097152 | tf_op jit(solution)/shard_map/all_to_all | solution.py:32
  243.9 35.8 %collective-permute-start = (bf16[2,128]{1,0:T(2,128)(2,1)S(1)}, bf16[2,128]{1,0:T(2,128)(2,1)S(1)}, u32[]{:S(2)}, u32[]{:S(2)}) collective-permute-start(bf16[2,128]{1,0:T(2,128)(2,1)S(1)} %slice.64), channel_id=1, source_target_pairs={{0,16},{16,32},{32,48},{48,64},{64,80},{80,96},{96,112},{112,128},... | collective-permute-start | bytes 1544 | tf_op jit(solution)/shard_map/ppermute | solution.py:49
  279.7 3.8 %copy-start.4 = (bf16[256,128]{1,0:T(8,128)(2,1)S(1)}, bf16[256,128]{1,0:T(8,128)(2,1)}, u32[]{:S(2)}) copy-start(bf16[256,128]{1,0:T(8,128)(2,1)} %param.19) | copy-start | bytes 196612
  285.7 6.6 %copy-start.10 = (bf16[64,640]{1,0:T(8,128)(2,1)S(1)}, bf16[64,640]{1,0:T(8,128)(2,1)}, u32[]{:S(2)}) copy-start(bf16[64,640]{1,0:T(8,128)(2,1)} %copy-done.9) | copy-start | bytes 245764
  287.1 8.2 %copy-start.17 = (f32[640,64]{0,1:T(8,128)S(1)}, f32[640,64]{0,1:T(8,128)}, u32[]{:S(2)}) copy-start(f32[640,64]{0,1:T(8,128)} %copy-done.16) | copy-start | bytes 491524
  287.1 8.2 %copy-start.19 = (f32[640,64]{0,1:T(8,128)S(1)}, f32[640,64]{0,1:T(8,128)}, u32[]{:S(2)}) copy-start(f32[640,64]{0,1:T(8,128)} %copy-done.18) | copy-start | bytes 491524
  287.1 60.9 %all-to-all-start.4 = ((f32[32,64,128]{2,1,0:T(8,128)}), f32[32,64,128]{2,1,0:T(8,128)S(1)}, u32[]{:S(2)}, u32[]{:S(2)}) async-start(f32[32,64,128]{2,1,0:T(8,128)} %bitcast.23), calls=%async_computation.4 | async-start | bytes 2097152 | tf_op jit(solution)/shard_map/all_to_all | solution.py:74
  295.3 5.2 %copy-start.8 = (bf16[64,640]{1,0:T(8,128)(2,1)S(1)}, bf16[64,640]{1,0:T(8,128)(2,1)}, u32[]{:S(2)}) copy-start(bf16[64,640]{1,0:T(8,128)(2,1)} %copy-done.7) | copy-start | bytes 245764
  298.4 39.3 %collective-permute-start.1 = (bf16[2,128]{1,0:T(2,128)(2,1)S(1)}, bf16[2,128]{1,0:T(2,128)(2,1)S(1)}, u32[]{:S(2)}, u32[]{:S(2)}) collective-permute-start(bf16[2,128]{1,0:T(2,128)(2,1)S(1)} %slice.68), channel_id=1, source_target_pairs={{16,0},{32,16},{48,32},{64,48},{80,64},{96,80},{112,96},{128,112},... | collective-permute-start | bytes 1544 | tf_op jit(solution)/shard_map/ppermute | solution.py:49
Sparse Core Ops, SparseCore 0:
  84.9 67.1 all-gather.2
where the time goes:
time: 357 us; the launch traced here: 356 us
  waiting for transfers between devices  128 us (36%)
  blocking collectives  111 us (31%)
  local copies, waits for them, and re-layouts  37.6 us (11%)
  starting transfers between devices  30.6 us (9%)
  matrix products  20.9 us (6%)
  between operations  14.6 us (4%)
  other arithmetic  12.9 us (4%)
    all_gather x1, waiting for transfers between devices, sent_together(): lax.all_gather(both, axis, axis=dim, tiled=True)  67.3 us
    all_to_all x1, blocking collectives, in_one_piece(): lax.all_to_all(both, axis, split_axis=split_dim, concat_axis=concat_dim,...  44.3 us
    all_to_all x1, blocking collectives, local(): lax.all_to_all(input_part.reshape(local_experts * slot_count, tp_count, w...  37.5 us
    ppermute x2, waiting for transfers between devices, from_behind(): return lax.ppermute(value, axis, pairs)  34.1 us
    all_gather x2, blocking collectives, all_blocks(): blocks = lax.all_gather(blocks, axes[k], axis=0, tiled=True)  29.6 us
    all_to_all x1, waiting for transfers between devices, local(): lax.all_to_all(slot_sums, SP, split_axis=1, concat_axis=0, tiled=True)  17.1 us
    all_to_all x1, starting transfers between devices, local(): lax.all_to_all(slot_sums, SP, split_axis=1, concat_axis=0, tiled=True)  15.4 us
    gather x2, local copies, waits for them, and re-layouts, local(): moe_input[token_row]  9.21 us
  transfers between devices with their start and end apart: 6, of which 4 were waited for; matrix products, arithmetic and copies ran while one was open for 4% of the time, Pallas kernels for 0%

commit v1 on v0

v1 whole, which is shorter than its diff:
```python
import jax
import jax.numpy as jnp
from jax import lax
from jax.sharding import Mesh
from jax.sharding import PartitionSpec as P

SP = ("z", "c")
TP = ("y", "x")
LIMIT = 7.0
ALPHA = 1.702
BF = jnp.bfloat16
F32 = jnp.float32


def swap(blocks, axis):
    return lax.all_to_all(blocks, axis, split_axis=0, concat_axis=0, tiled=True)


def from_everyone(value, axis):
    return swap(jnp.broadcast_to(value, (lax.axis_size(axis), *value.shape)), axis)


def turned(value, axis, by):
    count = lax.axis_size(axis)
    return lax.ppermute(value, axis, [(i, (i + by) % count) for i in range(count)])


def mirrored(value, axis, bit):
    return lax.ppermute(value, axis, [(i, i ^ bit) for i in range(lax.axis_size(axis))])


def doubled(value, axis):
    index = lax.axis_index(axis)
    bit = lax.axis_size(axis) // 2
    while bit:
        other = mirrored(value, axis, bit)
        high = (index & bit) > 0
        both = (jnp.where(high, other, value), jnp.where(high, value, other))
        value = jnp.stack(both, axis=value.ndim - 2)
        bit //= 2
    return value


def from_behind(value, axis, by):
    count = lax.axis_size(axis)
    pairs = [(i, i + by) for i in range(count) if 0 <= i + by < count]
    return lax.ppermute(value, axis, pairs)


def dot(a, b, ca, cb):
    return lax.dot_general(a, b, (((ca,), (cb,)), ((), ())), preferred_element_type=F32)


def expert_cots(rows, grads, gate_w, lin_w, down_w):
    gate_pre = dot(rows, gate_w, 1, 1)
    lin_pre = dot(rows, lin_w, 1, 1)
    act_grad = dot(grads, down_w, 1, 1)
    gate_cut = jnp.minimum(gate_pre, LIMIT)
    lin_cut = jnp.clip(lin_pre, -LIMIT, LIMIT)
    sigma = jax.nn.sigmoid(ALPHA * gate_cut)
    act = (gate_cut * sigma * (lin_cut + 1.0)).astype(BF)
    slope = sigma * (1.0 + ALPHA * gate_cut * (1.0 - sigma))
    gate_cot = jnp.where(gate_pre < LIMIT, act_grad * (lin_cut + 1.0) * slope, 0.0).astype(BF)
    lin_cot = jnp.where(jnp.abs(lin_pre) < LIMIT, act_grad * gate_cut * sigma, 0.0).astype(BF)
    return act, gate_cot, lin_cot


def local(
    moe_input,
    out_grad,
    route_ids,
    route_weights,
    gate_weight,
    lin_weight,
    down_weight,
    outer_gate,
    inner_gate,
    conv_input,
    conv_taps,
    out_proj,
):
    n_sp = lax.axis_size(SP)
    n_z, n_c, n_y, n_x = (lax.axis_size(a) for a in ("z", "c", "y", "x"))
    n_tp = n_y * n_x
    tokens, top = route_ids.shape
    width = moe_input.shape[1]
    wdev = width // n_tp
    wy = width // n_y
    chunks = wy // wdev
    hidden = gate_weight.shape[1]
    experts = n_sp
    cap = 5 * tokens // (2 * experts)
    kx = cap // n_x
    slots = experts * kx
    yi = lax.axis_index("y")
    xi = lax.axis_index("x")

    weights = jnp.concatenate([gate_weight, lin_weight, down_weight], axis=0)
    blocks = [weights] + [turned(weights, "x", d) for d in range(1, n_x)]

    flat = route_ids.reshape(-1)
    order = jnp.arange(flat.shape[0], dtype=jnp.int32)
    same = (flat[:, None] == flat[None, :]) & (order[None, :] < order[:, None])
    rank = jnp.sum(same.astype(jnp.int32), axis=1)
    position = (flat * cap + rank).reshape(tokens, top)
    first, second = position[:, 0], position[:, 1]

    mine = jnp.arange(slots, dtype=jnp.int32)
    mine = (mine // kx) * cap + xi * kx + mine % kx
    hit0 = mine[:, None] == first[None, :]
    hit1 = mine[:, None] == second[None, :]
    pick = (hit0 | hit1).astype(BF)
    slot_weight = jnp.sum(
        jnp.where(hit0, route_weights[:, 0][None, :], 0.0)
        + jnp.where(hit1, route_weights[:, 1][None, :], 0.0),
        axis=1,
    )
    my_rows = lax.dynamic_slice_in_dim(moe_input, yi * wy, wy, 1)
    my_grads = lax.dynamic_slice_in_dim(out_grad, yi * wy, wy, 1)
    send_rows = dot(pick, my_rows, 1, 0).astype(BF)
    send_grads = (slot_weight[:, None] * dot(pick, my_grads, 1, 0)).astype(BF)
    send = jnp.concatenate(
        [a.reshape(experts, kx, chunks, wdev) for a in (send_rows, send_grads)], axis=2
    )
    got = swap(send.reshape(experts, kx * 2 * chunks, wdev), SP)
    got = got.reshape(slots, 2 * chunks, wdev).transpose(1, 0, 2)
    got = from_everyone(got, "y").reshape(n_y, 2, chunks, slots, wdev)
    both = got.transpose(1, 3, 0, 2, 4).reshape(2, slots, width)
    rows, grads = both[0], both[1]

    gate_w, lin_w, down_w = (jnp.concatenate([b[k] for b in blocks], axis=0) for k in range(3))
    act, gate_cot, lin_cot = expert_cots(rows, grads, gate_w, lin_w, down_w)
    part = (dot(gate_cot, gate_w, 1, 0) + dot(lin_cot, lin_w, 1, 0)).astype(BF)
    part = part.reshape(slots, n_tp, wdev).transpose(1, 0, 2)
    part = swap(part, TP).reshape(n_y, n_x, experts, kx, wdev)
    slot_sums = jnp.sum(part.astype(F32), axis=0).astype(BF)
    slot_sums = slot_sums.transpose(1, 0, 2, 3).reshape(experts, cap, wdev)
    returned = swap(slot_sums, SP).reshape(experts * cap, wdev)

    terms = jnp.stack(
        [
            dot(cot, other, 0, 0).astype(BF).reshape(n_x, hidden, width)
            for cot, other in ((gate_cot, rows), (lin_cot, rows), (act, grads))
        ],
        axis=1,
    )
    total = terms[0].astype(F32)
    for d in range(1, n_x):
        total = total + turned(terms[d], "x", -d).astype(F32)
    weight_grads = total.astype(BF)
    gate_grad, lin_grad, down_grad = (weight_grads[k : k + 1] for k in range(3))

    every = jnp.arange(experts * cap, dtype=jnp.int32)[None, :]
    place = ((first[:, None] == every) | (second[:, None] == every)).astype(BF)
    row_grads = dot(place, returned, 1, 0).astype(BF)
    full_rows = from_everyone(row_grads, TP).transpose(1, 0, 2).reshape(tokens, width)
    stream_grad = (out_grad.astype(F32) + full_rows.astype(F32)).astype(BF)

    taps = conv_taps.shape[0]
    conv_values = (inner_gate.astype(F32) * conv_input.astype(F32)).astype(BF)
    prior_rows = from_behind(conv_values[tokens - (taps - 1) :], SP, 1)
    extended = jnp.concatenate([prior_rows, conv_values], axis=0).astype(F32)
    convolved = jnp.zeros((tokens, wdev), F32)
    for tap in range(taps):
        convolved = convolved + conv_taps[tap][None, :] * extended[tap : tap + tokens]
    mixed = (outer_gate.astype(F32) * convolved).astype(BF)

    proj = doubled(doubled(out_proj.T, "z"), "c").reshape(width, wdev)
    mixed_grad = dot(stream_grad, proj, 1, 0)
    terms = dot(stream_grad, mixed, 0, 0).astype(BF).reshape(n_z, n_c, -1, wdev)
    terms = swap(terms.transpose(1, 0, 2, 3), "c")
    terms = jnp.sum(terms.astype(F32), axis=0).astype(BF)
    out_proj_grad = jnp.sum(swap(terms, "z").astype(F32), axis=0)

    outer_gate_grad = (mixed_grad * convolved).astype(BF)
    conv_cot = (mixed_grad * outer_gate.astype(F32)).astype(BF)
    later_rows = from_behind(conv_cot[: taps - 1], SP, -1)
    extended_cot = jnp.concatenate([conv_cot, later_rows], axis=0).astype(F32)
    value_grad = jnp.zeros((tokens, wdev), F32)
    for tap in range(taps):
        start = taps - 1 - tap
        value_grad = value_grad + conv_taps[tap][None, :] * extended_cot[start : start + tokens]
    inner_gate_grad = (value_grad * conv_input.astype(F32)).astype(BF)
    conv_input_grad = (value_grad * inner_gate.astype(F32)).astype(BF)
    return (
        gate_grad,
        lin_grad,
        down_grad,
        out_proj_grad,
        outer_gate_grad,
        inner_gate_grad,
        conv_input_grad,
    )


def solution(mesh):
    torus = Mesh(mesh.devices.reshape(-1, 2, 4, 4), ("z", "c", "y", "x"))
    tokens = P(SP, None)
    expert = P(SP, TP, None)
    mixer = P(SP, TP)
    return jax.shard_map(
        local,
        mesh=torus,
        in_specs=(tokens,) * 4 + (expert,) * 3 + (mixer,) * 3 + (P(None, TP), P(TP, SP)),
        out_specs=(expert,) * 3 + (mixer,) * 4,
        check_vma=False,
    )
```

time: 357 us -> 249 us (0.70)
  the two profiles are of different devices: /device:TPU:1 before, /device:TPU:32 now
where the time goes in v1:
time: 249 us; the launch traced here: 247 us
  starting transfers between devices  104 us (42%)
  waiting for transfers between devices  79.7 us (32%)
  local copies, waits for them, and re-layouts  32.7 us (13%)
  other arithmetic  15 us (6%)
  matrix products  10.3 us (4%)
  blocking collectives  4.29 us (2%)
    all_to_all x6, starting transfers between devices, swap(): return lax.all_to_all(blocks, axis, split_axis=0, concat_axis=0, tiled=True)  48 us
    all_to_all x6, waiting for transfers between devices, swap(): return lax.all_to_all(blocks, axis, split_axis=0, concat_axis=0, tiled=True)  45.8 us
    ppermute x5, starting transfers between devices, mirrored(): lax.ppermute(value, axis, [(i, i ^ bit) for i in range(lax.axis_size(axis...  32 us
    ppermute x6, waiting for transfers between devices, turned(): lax.ppermute(value, axis, [(i, (i + by) % count) for i in range(count)])  20.6 us
    ppermute x6, starting transfers between devices, turned(): lax.ppermute(value, axis, [(i, (i + by) % count) for i in range(count)])  19.7 us
    ppermute x5, waiting for transfers between devices, mirrored(): lax.ppermute(value, axis, [(i, i ^ bit) for i in range(lax.axis_size(axis...  13.3 us
    dot_general x13, matrix products, dot(): lax.dot_general(a, b, (((ca,), (cb,)), ((), ())), preferred_element_type=...  10.3 us
    unnamed x77, local copies, waits for them, and re-layouts  7.07 us
  transfers between devices with their start and end apart: 19, of which 9 were waited for; matrix products, arithmetic and copies ran while one was open for 19% of the time, Pallas kernels for 0%

profile of v1, /device:TPU:32, one launch (start us, length us, event | category | flops | bytes accessed | tf_op | source)
XLA Modules:
  0.0 247.0 jit_solution(13617965257984226224)
XLA Ops:
  0.7 1.8 constant_dynamic-update-slice_fusion.2
  2.5 1.7 constant_dynamic-update-slice_fusion.1
  4.2 1.7 constant_dynamic-update-slice_fusion
  5.9 3.4 %collective-permute-start = (bf16[3,64,2048]{2,1,0:T(8,128)(2,1)}, bf16[3,64,2048]{2,1,0:T(8,128)(2,1)}, u32[]{:S(2)}, u32[]{:S(2)}) collective-permute-start(bf16[3,64,2048]{2,1,0:T(8,128)(2,1)} %constant_dynamic-update-slice_fusion), channel_id=1, source_target_pairs={{0,1},{1,2},{2,3},{3,0},{4,5},{5,6},{6,7},{7,4},{8,9},{9,10},{10,1... | collective-permute-start | bytes 2359304 | tf_op jit(solution)/shard_map/ppermute | solution.py:25
  9.3 4.6 %collective-permute-start.1 = (bf16[3,64,2048]{2,1,0:T(8,128)(2,1)}, bf16[3,64,2048]{2,1,0:T(8,128)(2,1)}, u32[]{:S(2)}, u32[]{:S(2)}) collective-permute-start(bf16[3,64,2048]{2,1,0:T(8,128)(2,1)} %constant_dynamic-update-slice_fusion), channel_id=1, source_target_pairs={{0,2},{1,3},{2,0},{3,1},{4,6},{5,7},{6,4},{7,5},{8,10},{9,11},{10,... | collective-permute-start | bytes 2359304 | tf_op jit(solution)/shard_map/ppermute | solution.py:25
  14.0 3.3 %collective-permute-start.2 = (bf16[3,64,2048]{2,1,0:T(8,128)(2,1)}, bf16[3,64,2048]{2,1,0:T(8,128)(2,1)}, u32[]{:S(2)}, u32[]{:S(2)}) collective-permute-start(bf16[3,64,2048]{2,1,0:T(8,128)(2,1)} %constant_dynamic-update-slice_fusion), channel_id=1, source_target_pairs={{0,3},{1,0},{2,1},{3,2},{4,7},{5,4},{6,5},{7,6},{8,11},{9,8},{10,9... | collective-permute-start | bytes 2359304 | tf_op jit(solution)/shard_map/ppermute | solution.py:25
  17.3 14.8 %collective-permute-start.7 = (bf16[64,128]{1,0:T(8,128)(2,1)}, bf16[64,128]{1,0:T(8,128)(2,1)S(1)}, u32[]{:S(2)}, u32[]{:S(2)}) collective-permute-start(bf16[64,128]{1,0:T(8,128)(2,1)} %bitcast.145), channel_id=1, source_target_pairs={{0,256},{32,288},{64,320},{96,352},{128,384},{160,416},{192,448},{... | collective-permute-start | bytes 49160 | tf_op jit(solution)/shard_map/ppermute | solution.py:29
  34.5 6.5 %collective-permute-start.8 = (bf16[2,64,128]{2,1,0:T(8,128)(2,1)S(1)}, bf16[2,64,128]{2,1,0:T(8,128)(2,1)S(1)}, u32[]{:S(2)}, u32[]{:S(2)}) collective-permute-start(bf16[2,64,128]{2,1,0:T(8,128)(2,1)S(1)} %pad_maximum_fusion.11), channel_id=1, source_target_pairs={{0,128},{32,160},{64,192},{96,224},{128,0},{160,32},{192,64},{224,... | collective-permute-start | bytes 98312 | tf_op jit(solution)/shard_map/ppermute | solution.py:29
  41.9 10.6 %all-to-all-start = ((bf16[32,40,128]{2,1,0:T(8,128)(2,1)}), bf16[32,40,128]{2,1,0:T(8,128)(2,1)S(1)}, u32[]{:S(2)}, u32[]{:S(2)}) async-start(bf16[32,40,128]{2,1,0:T(8,128)(2,1)} %maximum_bitcast_fusion), calls=%async_computation | async-start | bytes 655360 | tf_op jit(solution)/shard_map/all_to_all | solution.py:16
  52.5 4.3 %collective-permute-start.9 = (bf16[2,2,64,128]{3,2,1,0:T(8,128)(2,1)S(1)}, bf16[2,2,64,128]{3,2,1,0:T(8,128)(2,1)S(1)}, u32[]{:S(2)}, u32[]{:S(2)}) collective-permute-start(bf16[2,2,64,128]{3,2,1,0:T(8,128)(2,1)S(1)} %pad_maximum_fusion.10), channel_id=1, source_target_pairs={{0,64},{32,96},{64,0},{96,32},{128,192},{160,224},{192,128},{224,1... | collective-permute-start | bytes 196616 | tf_op jit(solution)/shard_map/ppermute | solution.py:29
  57.4 1.9 collective-permute-start.6
  59.3 10.9 %collective-permute-done.9 = bf16[2,2,64,128]{3,2,1,0:T(8,128)(2,1)S(1)} collective-permute-done((bf16[2,2,64,128]{3,2,1,0:T(8,128)(2,1)S(1)}, bf16[2,2,64,128]{3,2,1,0:T(8,128)(2,1)S(1)}, u32[]{:S(2)}, u32[]{:S(2)}) %collective-permute-start.9) | collective-permute-done | bytes 65568 | tf_op jit(solution)/shard_map/ppermute | solution.py:29
  71.0 4.4 %collective-permute-start.10 = (bf16[2,2,2,64,128]{4,3,2,1,0:T(8,128)(2,1)}, bf16[2,2,2,64,128]{4,3,2,1,0:T(8,128)(2,1)}, u32[]{:S(2)}, u32[]{:S(2)}) collective-permute-start(bf16[2,2,2,64,128]{4,3,2,1,0:T(8,128)(2,1)} %pad_maximum_fusion.9), channel_id=1, source_target_pairs={{0,32},{32,0},{64,96},{96,64},{128,160},{160,128},{192,224},{224,1... | collective-permute-start | bytes 393224 | tf_op jit(solution)/shard_map/ppermute | solution.py:29
  76.5 2.4 collective-permute-done.10
  78.9 1.6 select_bitcast_fusion.3
  80.5 1.3 broadcast_in_dim.42
  81.8 4.5 %all-to-all-start.1 = ((bf16[4,8,160,128]{3,2,1,0:T(8,128)(2,1)}), bf16[4,8,160,128]{3,2,1,0:T(8,128)(2,1)S(1)}, u32[]{:S(2)}, u32[]{:S(2)}) async-start(bf16[4,8,160,128]{3,2,1,0:T(8,128)(2,1)} %broadcast_in_dim.42), calls=%async_computation.1 | async-start | bytes 2621440 | tf_op jit(solution)/shard_map/all_to_all | solution.py:16
  86.3 2.1 slice_bitcast_fusion.9
  88.3 2.0 slice_bitcast_fusion.8
  90.4 2.0 slice_bitcast_fusion.7
  92.4 10.9 %all-to-all-done.1 = bf16[4,8,160,128]{3,2,1,0:T(8,128)(2,1)S(1)} async-done(((bf16[4,8,160,128]{3,2,1,0:T(8,128)(2,1)}), bf16[4,8,160,128]{3,2,1,0:T(8,128)(2,1)S(1)}, u32[]{:S(2)}, u32[]{:S(2)}) %all-to-all-start.1) | async-done | bytes 1310752 | tf_op jit(solution)/shard_map/all_to_all | solution.py:16
  105.4 1.6 squeeze.52
  108.2 1.6 squeeze.57
  109.8 1.8 fusion.24
  114.4 1.5 convolution_convert_fusion.2
  117.2 4.3 %all-to-all-start.2 = ((bf16[16,160,128]{2,1,0:T(8,128)(2,1)}), bf16[16,160,128]{2,1,0:T(8,128)(2,1)}, u32[]{:S(2)}, u32[]{:S(2)}) async-start(bf16[16,160,128]{2,1,0:T(8,128)(2,1)} %bitcast.133), calls=%async_computation.2 | async-start | bytes 1310720 | tf_op jit(solution)/shard_map/all_to_all | solution.py:16
  121.5 1.4 convolution_convert_fusion.1
  122.9 1.5 convolution_convert_fusion
  124.4 1.9 pad_maximum_fusion
  126.3 6.4 %all-to-all-done.2 = bf16[16,160,128]{2,1,0:T(8,128)(2,1)} async-done(((bf16[16,160,128]{2,1,0:T(8,128)(2,1)}), bf16[16,160,128]{2,1,0:T(8,128)(2,1)}, u32[]{:S(2)}, u32[]{:S(2)}) %all-to-all-start.2) | async-done | bytes 655392 | tf_op jit(solution)/shard_map/all_to_all | solution.py:16
  134.8 12.3 %all-to-all-start.3 = ((bf16[32,20,128]{2,1,0:T(8,128)(2,1)}), bf16[32,20,128]{2,1,0:T(8,128)(2,1)S(1)}, u32[]{:S(2)}, u32[]{:S(2)}) async-start(bf16[32,20,128]{2,1,0:T(8,128)(2,1)} %copy.132), calls=%async_computation.3 | async-start | bytes 393216 | tf_op jit(solution)/shard_map/all_to_all | solution.py:16
  147.1 3.2 %slice_bitcast_fusion.2 = (bf16[3,64,2048]{2,1,0:T(8,128)(2,1)}, bf16[3,64,2048]{2,1,0:T(8,128)(2,1)}, bf16[3,64,2048]{2,1,0:T(8,128)(2,1)}) fusion(bf16[4,3,64,2048]{3,2,1,0:T(8,128)(2,1)} %pad_maximum_fusion), kind=kLoop, calls=%fused_computation.33 | loop fusion | bytes 4718592 | tf_op jit(solution)/shard_map/squeeze | solution.py:149
  150.3 2.4 collective-permute-start.3
  152.7 4.1 %collective-permute-start.4 = (bf16[3,64,2048]{2,1,0:T(8,128)(2,1)}, bf16[3,64,2048]{2,1,0:T(8,128)(2,1)}, u32[]{:S(2)}, u32[]{:S(2)}) collective-permute-start(bf16[3,64,2048]{2,1,0:T(8,128)(2,1)} %get-tuple-element.13), channel_id=1, source_target_pairs={{0,2},{1,3},{2,0},{3,1},{4,6},{5,7},{6,4},{7,5},{8,10},{9,11},{10,... | collective-permute-start | bytes 2359304 | tf_op jit(solution)/shard_map/ppermute | solution.py:25
  156.8 1.9 collective-permute-start.5
  158.8 2.1 collective-permute-start.11
  160.8 4.6 %all-to-all-done.3 = bf16[32,20,128]{2,1,0:T(8,128)(2,1)S(1)} async-done(((bf16[32,20,128]{2,1,0:T(8,128)(2,1)}), bf16[32,20,128]{2,1,0:T(8,128)(2,1)S(1)}, u32[]{:S(2)}, u32[]{:S(2)}) %all-to-all-start.3) | async-done | bytes 163872 | tf_op jit(solution)/shard_map/all_to_all | solution.py:16
  165.8 1.2 broadcast_in_dim.43
  167.0 4.5 %all-to-all-start.4 = ((bf16[16,256,128]{2,1,0:T(8,128)(2,1)}), bf16[16,256,128]{2,1,0:T(8,128)(2,1)}, u32[]{:S(2)}, u32[]{:S(2)}) async-start(bf16[16,256,128]{2,1,0:T(8,128)(2,1)} %broadcast_in_dim.43), calls=%async_computation.4 | async-start | bytes 2097152 | tf_op jit(solution)/shard_map/all_to_all | solution.py:16
  173.2 3.7 %collective-permute-done.4 = bf16[3,64,2048]{2,1,0:T(8,128)(2,1)} collective-permute-done((bf16[3,64,2048]{2,1,0:T(8,128)(2,1)}, bf16[3,64,2048]{2,1,0:T(8,128)(2,1)}, u32[]{:S(2)}, u32[]{:S(2)}) %collective-permute-start.4) | collective-permute-done | bytes 786464 | tf_op jit(solution)/shard_map/ppermute | solution.py:25
  176.9 16.9 %collective-permute-done.5 = bf16[3,64,2048]{2,1,0:T(8,128)(2,1)} collective-permute-done((bf16[3,64,2048]{2,1,0:T(8,128)(2,1)}, bf16[3,64,2048]{2,1,0:T(8,128)(2,1)}, u32[]{:S(2)}, u32[]{:S(2)}) %collective-permute-start.5) | collective-permute-done | bytes 786464 | tf_op jit(solution)/shard_map/ppermute | solution.py:25
  193.8 3.4 %fusion.4 = bf16[3,64,2048]{2,1,0:T(8,128)(2,1)} fusion(bf16[3,64,2048]{2,1,0:T(8,128)(2,1)} %collective-permute-done.5, bf16[3,64,2048]{2,1,0:T(8,128)(2,1)} %collective-permute-done.4, bf16[3,64,2048]{2,1,0:T(8,128)(2,1)} %collective-permute-done.3, bf16[4,3,64,2048]{3,2,1,0:T(8,128)(2,1)} %pad_maximum_fusion), kind=kLoop, calls=%fused_computation.12 | loop fusion | flops 3145728 | bytes 3932160 | tf_op jit(solution)/shard_map/convert_element_type | solution.py:150
  197.1 7.8 %all-to-all-done.4 = bf16[16,256,128]{2,1,0:T(8,128)(2,1)} async-done(((bf16[16,256,128]{2,1,0:T(8,128)(2,1)}), bf16[16,256,128]{2,1,0:T(8,128)(2,1)}, u32[]{:S(2)}, u32[]{:S(2)}) %all-to-all-start.4) | async-done | bytes 1048608 | tf_op jit(solution)/shard_map/all_to_all | solution.py:16
  204.9 1.5 copy.133
  208.6 1.9 collective-permute-start.12
  211.0 4.3 %all_to_all.35 = bf16[2,16,64,128]{3,2,1,0:T(8,128)(2,1)S(1)} all-to-all(bf16[2,16,64,128]{3,2,1,0:T(8,128)(2,1)S(1)} %bitcast.135), channel_id=1, replica_groups=mesh['z'=16,'c'=2,'y'=4,'x'=4] {'c'}, dimensions={0} | all-to-all | bytes 1048576 | tf_op jit(solution)/shard_map/all_to_all | solution.py:16
  216.2 11.8 %all-to-all-start.6 = ((bf16[16,64,128]{2,1,0:T(8,128)(2,1)}), bf16[16,64,128]{2,1,0:T(8,128)(2,1)S(1)}, u32[]{:S(2)}, u32[]{:S(2)}) async-start(bf16[16,64,128]{2,1,0:T(8,128)(2,1)} %reduce_sum.57), calls=%async_computation.6 | async-start | bytes 524288 | tf_op jit(solution)/shard_map/all_to_all | solution.py:16
  230.3 16.1 %all-to-all-done.6 = bf16[16,64,128]{2,1,0:T(8,128)(2,1)S(1)} async-done(((bf16[16,64,128]{2,1,0:T(8,128)(2,1)}), bf16[16,64,128]{2,1,0:T(8,128)(2,1)S(1)}, u32[]{:S(2)}, u32[]{:S(2)}) %all-to-all-start.6) | async-done | bytes 262176 | tf_op jit(solution)/shard_map/all_to_all | solution.py:16
  (137 shorter events, 23.3 us)
Async XLA Ops:
  0.6 33.5 %copy-start = (bf16[256,2048]{1,0:T(8,128)(2,1)S(1)}, bf16[256,2048]{1,0:T(8,128)(2,1)}, u32[]{:S(2)}) copy-start(bf16[256,2048]{1,0:T(8,128)(2,1)} %param.12) | copy-start | bytes 3145732
  0.6 33.8 %copy-start.31 = (bf16[128,64]{0,1:T(8,128)(2,1)S(1)}, bf16[128,64]{0,1:T(8,128)(2,1)}, u32[]{:S(2)}) copy-start(bf16[128,64]{0,1:T(8,128)(2,1)} %param.23) | copy-start | bytes 49156
  0.7 33.0 %copy-start.32 = (s32[256,2]{0,1:T(2,128)S(1)}, s32[256,2]{0,1:T(2,128)}, u32[]{:S(2)}) copy-start(s32[256,2]{0,1:T(2,128)} %param.14) | copy-start | bytes 6148
  0.7 33.0 %copy-start.34 = (f32[256,2]{0,1:T(2,128)S(1)}, f32[256,2]{0,1:T(2,128)}, u32[]{:S(2)}) copy-start(f32[256,2]{0,1:T(2,128)} %param.15) | copy-start | bytes 6148
  0.7 33.2 %copy-start.6 = (bf16[256,2048]{1,0:T(8,128)(2,1)S(1)}, bf16[256,2048]{1,0:T(8,128)(2,1)}, u32[]{:S(2)}) copy-start(bf16[256,2048]{1,0:T(8,128)(2,1)} %param.13) | copy-start | bytes 3145732
  4.2 52.6 %copy-start.10 = (bf16[256,128]{1,0:T(8,128)(2,1)S(1)}, bf16[256,128]{1,0:T(8,128)(2,1)}, u32[]{:S(2)}) copy-start(bf16[256,128]{1,0:T(8,128)(2,1)} %param.20) | copy-start | bytes 196612
  4.2 52.6 %copy-start.17 = (bf16[256,128]{1,0:T(8,128)(2,1)S(1)}, bf16[256,128]{1,0:T(8,128)(2,1)}, u32[]{:S(2)}) copy-start(bf16[256,128]{1,0:T(8,128)(2,1)} %param.21) | copy-start | bytes 196612
  5.9 80.4 %collective-permute-start = (bf16[3,64,2048]{2,1,0:T(8,128)(2,1)}, bf16[3,64,2048]{2,1,0:T(8,128)(2,1)}, u32[]{:S(2)}, u32[]{:S(2)}) collective-permute-start(bf16[3,64,2048]{2,1,0:T(8,128)(2,1)} %constant_dynamic-update-slice_fusion), channel_id=1, source_target_pairs={{0,1},{1,2},{2,3},{3,0},{4,5},{5,6},{6,7},{7,4},{8,9},{9,10},{10,1... | collective-permute-start | bytes 2359304 | tf_op jit(solution)/shard_map/ppermute | solution.py:25
  9.3 79.0 %collective-permute-start.1 = (bf16[3,64,2048]{2,1,0:T(8,128)(2,1)}, bf16[3,64,2048]{2,1,0:T(8,128)(2,1)}, u32[]{:S(2)}, u32[]{:S(2)}) collective-permute-start(bf16[3,64,2048]{2,1,0:T(8,128)(2,1)} %constant_dynamic-update-slice_fusion), channel_id=1, source_target_pairs={{0,2},{1,3},{2,0},{3,1},{4,6},{5,7},{6,4},{7,5},{8,10},{9,11},{10,... | collective-permute-start | bytes 2359304 | tf_op jit(solution)/shard_map/ppermute | solution.py:25
  14.0 76.4 %collective-permute-start.2 = (bf16[3,64,2048]{2,1,0:T(8,128)(2,1)}, bf16[3,64,2048]{2,1,0:T(8,128)(2,1)}, u32[]{:S(2)}, u32[]{:S(2)}) collective-permute-start(bf16[3,64,2048]{2,1,0:T(8,128)(2,1)} %constant_dynamic-update-slice_fusion), channel_id=1, source_target_pairs={{0,3},{1,0},{2,1},{3,2},{4,7},{5,4},{6,5},{7,6},{8,11},{9,8},{10,9... | collective-permute-start | bytes 2359304 | tf_op jit(solution)/shard_map/ppermute | solution.py:25
  17.3 17.2 %collective-permute-start.7 = (bf16[64,128]{1,0:T(8,128)(2,1)}, bf16[64,128]{1,0:T(8,128)(2,1)S(1)}, u32[]{:S(2)}, u32[]{:S(2)}) collective-permute-start(bf16[64,128]{1,0:T(8,128)(2,1)} %bitcast.145), channel_id=1, source_target_pairs={{0,256},{32,288},{64,320},{96,352},{128,384},{160,416},{192,448},{... | collective-permute-start | bytes 49160 | tf_op jit(solution)/shard_map/ppermute | solution.py:29
  33.5 41.9 %copy-start.35 = (f32[3,128]{1,0:T(4,128)S(1)}, f32[3,128]{1,0:T(4,128)}, u32[]{:S(2)}) copy-start(f32[3,128]{1,0:T(4,128)} %param.22) | copy-start | bytes 4612
  34.5 17.9 %collective-permute-start.8 = (bf16[2,64,128]{2,1,0:T(8,128)(2,1)S(1)}, bf16[2,64,128]{2,1,0:T(8,128)(2,1)S(1)}, u32[]{:S(2)}, u32[]{:S(2)}) collective-permute-start(bf16[2,64,128]{2,1,0:T(8,128)(2,1)S(1)} %pad_maximum_fusion.11), channel_id=1, source_target_pairs={{0,128},{32,160},{64,192},{96,224},{128,0},{160,32},{192,64},{224,... | collective-permute-start | bytes 98312 | tf_op jit(solution)/shard_map/ppermute | solution.py:29
  41.9 38.6 %all-to-all-start = ((bf16[32,40,128]{2,1,0:T(8,128)(2,1)}), bf16[32,40,128]{2,1,0:T(8,128)(2,1)S(1)}, u32[]{:S(2)}, u32[]{:S(2)}) async-start(bf16[32,40,128]{2,1,0:T(8,128)(2,1)} %maximum_bitcast_fusion), calls=%async_computation | async-start | bytes 655360 | tf_op jit(solution)/shard_map/all_to_all | solution.py:16
  52.5 17.7 %collective-permute-start.9 = (bf16[2,2,64,128]{3,2,1,0:T(8,128)(2,1)S(1)}, bf16[2,2,64,128]{3,2,1,0:T(8,128)(2,1)S(1)}, u32[]{:S(2)}, u32[]{:S(2)}) collective-permute-start(bf16[2,2,64,128]{3,2,1,0:T(8,128)(2,1)S(1)} %pad_maximum_fusion.10), channel_id=1, source_target_pairs={{0,64},{32,96},{64,0},{96,32},{128,192},{160,224},{192,128},{224,1... | collective-permute-start | bytes 196616 | tf_op jit(solution)/shard_map/ppermute | solution.py:29
  56.9 18.5 %copy-start.12 = (bf16[256,128]{1,0:T(8,128)(2,1)}, bf16[256,128]{1,0:T(8,128)(2,1)S(1)}, u32[]{:S(2)}) copy-start(bf16[256,128]{1,0:T(8,128)(2,1)S(1)} %fusion.30) | copy-start | bytes 196612
  57.4 114.2 %collective-permute-start.6 = (bf16[2,128]{1,0:T(2,128)(2,1)}, bf16[2,128]{1,0:T(2,128)(2,1)}, u32[]{:S(2)}, u32[]{:S(2)}) collective-permute-start(bf16[2,128]{1,0:T(2,128)(2,1)} %slice.157), channel_id=1, source_target_pairs={{0,16},{16,32},{32,48},{48,64},{64,80},{80,96},{96,112},{112,128},... | collective-permute-start | bytes 1544 | tf_op jit(solution)/shard_map/ppermute | solution.py:47
  70.3 5.1 %copy-start.7 = (bf16[2,2,1,64,128]{4,3,2,1,0:T(8,128)(2,1)}, bf16[2,2,1,64,128]{4,3,2,1,0:T(8,128)(2,1)S(1)}, u32[]{:S(2)}) copy-start(bf16[2,2,1,64,128]{4,3,2,1,0:T(8,128)(2,1)S(1)} %get-tuple-element.35) | copy-start | bytes 196612
  70.3 5.1 %copy-start.8 = (bf16[2,2,1,64,128]{4,3,2,1,0:T(8,128)(2,1)}, bf16[2,2,1,64,128]{4,3,2,1,0:T(8,128)(2,1)S(1)}, u32[]{:S(2)}) copy-start(bf16[2,2,1,64,128]{4,3,2,1,0:T(8,128)(2,1)S(1)} %get-tuple-element.36) | copy-start | bytes 196612
  71.0 7.9 %collective-permute-start.10 = (bf16[2,2,2,64,128]{4,3,2,1,0:T(8,128)(2,1)}, bf16[2,2,2,64,128]{4,3,2,1,0:T(8,128)(2,1)}, u32[]{:S(2)}, u32[]{:S(2)}) collective-permute-start(bf16[2,2,2,64,128]{4,3,2,1,0:T(8,128)(2,1)} %pad_maximum_fusion.9), channel_id=1, source_target_pairs={{0,32},{32,0},{64,96},{96,64},{128,160},{160,128},{192,224},{224,1... | collective-permute-start | bytes 393224 | tf_op jit(solution)/shard_map/ppermute | solution.py:29
  81.8 21.5 %all-to-all-start.1 = ((bf16[4,8,160,128]{3,2,1,0:T(8,128)(2,1)}), bf16[4,8,160,128]{3,2,1,0:T(8,128)(2,1)S(1)}, u32[]{:S(2)}, u32[]{:S(2)}) async-start(bf16[4,8,160,128]{3,2,1,0:T(8,128)(2,1)} %broadcast_in_dim.42), calls=%async_computation.1 | async-start | bytes 2621440 | tf_op jit(solution)/shard_map/all_to_all | solution.py:16
  104.2 2.8 %copy-start.3 = (bf16[1,160,4,4,128]{4,1,3,0,2:T(8,128)(2,1)S(1)}, bf16[1,160,4,4,128]{4,1,3,0,2:T(8,128)(2,1)}, u32[]{:S(2)}) copy-start(bf16[1,160,4,4,128]{4,1,3,0,2:T(8,128)(2,1)} %get-tuple-element.15) | copy-start | bytes 1966084
  109.7 1.8 copy-start.16
  109.8 1.8 copy-start.19
  109.8 1.8 copy-start.21
  109.8 1.8 copy-start.25
  111.6 1.0 copy-start.22
  111.6 1.1 copy-start.24
  111.6 1.2 copy-start.27
  112.2 1.2 copy-start.29
  112.8 1.1 copy-start.23
  112.8 1.2 copy-start.26
  117.2 15.5 %all-to-all-start.2 = ((bf16[16,160,128]{2,1,0:T(8,128)(2,1)}), bf16[16,160,128]{2,1,0:T(8,128)(2,1)}, u32[]{:S(2)}, u32[]{:S(2)}) async-start(bf16[16,160,128]{2,1,0:T(8,128)(2,1)} %bitcast.133), calls=%async_computation.2 | async-start | bytes 1310720 | tf_op jit(solution)/shard_map/all_to_all | solution.py:16
  121.5 2.9 %copy-start.1 = (bf16[256,2048]{1,0:T(8,128)(2,1)S(1)}, bf16[256,2048]{1,0:T(8,128)(2,1)}, u32[]{:S(2)}) copy-start(bf16[256,2048]{1,0:T(8,128)(2,1)} %convolution_convert_fusion.2) | copy-start | bytes 3145732
  134.8 30.7 %all-to-all-start.3 = ((bf16[32,20,128]{2,1,0:T(8,128)(2,1)}), bf16[32,20,128]{2,1,0:T(8,128)(2,1)S(1)}, u32[]{:S(2)}, u32[]{:S(2)}) async-start(bf16[32,20,128]{2,1,0:T(8,128)(2,1)} %copy.132), calls=%async_computation.3 | async-start | bytes 393216 | tf_op jit(solution)/shard_map/all_to_all | solution.py:16
  147.1 11.6 %copy-start.5 = (bf16[2,2,2,1,64,128]{5,4,3,2,1,0:T(8,128)(2,1)S(1)}, bf16[2,2,2,1,64,128]{5,4,3,2,1,0:T(8,128)(2,1)}, u32[]{:S(2)}) copy-start(bf16[2,2,2,1,64,128]{5,4,3,2,1,0:T(8,128)(2,1)} %get-tuple-element.33) | copy-start | bytes 393220
  150.3 22.8 %collective-permute-start.3 = (bf16[3,64,2048]{2,1,0:T(8,128)(2,1)}, bf16[3,64,2048]{2,1,0:T(8,128)(2,1)}, u32[]{:S(2)}, u32[]{:S(2)}) collective-permute-start(bf16[3,64,2048]{2,1,0:T(8,128)(2,1)} %get-tuple-element.11), channel_id=1, source_target_pairs={{0,3},{1,0},{2,1},{3,2},{4,7},{5,4},{6,5},{7,6},{8,11},{9,8},{10,9... | collective-permute-start | bytes 2359304 | tf_op jit(solution)/shard_map/ppermute | solution.py:25
  152.7 24.2 %collective-permute-start.4 = (bf16[3,64,2048]{2,1,0:T(8,128)(2,1)}, bf16[3,64,2048]{2,1,0:T(8,128)(2,1)}, u32[]{:S(2)}, u32[]{:S(2)}) collective-permute-start(bf16[3,64,2048]{2,1,0:T(8,128)(2,1)} %get-tuple-element.13), channel_id=1, source_target_pairs={{0,2},{1,3},{2,0},{3,1},{4,6},{5,7},{6,4},{7,5},{8,10},{9,11},{10,... | collective-permute-start | bytes 2359304 | tf_op jit(solution)/shard_map/ppermute | solution.py:25
  156.8 37.0 %collective-permute-start.5 = (bf16[3,64,2048]{2,1,0:T(8,128)(2,1)}, bf16[3,64,2048]{2,1,0:T(8,128)(2,1)}, u32[]{:S(2)}, u32[]{:S(2)}) collective-permute-start(bf16[3,64,2048]{2,1,0:T(8,128)(2,1)} %get-tuple-element.12), channel_id=1, source_target_pairs={{0,1},{1,2},{2,3},{3,0},{4,5},{5,6},{6,7},{7,4},{8,9},{9,10},{10,1... | collective-permute-start | bytes 2359304 | tf_op jit(solution)/shard_map/ppermute | solution.py:25
  158.8 12.8 %copy-start.13 = (bf16[256,128]{1,0:T(8,128)(2,1)S(1)}, bf16[256,128]{1,0:T(8,128)(2,1)}, u32[]{:S(2)}) copy-start(bf16[256,128]{1,0:T(8,128)(2,1)} %copy-done.12) | copy-start | bytes 196612
  158.8 13.5 %collective-permute-start.11 = (bf16[2,2,2,2,64,128]{5,4,3,2,1,0:T(8,128)(2,1)S(1)}, bf16[2,2,2,2,64,128]{5,4,3,2,1,0:T(8,128)(2,1)S(1)}, u32[]{:S(2)}, u32[]{:S(2)}) collective-permute-start(bf16[2,2,2,2,64,128]{5,4,3,2,1,0:T(8,128)(2,1)S(1)} %pad_maximum_fusion.4), channel_id=1, source_target_pairs={{0,16},{16,0},{1,17},{17,1},{2,18},{18,2},{3,19},{19,3},{4,20},{20... | collective-permute-start | bytes 786440 | tf_op jit(solution)/shard_map/ppermute | solution.py:29
  167.0 37.9 %all-to-all-start.4 = ((bf16[16,256,128]{2,1,0:T(8,128)(2,1)}), bf16[16,256,128]{2,1,0:T(8,128)(2,1)}, u32[]{:S(2)}, u32[]{:S(2)}) async-start(bf16[16,256,128]{2,1,0:T(8,128)(2,1)} %broadcast_in_dim.43), calls=%async_computation.4 | async-start | bytes 2097152 | tf_op jit(solution)/shard_map/all_to_all | solution.py:16
  206.4 1.0 copy-start.4
  208.6 20.3 %collective-permute-start.12 = (bf16[2,128]{1,0:T(2,128)(2,1)S(1)}, bf16[2,128]{1,0:T(2,128)(2,1)S(1)}, u32[]{:S(2)}, u32[]{:S(2)}) collective-permute-start(bf16[2,128]{1,0:T(2,128)(2,1)S(1)} %slice.161), channel_id=1, source_target_pairs={{16,0},{32,16},{48,32},{64,48},{80,64},{96,80},{112,96},{128,112},... | collective-permute-start | bytes 1544 | tf_op jit(solution)/shard_map/ppermute | solution.py:47
  211.0 17.1 %copy-start.2 = (bf16[3,64,2048]{2,1,0:T(8,128)(2,1)S(1)}, bf16[3,64,2048]{2,1,0:T(8,128)(2,1)}, u32[]{:S(2)}) copy-start(bf16[3,64,2048]{2,1,0:T(8,128)(2,1)} %fusion.4) | copy-start | bytes 2359300
  211.0 17.9 %copy-start.11 = (bf16[256,128]{1,0:T(8,128)(2,1)S(1)}, bf16[256,128]{1,0:T(8,128)(2,1)}, u32[]{:S(2)}) copy-start(bf16[256,128]{1,0:T(8,128)(2,1)} %param.20) | copy-start | bytes 196612
  215.3 14.3 %copy-start.18 = (bf16[256,128]{1,0:T(8,128)(2,1)S(1)}, bf16[256,128]{1,0:T(8,128)(2,1)}, u32[]{:S(2)}) copy-start(bf16[256,128]{1,0:T(8,128)(2,1)} %param.21) | copy-start | bytes 196612
  216.2 30.2 %all-to-all-start.6 = ((bf16[16,64,128]{2,1,0:T(8,128)(2,1)}), bf16[16,64,128]{2,1,0:T(8,128)(2,1)S(1)}, u32[]{:S(2)}, u32[]{:S(2)}) async-start(bf16[16,64,128]{2,1,0:T(8,128)(2,1)} %reduce_sum.57), calls=%async_computation.6 | async-start | bytes 524288 | tf_op jit(solution)/shard_map/all_to_all | solution.py:16
  (7 other events, 6.7 us)

commit v2 on v1

v2 whole, which is shorter than its diff:
```python
import functools

import jax
import jax.numpy as jnp
from jax import lax
from jax.experimental import pallas as pl
from jax.experimental.pallas import tpu as pltpu
from jax.sharding import Mesh
from jax.sharding import PartitionSpec as P


SP = ("z", "c")
TP = ("y", "x")
LIMIT = 7.0
ALPHA = 1.702
LANES = 128
BF = jnp.bfloat16
F32 = jnp.float32


def swap(blocks, axis):
    return lax.all_to_all(blocks, axis, split_axis=0, concat_axis=0, tiled=True)


def turned(value, axis, by):
    count = lax.axis_size(axis)
    return lax.ppermute(value, axis, [(i, (i + by) % count) for i in range(count)])


def mirrored(value, axis, bit):
    return lax.ppermute(value, axis, [(i, i ^ bit) for i in range(lax.axis_size(axis))])


def doubled(value, axis):
    index = lax.axis_index(axis)
    bit = lax.axis_size(axis) // 2
    while bit:
        other = mirrored(value, axis, bit)
        high = (index & bit) > 0
        both = (jnp.where(high, other, value), jnp.where(high, value, other))
        value = jnp.stack(both, axis=value.ndim - 2)
        bit //= 2
    return value


def from_behind(value, axis, by):
    count = lax.axis_size(axis)
    pairs = [(i, i + by) for i in range(count) if 0 <= i + by < count]
    return lax.ppermute(value, axis, pairs)


def dot(a, b, ca, cb):
    return lax.dot_general(a, b, (((ca,), (cb,)), ((), ())), preferred_element_type=F32)


def expert_cots(rows, grads, gate_w, lin_w, down_w):
    gate_pre = dot(rows, gate_w, 1, 1)
    lin_pre = dot(rows, lin_w, 1, 1)
    act_grad = dot(grads, down_w, 1, 1)
    gate_cut = jnp.minimum(gate_pre, LIMIT)
    lin_cut = jnp.clip(lin_pre, -LIMIT, LIMIT)
    sigma = jax.nn.sigmoid(ALPHA * gate_cut)
    act = (gate_cut * sigma * (lin_cut + 1.0)).astype(BF)
    slope = sigma * (1.0 + ALPHA * gate_cut * (1.0 - sigma))
    gate_cot = jnp.where(gate_pre < LIMIT, act_grad * (lin_cut + 1.0) * slope, 0.0).astype(BF)
    lin_cot = jnp.where(jnp.abs(lin_pre) < LIMIT, act_grad * gate_cut * sigma, 0.0).astype(BF)
    return act, gate_cot, lin_cot


def routing_kernel(yi_ref, xi_ref, ids_ref, weights_ref, rows_ref, grads_ref, send_ref, place_ref, *, kx, cap, padded):
    tokens = ids_ref.shape[1]
    experts = send_ref.shape[0] // kx
    ids = ids_ref[...]
    expert = lax.broadcasted_iota(jnp.int32, (experts, tokens), 0)
    first = expert == ids[0:1, :]
    second = expert == ids[1:2, :]
    one = jnp.where(first | second, 1.0, 0.0).astype(BF)
    early = lax.broadcasted_iota(jnp.int32, (tokens, tokens), 0)
    late = lax.broadcasted_iota(jnp.int32, (tokens, tokens), 1)
    before = dot(one, jnp.where(early < late, 1.0, 0.0).astype(BF), 1, 0)
    rank0 = jnp.sum(jnp.where(first, before, 0.0), axis=0, keepdims=True).astype(jnp.int32)
    rank1 = jnp.sum(jnp.where(second, before, 0.0), axis=0, keepdims=True).astype(jnp.int32)
    place_ref[0:1, :] = ids[0:1, :] * padded + rank0
    place_ref[1:2, :] = ids[1:2, :] * padded + rank1
    slots = experts * kx
    slot = lax.broadcasted_iota(jnp.int32, (slots, tokens), 0)
    owner = slot // kx
    slot = owner * cap + xi_ref[0] * kx + (slot - owner * kx)
    hit0 = slot == ids[0:1, :] * cap + rank0
    hit1 = slot == ids[1:2, :] * cap + rank1
    pick = jnp.where(hit0 | hit1, 1.0, 0.0).astype(BF)
    w = weights_ref[...]
    weight = jnp.sum(
        jnp.where(hit0, w[0:1, :], 0.0) + jnp.where(hit1, w[1:2, :], 0.0), axis=1, keepdims=True
    )
    rows = dot(pick, rows_ref[...], 1, 0)
    grads = weight * dot(pick, grads_ref[...], 1, 0)
    both = jnp.concatenate([rows, grads], axis=1)
    send_ref[...] = both.reshape(slots, both.shape[1] // LANES, LANES).astype(BF)


def route(route_ids, route_weights, moe_input, out_grad, yi, xi, n_y, kx, experts, cap, padded):
    tokens, width = moe_input.shape
    wy = width // n_y
    slots = experts * kx
    return pl.pallas_call(
        functools.partial(routing_kernel, kx=kx, cap=cap, padded=padded),
        grid_spec=pltpu.PrefetchScalarGridSpec(
            num_scalar_prefetch=2,
            grid=(1,),
            in_specs=[
                pl.BlockSpec((2, tokens), lambda i, y, x: (0, 0)),
                pl.BlockSpec((2, tokens), lambda i, y, x: (0, 0)),
                pl.BlockSpec((tokens, wy), lambda i, y, x: (0, y[0])),
                pl.BlockSpec((tokens, wy), lambda i, y, x: (0, y[0])),
            ],
            out_specs=[
                pl.BlockSpec((slots, 2 * wy // LANES, LANES), lambda i, y, x: (0, 0, 0)),
                pl.BlockSpec((2, tokens), lambda i, y, x: (0, 0)),
            ],
        ),
        out_shape=[
            jax.ShapeDtypeStruct((slots, 2 * wy // LANES, LANES), BF),
            jax.ShapeDtypeStruct((2, tokens), jnp.int32),
        ],
        name="route",
    )(yi[None], xi[None], route_ids.T, route_weights.T, moe_input, out_grad)


def regroup_kernel(got_ref, out_ref):
    _, both, _ = got_ref.shape
    got = got_ref[...].astype(F32)
    for f in range(both):
        piece = got[:, f, :].astype(BF)
        for y in range(out_ref.shape[0]):
            out_ref[y, f] = piece


def expert_kernel(got_ref, w0_ref, w1_ref, w2_ref, w3_ref, part_ref, cots_ref):
    n_y, both, _, lanes = got_ref.shape
    chunks = both // 2
    rows = jnp.concatenate([got_ref[y, f] for y in range(n_y) for f in range(chunks)], axis=1)
    grads = jnp.concatenate(
        [got_ref[y, chunks + f] for y in range(n_y) for f in range(chunks)], axis=1
    )
    refs = (w0_ref, w1_ref, w2_ref, w3_ref)
    gate_w, lin_w, down_w = (jnp.concatenate([r[k] for r in refs], axis=0) for k in range(3))
    act, gate_cot, lin_cot = expert_cots(rows, grads, gate_w, lin_w, down_w)
    cots_ref[0] = gate_cot
    cots_ref[1] = lin_cot
    cots_ref[2] = act
    part = dot(gate_cot, gate_w, 1, 0) + dot(lin_cot, lin_w, 1, 0)
    for t in range(part_ref.shape[0]):
        part_ref[t] = part[:, t * lanes : (t + 1) * lanes].astype(BF)


def weight_grad_kernel(got_ref, cots_ref, o0_ref, o1_ref, o2_ref, o3_ref):
    n_y, both, _, _ = got_ref.shape
    chunks = both // 2
    outs = (o0_ref, o1_ref, o2_ref, o3_ref)
    hidden = o0_ref.shape[1]
    for k in range(3):
        offset = chunks if k == 2 else 0
        other = jnp.concatenate(
            [got_ref[y, offset + f] for y in range(n_y) for f in range(chunks)], axis=1
        )
        terms = dot(cots_ref[k], other, 0, 0)
        for d, ref in enumerate(outs):
            ref[k] = terms[d * hidden : (d + 1) * hidden].astype(ref.dtype)


def slot_sum_kernel(part_ref, out_ref, *, n_y, n_x, kx, padded):
    _, slots, lanes = part_ref.shape
    rows = out_ref.shape[0]
    cols = n_x * slots
    row = lax.broadcasted_iota(jnp.int32, (rows, cols), 0)
    col = lax.broadcasted_iota(jnp.int32, (rows, cols), 1)
    owner = row // padded
    at = row - owner * padded
    group = at // kx
    wanted = jnp.where(group < n_x, group * slots + owner * kx + (at - group * kx), -1)
    pick = jnp.where(wanted == col, 1.0, 0.0).astype(BF)
    total = jnp.zeros((rows, lanes), F32)
    for y in range(n_y):
        group_rows = jnp.concatenate([part_ref[y * n_x + x] for x in range(n_x)], axis=0)
        total = total + dot(pick, group_rows, 1, 0)
    out_ref[...] = total.astype(BF)


def combine_kernel(place_ref, back_ref, out_ref):
    tokens = place_ref.shape[1]
    every = lax.broadcasted_iota(jnp.int32, (back_ref.shape[0], tokens), 0)
    place = place_ref[...]
    hit = (every == place[0:1, :]) | (every == place[1:2, :])
    row_grads = dot(jnp.where(hit, 1.0, 0.0).astype(BF), back_ref[...], 0, 0).astype(BF)
    for t in range(out_ref.shape[0]):
        out_ref[t] = row_grads


def mixer_kernel(full_ref, out_grad_ref, proj_ref, mixed_ref, convolved_ref, outer_ref, terms_ref, outer_grad_ref, cot_ref):
    n_tp, _, _ = full_ref.shape
    n_c, n_z, per, _ = terms_ref.shape
    full = jnp.concatenate([full_ref[t] for t in range(n_tp)], axis=1)
    stream = (out_grad_ref[...].astype(F32) + full.astype(F32)).astype(BF)
    terms = dot(stream, mixed_ref[...], 0, 0).astype(BF)
    for z in range(n_z):
        for c in range(n_c):
            at = (z * n_c + c) * per
            terms_ref[c, z] = terms[at : at + per]
    mixed_grad = dot(stream, proj_ref[...], 1, 0)
    outer_grad_ref[...] = (mixed_grad * convolved_ref[...]).astype(BF)
    cot_ref[...] = (mixed_grad * outer_ref[...].astype(F32)).astype(BF)


def on_core(kernel, outs, *args, **static):
    return pl.pallas_call(
        functools.partial(kernel, **static) if static else kernel,
        out_shape=[jax.ShapeDtypeStruct(s, t) for s, t in outs],
    )(*args)


def local(
    moe_input,
    out_grad,
    route_ids,
    route_weights,
    gate_weight,
    lin_weight,
    down_weight,
    outer_gate,
    inner_gate,
    conv_input,
    conv_taps,
    out_proj,
):
    n_sp = lax.axis_size(SP)
    n_z, n_c, n_y, n_x = (lax.axis_size(a) for a in ("z", "c", "y", "x"))
    n_tp = n_y * n_x
    tokens, _ = route_ids.shape
    width = moe_input.shape[1]
    wdev = width // n_tp
    wy = width // n_y
    chunks = wy // wdev
    hidden = gate_weight.shape[1]
    experts = n_sp
    cap = 5 * tokens // (2 * experts)
    kx = cap // n_x
    slots = experts * kx
    padded = -(-cap // 8) * 8
    yi = lax.axis_index("y")
    xi = lax.axis_index("x")

    weights = jnp.concatenate([gate_weight, lin_weight, down_weight], axis=0)
    blocks = [weights] + [turned(weights, "x", d) for d in range(1, n_x)]

    send, place = route(
        route_ids, route_weights, moe_input, out_grad, yi, xi, n_y, kx, experts, cap, padded
    )
    got = swap(send.reshape(experts, kx * 2 * chunks, wdev), SP)
    (got,) = on_core(
        regroup_kernel, [((n_y, 2 * chunks, slots, wdev), BF)], got.reshape(slots, 2 * chunks, wdev)
    )
    got = swap(got, "y")

    part, cots = on_core(
        expert_kernel, [((n_tp, slots, wdev), BF), ((3, slots, n_x * hidden), BF)], got, *blocks
    )
    part = swap(part, TP)
    terms = on_core(weight_grad_kernel, [((3, hidden, width), BF)] * n_x, got, cots)
    (slot_sums,) = on_core(
        slot_sum_kernel,
        [((experts * padded, wdev), BF)],
        part,
        n_y=n_y,
        n_x=n_x,
        kx=kx,
        padded=padded,
    )
    back = swap(slot_sums.reshape(experts, padded, wdev), SP)
    back = back.reshape(experts * padded, wdev)

    total = terms[0].astype(F32)
    for d in range(1, n_x):
        total = total + turned(terms[d], "x", -d).astype(F32)
    weight_grads = total.astype(BF)
    gate_grad, lin_grad, down_grad = (weight_grads[k : k + 1] for k in range(3))

    (row_grads,) = on_core(combine_kernel, [((n_tp, tokens, wdev), BF)], place, back)
    full = swap(row_grads, TP)

    taps = conv_taps.shape[0]
    conv_values = (inner_gate.astype(F32) * conv_input.astype(F32)).astype(BF)
    prior_rows = from_behind(conv_values[tokens - (taps - 1) :], SP, 1)
    extended = jnp.concatenate([prior_rows, conv_values], axis=0).astype(F32)
    convolved = jnp.zeros((tokens, wdev), F32)
    for tap in range(taps):
        convolved = convolved + conv_taps[tap][None, :] * extended[tap : tap + tokens]
    mixed = (outer_gate.astype(F32) * convolved).astype(BF)

    proj = doubled(doubled(out_proj.T, "z"), "c").reshape(width, wdev)
    pair, outer_gate_grad, conv_cot = on_core(
        mixer_kernel,
        [((n_c, n_z, width // n_sp, wdev), BF), ((tokens, wdev), BF), ((tokens, wdev), BF)],
        full,
        out_grad,
        proj,
        mixed,
        convolved,
        outer_gate,
    )
    terms = swap(pair, "c")
    terms = jnp.sum(terms.astype(F32), axis=0).astype(BF)
    out_proj_grad = jnp.sum(swap(terms, "z").astype(F32), axis=0)

    later_rows = from_behind(conv_cot[: taps - 1], SP, -1)
    extended_cot = jnp.concatenate([conv_cot, later_rows], axis=0).astype(F32)
    value_grad = jnp.zeros((tokens, wdev), F32)
    for tap in range(taps):
        start = taps - 1 - tap
        value_grad = value_grad + conv_taps[tap][None, :] * extended_cot[start : start + tokens]
    inner_gate_grad = (value_grad * conv_input.astype(F32)).astype(BF)
    conv_input_grad = (value_grad * inner_gate.astype(F32)).astype(BF)
    return (
        gate_grad,
        lin_grad,
        down_grad,
        out_proj_grad,
        outer_gate_grad,
        inner_gate_grad,
        conv_input_grad,
    )


def solution(mesh):
    torus = Mesh(mesh.devices.reshape(-1, 2, 4, 4), ("z", "c", "y", "x"))
    tokens = P(SP, None)
    expert = P(SP, TP, None)
    mixer = P(SP, TP)
    return jax.shard_map(
        local,
        mesh=torus,
        in_specs=(tokens,) * 4 + (expert,) * 3 + (mixer,) * 3 + (P(None, TP), P(TP, SP)),
        out_specs=(expert,) * 3 + (mixer,) * 4,
        check_vma=False,
    )
```

time: 249 us -> 241 us (0.968)
  the two profiles are of different devices: /device:TPU:32 before, /device:TPU:6 now
where the time goes in v2:
time: 241 us; the launch traced here: 239 us
  waiting for transfers between devices  116 us (48%)
  starting transfers between devices  82.4 us (34%)
  Pallas kernels  23 us (10%)
  local copies, waits for them, and re-layouts  6.23 us (3%)
  other arithmetic  5.7 us (2%)
  blocking collectives  5.35 us (2%)
    all_to_all x6, waiting for transfers between devices, swap(): return lax.all_to_all(blocks, axis, split_axis=0, concat_axis=0, tiled=True)  49.8 us
    all_to_all x6, starting transfers between devices, swap(): return lax.all_to_all(blocks, axis, split_axis=0, concat_axis=0, tiled=True)  49.6 us
    ppermute x6, waiting for transfers between devices, turned(): lax.ppermute(value, axis, [(i, (i + by) % count) for i in range(count)])  38.9 us
    ppermute x5, waiting for transfers between devices, mirrored(): lax.ppermute(value, axis, [(i, i ^ bit) for i in range(lax.axis_size(axis...  26.2 us
    pallas_call x6, Pallas kernels, on_core(): pl.pallas_call(functools.partial(kernel, **static) if static else kernel,...  20.7 us
    ppermute x6, starting transfers between devices, turned(): lax.ppermute(value, axis, [(i, (i + by) % count) for i in range(count)])  18.5 us
    ppermute x5, starting transfers between devices, mirrored(): lax.ppermute(value, axis, [(i, i ^ bit) for i in range(lax.axis_size(axis...  11.7 us
    all_to_all x1, blocking collectives, swap(): return lax.all_to_all(blocks, axis, split_axis=0, concat_axis=0, tiled=True)  5.35 us
  transfers between devices with their start and end apart: 19, of which 12 were waited for; matrix products, arithmetic and copies ran while one was open for 3% of the time, Pallas kernels for 6%

profile of v2, /device:TPU:6, one launch (start us, length us, event | category | flops | bytes accessed | tf_op | source)
XLA Modules:
  0.0 239.4 jit_solution(3818967636281659664)
XLA Ops:
  0.7 2.3 route.1
  3.0 15.5 %all-to-all-start = ((bf16[32,40,128]{2,1,0:T(8,128)(2,1)}), bf16[32,40,128]{2,1,0:T(8,128)(2,1)S(1)}, u32[]{:S(2)}, u32[]{:S(2)}) async-start(bf16[32,40,128]{2,1,0:T(8,128)(2,1)} %bitcast.42), calls=%async_computation | async-start | bytes 655360 | tf_op jit(solution)/shard_map/all_to_all | solution.py:22
  18.5 25.4 %all-to-all-done = bf16[32,40,128]{2,1,0:T(8,128)(2,1)S(1)} async-done(((bf16[32,40,128]{2,1,0:T(8,128)(2,1)}), bf16[32,40,128]{2,1,0:T(8,128)(2,1)S(1)}, u32[]{:S(2)}, u32[]{:S(2)}) %all-to-all-start) | async-done | bytes 327712 | tf_op jit(solution)/shard_map/all_to_all | solution.py:22
  43.9 0.8 copy-done.4
  44.7 2.5 %shard_map.171 = bf16[4,8,160,128]{3,2,1,0:T(8,128)(2,1)} custom-call(bf16[160,8,128]{2,1,0:T(8,128)(2,1)} %bitcast.39), custom_call_target="tpu_custom_call" | custom-call | tf_op jit(solution)/shard_map/pallas_call | solution.py:216
  47.1 4.6 %all-to-all-start.1 = ((bf16[4,8,160,128]{3,2,1,0:T(8,128)(2,1)}), bf16[4,8,160,128]{3,2,1,0:T(8,128)(2,1)S(1)}, u32[]{:S(2)}, u32[]{:S(2)}) async-start(bf16[4,8,160,128]{3,2,1,0:T(8,128)(2,1)} %shard_map.171), calls=%async_computation.1 | async-start | bytes 2621440 | tf_op jit(solution)/shard_map/all_to_all | solution.py:22
  51.7 2.4 collective-permute-start
  54.1 4.3 %collective-permute-start.1 = (bf16[3,64,2048]{2,1,0:T(8,128)(2,1)S(1)}, bf16[3,64,2048]{2,1,0:T(8,128)(2,1)}, u32[]{:S(2)}, u32[]{:S(2)}) collective-permute-start(bf16[3,64,2048]{2,1,0:T(8,128)(2,1)S(1)} %constant_dynamic-update-slice_fusion.w0_ref), channel_id=1, source_target_pairs={{0,2},{1,3},{2,0},{3,1},{4,6},{5,7},{6,4},{7,5},{8,10},{9,11},{10,... | collective-permute-start | bytes 2359304 | tf_op jit(solution)/shard_map/ppermute | solution.py:27
  58.5 1.9 collective-permute-start.2
  60.4 2.1 collective-permute-start.6
  62.5 12.5 %collective-permute-done.6 = bf16[64,128]{1,0:T(8,128)(2,1)S(1)} collective-permute-done((bf16[64,128]{1,0:T(8,128)(2,1)S(1)}, bf16[64,128]{1,0:T(8,128)(2,1)S(1)}, u32[]{:S(2)}, u32[]{:S(2)}) %collective-permute-start.6) | collective-permute-done | bytes 16416 | tf_op jit(solution)/shard_map/ppermute | solution.py:31
  75.1 1.9 collective-permute-start.7
  77.0 1.1 collective-permute-done.1.w2_ref
  78.1 15.1 %collective-permute-done.2.w3_ref = bf16[3,64,2048]{2,1,0:T(8,128)(2,1)} collective-permute-done((bf16[3,64,2048]{2,1,0:T(8,128)(2,1)S(1)}, bf16[3,64,2048]{2,1,0:T(8,128)(2,1)}, u32[]{:S(2)}, u32[]{:S(2)}) %collective-permute-start.2) | collective-permute-done | bytes 786464 | tf_op jit(solution)/shard_map/ppermute | solution.py:27
  93.2 1.1 copy-done
  94.3 5.3 %shard_map.172 = (bf16[16,160,128]{2,1,0:T(8,128)(2,1)}, bf16[3,160,256]{2,1,0:T(8,128)(2,1)}) custom-call(bf16[4,8,160,128]{3,2,1,0:T(8,128)(2,1)} %copy-done, bf16[3,64,2048]{2,1,0:T(8,128)(2,1)} %copy-done.3, bf16[3,64,2048]{2,1,0:T(8,128)(2,1)} %copy-done.7, bf16[3,64,2048]{2,1,0:T(8,128)(2,1)} %collective-permute-done.1.w2_ref, ...), custom_call_target="tpu_custom_call" | custom-call | tf_op jit(solution)/shard_map/pallas_call | solution.py:216
  99.7 7.7 %all-to-all-start.2 = ((bf16[16,160,128]{2,1,0:T(8,128)(2,1)}), bf16[16,160,128]{2,1,0:T(8,128)(2,1)S(1)}, u32[]{:S(2)}, u32[]{:S(2)}) async-start(bf16[16,160,128]{2,1,0:T(8,128)(2,1)} %get-tuple-element.25), calls=%async_computation.2 | async-start | bytes 1310720 | tf_op jit(solution)/shard_map/all_to_all | solution.py:22
  107.4 2.2 collective-permute-start.8
  109.7 1.3 collective-permute-start.11
  111.0 3.5 %collective-permute-done.8 = bf16[2,2,64,128]{3,2,0,1:T(8,128)(2,1)S(1)} collective-permute-done((bf16[2,2,64,128]{3,2,0,1:T(8,128)(2,1)S(1)}, bf16[2,2,64,128]{3,2,0,1:T(8,128)(2,1)S(1)}, u32[]{:S(2)}, u32[]{:S(2)}) %collective-permute-start.8) | collective-permute-done | bytes 65568 | tf_op jit(solution)/shard_map/ppermute | solution.py:31
  114.5 3.0 %all-to-all-done.2.part_ref = bf16[16,160,128]{2,1,0:T(8,128)(2,1)S(1)} async-done(((bf16[16,160,128]{2,1,0:T(8,128)(2,1)}), bf16[16,160,128]{2,1,0:T(8,128)(2,1)S(1)}, u32[]{:S(2)}, u32[]{:S(2)}) %all-to-all-start.2) | async-done | bytes 655392 | tf_op jit(solution)/shard_map/all_to_all | solution.py:22
  117.5 0.8 copy-done.2
  118.3 3.3 %shard_map.174 = bf16[768,128]{1,0:T(8,128)(2,1)} custom-call(bf16[16,160,128]{2,1,0:T(8,128)(2,1)} %copy-done.2), custom_call_target="tpu_custom_call" | custom-call | tf_op jit(solution)/shard_map/pallas_call | solution.py:216
  121.7 3.9 %all-to-all-start.3 = ((bf16[32,24,128]{2,1,0:T(8,128)(2,1)}), bf16[32,24,128]{2,1,0:T(8,128)(2,1)S(1)}, u32[]{:S(2)}, u32[]{:S(2)}) async-start(bf16[32,24,128]{2,1,0:T(8,128)(2,1)} %bitcast.41), calls=%async_computation.3 | async-start | bytes 393216 | tf_op jit(solution)/shard_map/all_to_all | solution.py:22
  125.6 3.6 %collective-permute-start.9 = (bf16[2,2,2,64,128]{4,3,0,1,2:T(8,128)(2,1)S(1)}, bf16[2,2,2,64,128]{4,3,0,1,2:T(8,128)(2,1)S(1)}, u32[]{:S(2)}, u32[]{:S(2)}) collective-permute-start(bf16[2,2,2,64,128]{4,3,0,1,2:T(8,128)(2,1)S(1)} %pad_maximum_fusion.2), channel_id=1, source_target_pairs={{0,32},{32,0},{64,96},{96,64},{128,160},{160,128},{192,224},{224,1... | collective-permute-start | bytes 393224 | tf_op jit(solution)/shard_map/ppermute | solution.py:31
  129.2 10.2 %collective-permute-done.9 = bf16[2,2,2,64,128]{4,3,0,1,2:T(8,128)(2,1)S(1)} collective-permute-done((bf16[2,2,2,64,128]{4,3,0,1,2:T(8,128)(2,1)S(1)}, bf16[2,2,2,64,128]{4,3,0,1,2:T(8,128)(2,1)S(1)}, u32[]{:S(2)}, u32[]{:S(2)}) %collective-permute-start.9) | collective-permute-done | bytes 131104 | tf_op jit(solution)/shard_map/ppermute | solution.py:31
  139.4 4.0 %shard_map.173 = (bf16[3,64,2048]{2,1,0:T(8,128)(2,1)}, bf16[3,64,2048]{2,1,0:T(8,128)(2,1)}, bf16[3,64,2048]{2,1,0:T(8,128)(2,1)}, bf16[3,64,2048]{2,1,0:T(8,128)(2,1)}) custom-call(bf16[4,8,160,128]{3,2,1,0:T(8,128)(2,1)} %copy-done, bf16[3,160,256]{2,1,0:T(8,128)(2,1)} %get-tuple-element.19.cots_ref), custom_call_target="tpu_custom_call" | custom-call | tf_op jit(solution)/shard_map/pallas_call | solution.py:216
  143.4 4.6 %collective-permute-start.5 = (bf16[3,64,2048]{2,1,0:T(8,128)(2,1)}, bf16[3,64,2048]{2,1,0:T(8,128)(2,1)S(1)}, u32[]{:S(2)}, u32[]{:S(2)}) collective-permute-start(bf16[3,64,2048]{2,1,0:T(8,128)(2,1)} %get-tuple-element.23), channel_id=1, source_target_pairs={{0,1},{1,2},{2,3},{3,0},{4,5},{5,6},{6,7},{7,4},{8,9},{9,10},{10,1... | collective-permute-start | bytes 2359304 | tf_op jit(solution)/shard_map/ppermute | solution.py:27
  148.0 2.1 collective-permute-start.4
  150.2 3.1 %collective-permute-start.3 = (bf16[3,64,2048]{2,1,0:T(8,128)(2,1)}, bf16[3,64,2048]{2,1,0:T(8,128)(2,1)}, u32[]{:S(2)}, u32[]{:S(2)}) collective-permute-start(bf16[3,64,2048]{2,1,0:T(8,128)(2,1)} %get-tuple-element.21), channel_id=1, source_target_pairs={{0,3},{1,0},{2,1},{3,2},{4,7},{5,4},{6,5},{7,6},{8,11},{9,8},{10,9... | collective-permute-start | bytes 2359304 | tf_op jit(solution)/shard_map/ppermute | solution.py:27
  153.3 1.9 collective-permute-start.10
  156.0 2.3 shard_map.175
  158.3 6.5 %all-to-all-start.4 = ((bf16[16,256,128]{2,1,0:T(8,128)(2,1)}), bf16[16,256,128]{2,1,0:T(8,128)(2,1)S(1)}, u32[]{:S(2)}, u32[]{:S(2)}) async-start(bf16[16,256,128]{2,1,0:T(8,128)(2,1)} %shard_map.175), calls=%async_computation.4 | async-start | bytes 2097152 | tf_op jit(solution)/shard_map/all_to_all | solution.py:22
  164.7 0.7 multiply_convert_fusion
  165.6 0.8 copy.20
  166.4 20.3 %collective-permute-done.5 = bf16[3,64,2048]{2,1,0:T(8,128)(2,1)S(1)} collective-permute-done((bf16[3,64,2048]{2,1,0:T(8,128)(2,1)}, bf16[3,64,2048]{2,1,0:T(8,128)(2,1)S(1)}, u32[]{:S(2)}, u32[]{:S(2)}) %collective-permute-start.5) | collective-permute-done | bytes 786464 | tf_op jit(solution)/shard_map/ppermute | solution.py:27
  186.8 2.3 collective-permute-done.3
  189.1 1.9 add_convert_fusion
  191.0 7.3 %all-to-all-done.4.full_ref = bf16[16,256,128]{2,1,0:T(8,128)(2,1)S(1)} async-done(((bf16[16,256,128]{2,1,0:T(8,128)(2,1)}), bf16[16,256,128]{2,1,0:T(8,128)(2,1)S(1)}, u32[]{:S(2)}, u32[]{:S(2)}) %all-to-all-start.4) | async-done | bytes 1048608 | tf_op jit(solution)/shard_map/all_to_all | solution.py:22
  198.4 1.0 copy-done.1
  199.4 3.3 %shard_map.176 = (bf16[2,16,64,128]{3,2,1,0:T(8,128)(2,1)}, bf16[256,128]{1,0:T(8,128)(2,1)}, bf16[256,128]{1,0:T(8,128)(2,1)}) custom-call(bf16[16,256,128]{2,1,0:T(8,128)(2,1)} %copy-done.1, bf16[256,2048]{1,0:T(8,128)(2,1)} %out_grad_ref.1, bf16[2048,128]{1,0:T(8,128)(2,1)} %bitcast.38, bf16[256,128]{1,0:T(8,128)(2,1)} %get-tuple-element.31.mixed_ref, ...), custom_call_target="tpu_custom_call" | custom-call | tf_op jit(solution)/shard_map/pallas_call | solution.py:216
  202.6 5.3 %all_to_all.35 = bf16[2,16,64,128]{3,2,1,0:T(8,128)(2,1)S(1)} all-to-all(bf16[2,16,64,128]{3,2,1,0:T(8,128)(2,1)} %get-tuple-element.26), channel_id=1, replica_groups=mesh['z'=16,'c'=2,'y'=4,'x'=4] {'c'}, dimensions={0} | all-to-all | bytes 1048576 | tf_op jit(solution)/shard_map/all_to_all | solution.py:22
  208.0 0.8 reduce_sum.21
  208.8 11.5 %all-to-all-start.6 = ((bf16[16,64,128]{2,1,0:T(8,128)(2,1)}), bf16[16,64,128]{2,1,0:T(8,128)(2,1)S(1)}, u32[]{:S(2)}, u32[]{:S(2)}) async-start(bf16[16,64,128]{2,1,0:T(8,128)(2,1)} %reduce_sum.21), calls=%async_computation.6 | async-start | bytes 524288 | tf_op jit(solution)/shard_map/all_to_all | solution.py:22
  220.3 1.3 collective-permute-start.12
  221.6 0.9 fusion.9
  222.5 0.9 collective-permute-done.12
  224.7 14.1 %all-to-all-done.6 = bf16[16,64,128]{2,1,0:T(8,128)(2,1)S(1)} async-done(((bf16[16,64,128]{2,1,0:T(8,128)(2,1)}), bf16[16,64,128]{2,1,0:T(8,128)(2,1)S(1)}, u32[]{:S(2)}, u32[]{:S(2)}) %all-to-all-start.6) | async-done | bytes 262176 | tf_op jit(solution)/shard_map/all_to_all | solution.py:22
  (59 shorter events, 3.1 us)
Async XLA Ops:
  0.6 17.8 %copy-start.10 = (bf16[1,64,2048]{2,1,0:T(8,128)(2,1)S(1)}, bf16[1,64,2048]{2,1,0:T(8,128)(2,1)}, u32[]{:S(2)}) copy-start(bf16[1,64,2048]{2,1,0:T(8,128)(2,1)} %param.16) | copy-start | bytes 786436
  0.6 17.8 %copy-start.11 = (bf16[1,64,2048]{2,1,0:T(8,128)(2,1)S(1)}, bf16[1,64,2048]{2,1,0:T(8,128)(2,1)}, u32[]{:S(2)}) copy-start(bf16[1,64,2048]{2,1,0:T(8,128)(2,1)} %param.17) | copy-start | bytes 786436
  3.0 41.0 %all-to-all-start = ((bf16[32,40,128]{2,1,0:T(8,128)(2,1)}), bf16[32,40,128]{2,1,0:T(8,128)(2,1)S(1)}, u32[]{:S(2)}, u32[]{:S(2)}) async-start(bf16[32,40,128]{2,1,0:T(8,128)(2,1)} %bitcast.42), calls=%async_computation | async-start | bytes 655360 | tf_op jit(solution)/shard_map/all_to_all | solution.py:22
  43.9 0.8 copy-start.4
  47.1 4.6 %copy-start.12 = (bf16[1,64,2048]{2,1,0:T(8,128)(2,1)S(1)}, bf16[1,64,2048]{2,1,0:T(8,128)(2,1)}, u32[]{:S(2)}) copy-start(bf16[1,64,2048]{2,1,0:T(8,128)(2,1)} %param.18) | copy-start | bytes 786436
  47.1 13.3 %copy-start.15 = (bf16[128,64]{0,1:T(8,128)(2,1)S(1)}, bf16[128,64]{0,1:T(8,128)(2,1)}, u32[]{:S(2)}) copy-start(bf16[128,64]{0,1:T(8,128)(2,1)} %param.23) | copy-start | bytes 49156
  47.1 46.1 %all-to-all-start.1 = ((bf16[4,8,160,128]{3,2,1,0:T(8,128)(2,1)}), bf16[4,8,160,128]{3,2,1,0:T(8,128)(2,1)S(1)}, u32[]{:S(2)}, u32[]{:S(2)}) async-start(bf16[4,8,160,128]{3,2,1,0:T(8,128)(2,1)} %shard_map.171), calls=%async_computation.1 | async-start | bytes 2621440 | tf_op jit(solution)/shard_map/all_to_all | solution.py:22
  51.7 41.5 %copy-start.3 = (bf16[3,64,2048]{2,1,0:T(8,128)(2,1)}, bf16[3,64,2048]{2,1,0:T(8,128)(2,1)S(1)}, u32[]{:S(2)}) copy-start(bf16[3,64,2048]{2,1,0:T(8,128)(2,1)S(1)} %constant_dynamic-update-slice_fusion.w0_ref) | copy-start | bytes 2359300
  51.7 25.2 %collective-permute-start = (bf16[3,64,2048]{2,1,0:T(8,128)(2,1)S(1)}, bf16[3,64,2048]{2,1,0:T(8,128)(2,1)S(1)}, u32[]{:S(2)}, u32[]{:S(2)}) collective-permute-start(bf16[3,64,2048]{2,1,0:T(8,128)(2,1)S(1)} %constant_dynamic-update-slice_fusion.w0_ref), channel_id=1, source_target_pairs={{0,1},{1,2},{2,3},{3,0},{4,5},{5,6},{6,7},{7,4},{8,9},{9,10},{10,1... | collective-permute-start | bytes 2359304 | tf_op jit(solution)/shard_map/ppermute | solution.py:27
  54.1 24.0 %collective-permute-start.1 = (bf16[3,64,2048]{2,1,0:T(8,128)(2,1)S(1)}, bf16[3,64,2048]{2,1,0:T(8,128)(2,1)}, u32[]{:S(2)}, u32[]{:S(2)}) collective-permute-start(bf16[3,64,2048]{2,1,0:T(8,128)(2,1)S(1)} %constant_dynamic-update-slice_fusion.w0_ref), channel_id=1, source_target_pairs={{0,2},{1,3},{2,0},{3,1},{4,6},{5,7},{6,4},{7,5},{8,10},{9,11},{10,... | collective-permute-start | bytes 2359304 | tf_op jit(solution)/shard_map/ppermute | solution.py:27
  58.5 34.7 %collective-permute-start.2 = (bf16[3,64,2048]{2,1,0:T(8,128)(2,1)S(1)}, bf16[3,64,2048]{2,1,0:T(8,128)(2,1)}, u32[]{:S(2)}, u32[]{:S(2)}) collective-permute-start(bf16[3,64,2048]{2,1,0:T(8,128)(2,1)S(1)} %constant_dynamic-update-slice_fusion.w0_ref), channel_id=1, source_target_pairs={{0,3},{1,0},{2,1},{3,2},{4,7},{5,4},{6,5},{7,6},{8,11},{9,8},{10,9... | collective-permute-start | bytes 2359304 | tf_op jit(solution)/shard_map/ppermute | solution.py:27
  60.4 14.6 %collective-permute-start.6 = (bf16[64,128]{1,0:T(8,128)(2,1)S(1)}, bf16[64,128]{1,0:T(8,128)(2,1)S(1)}, u32[]{:S(2)}, u32[]{:S(2)}) collective-permute-start(bf16[64,128]{1,0:T(8,128)(2,1)S(1)} %bitcast.43), channel_id=1, source_target_pairs={{0,256},{32,288},{64,320},{96,352},{128,384},{160,416},{192,448},{... | collective-permute-start | bytes 49160 | tf_op jit(solution)/shard_map/ppermute | solution.py:31
  75.1 32.3 %collective-permute-start.7 = (bf16[2,64,128]{2,1,0:T(8,128)(2,1)S(1)}, bf16[2,64,128]{2,1,0:T(8,128)(2,1)S(1)}, u32[]{:S(2)}, u32[]{:S(2)}) collective-permute-start(bf16[2,64,128]{2,1,0:T(8,128)(2,1)S(1)} %pad_maximum_fusion.4), channel_id=1, source_target_pairs={{0,128},{32,160},{64,192},{96,224},{128,0},{160,32},{192,64},{224,... | collective-permute-start | bytes 98312 | tf_op jit(solution)/shard_map/ppermute | solution.py:31
  77.0 16.2 %copy-start.7 = (bf16[3,64,2048]{2,1,0:T(8,128)(2,1)}, bf16[3,64,2048]{2,1,0:T(8,128)(2,1)S(1)}, u32[]{:S(2)}) copy-start(bf16[3,64,2048]{2,1,0:T(8,128)(2,1)S(1)} %collective-permute-done.w1_ref) | copy-start | bytes 2359300
  93.2 1.1 copy-start
  99.6 10.0 %copy-start.9 = (bf16[256,128]{1,0:T(8,128)(2,1)S(1)}, bf16[256,128]{1,0:T(8,128)(2,1)}, u32[]{:S(2)}) copy-start(bf16[256,128]{1,0:T(8,128)(2,1)} %param.20) | copy-start | bytes 196612
  99.7 10.0 %copy-start.13 = (bf16[256,128]{1,0:T(8,128)(2,1)S(1)}, bf16[256,128]{1,0:T(8,128)(2,1)}, u32[]{:S(2)}) copy-start(bf16[256,128]{1,0:T(8,128)(2,1)} %param.21) | copy-start | bytes 196612
  99.7 17.8 %all-to-all-start.2 = ((bf16[16,160,128]{2,1,0:T(8,128)(2,1)}), bf16[16,160,128]{2,1,0:T(8,128)(2,1)S(1)}, u32[]{:S(2)}, u32[]{:S(2)}) async-start(bf16[16,160,128]{2,1,0:T(8,128)(2,1)} %get-tuple-element.25), calls=%async_computation.2 | async-start | bytes 1310720 | tf_op jit(solution)/shard_map/all_to_all | solution.py:22
  107.4 21.8 %copy-start.16 = (f32[3,128]{1,0:T(4,128)S(1)}, f32[3,128]{1,0:T(4,128)}, u32[]{:S(2)}) copy-start(f32[3,128]{1,0:T(4,128)} %param.22) | copy-start | bytes 4612
  107.4 7.1 %collective-permute-start.8 = (bf16[2,2,64,128]{3,2,0,1:T(8,128)(2,1)S(1)}, bf16[2,2,64,128]{3,2,0,1:T(8,128)(2,1)S(1)}, u32[]{:S(2)}, u32[]{:S(2)}) collective-permute-start(bf16[2,2,64,128]{3,2,0,1:T(8,128)(2,1)S(1)} %pad_maximum_fusion.3), channel_id=1, source_target_pairs={{0,64},{32,96},{64,0},{96,32},{128,192},{160,224},{192,128},{224,1... | collective-permute-start | bytes 196616 | tf_op jit(solution)/shard_map/ppermute | solution.py:31
  109.7 45.5 %collective-permute-start.11 = (bf16[2,128]{1,0:T(2,128)(2,1)S(1)}, bf16[2,128]{1,0:T(2,128)(2,1)S(1)}, u32[]{:S(2)}, u32[]{:S(2)}) collective-permute-start(bf16[2,128]{1,0:T(2,128)(2,1)S(1)} %slice.62), channel_id=1, source_target_pairs={{0,16},{16,32},{32,48},{48,64},{64,80},{80,96},{96,112},{112,128},... | collective-permute-start | bytes 1544 | tf_op jit(solution)/shard_map/ppermute | solution.py:49
  117.5 0.8 copy-start.2
  121.7 33.6 %all-to-all-start.3 = ((bf16[32,24,128]{2,1,0:T(8,128)(2,1)}), bf16[32,24,128]{2,1,0:T(8,128)(2,1)S(1)}, u32[]{:S(2)}, u32[]{:S(2)}) async-start(bf16[32,24,128]{2,1,0:T(8,128)(2,1)} %bitcast.41), calls=%async_computation.3 | async-start | bytes 393216 | tf_op jit(solution)/shard_map/all_to_all | solution.py:22
  125.6 13.8 %collective-permute-start.9 = (bf16[2,2,2,64,128]{4,3,0,1,2:T(8,128)(2,1)S(1)}, bf16[2,2,2,64,128]{4,3,0,1,2:T(8,128)(2,1)S(1)}, u32[]{:S(2)}, u32[]{:S(2)}) collective-permute-start(bf16[2,2,2,64,128]{4,3,0,1,2:T(8,128)(2,1)S(1)} %pad_maximum_fusion.2), channel_id=1, source_target_pairs={{0,32},{32,0},{64,96},{96,64},{128,160},{160,128},{192,224},{224,1... | collective-permute-start | bytes 393224 | tf_op jit(solution)/shard_map/ppermute | solution.py:31
  143.4 43.4 %collective-permute-start.5 = (bf16[3,64,2048]{2,1,0:T(8,128)(2,1)}, bf16[3,64,2048]{2,1,0:T(8,128)(2,1)S(1)}, u32[]{:S(2)}, u32[]{:S(2)}) collective-permute-start(bf16[3,64,2048]{2,1,0:T(8,128)(2,1)} %get-tuple-element.23), channel_id=1, source_target_pairs={{0,1},{1,2},{2,3},{3,0},{4,5},{5,6},{6,7},{7,4},{8,9},{9,10},{10,1... | collective-permute-start | bytes 2359304 | tf_op jit(solution)/shard_map/ppermute | solution.py:27
  148.0 38.7 %collective-permute-start.4 = (bf16[3,64,2048]{2,1,0:T(8,128)(2,1)}, bf16[3,64,2048]{2,1,0:T(8,128)(2,1)}, u32[]{:S(2)}, u32[]{:S(2)}) collective-permute-start(bf16[3,64,2048]{2,1,0:T(8,128)(2,1)} %get-tuple-element.22), channel_id=1, source_target_pairs={{0,2},{1,3},{2,0},{3,1},{4,6},{5,7},{6,4},{7,5},{8,10},{9,11},{10,... | collective-permute-start | bytes 2359304 | tf_op jit(solution)/shard_map/ppermute | solution.py:27
  150.2 39.0 %collective-permute-start.3 = (bf16[3,64,2048]{2,1,0:T(8,128)(2,1)}, bf16[3,64,2048]{2,1,0:T(8,128)(2,1)}, u32[]{:S(2)}, u32[]{:S(2)}) collective-permute-start(bf16[3,64,2048]{2,1,0:T(8,128)(2,1)} %get-tuple-element.21), channel_id=1, source_target_pairs={{0,3},{1,0},{2,1},{3,2},{4,7},{5,4},{6,5},{7,6},{8,11},{9,8},{10,9... | collective-permute-start | bytes 2359304 | tf_op jit(solution)/shard_map/ppermute | solution.py:27
  153.3 12.1 %collective-permute-start.10 = (bf16[2,2,2,2,64,128]{5,4,0,1,2,3:T(8,128)(2,1)S(1)}, bf16[2,2,2,2,64,128]{5,4,0,1,2,3:T(8,128)(2,1)S(1)}, u32[]{:S(2)}, u32[]{:S(2)}) collective-permute-start(bf16[2,2,2,2,64,128]{5,4,0,1,2,3:T(8,128)(2,1)S(1)} %pad_maximum_fusion.1), channel_id=1, source_target_pairs={{0,16},{16,0},{1,17},{17,1},{2,18},{18,2},{3,19},{19,3},{4,20},{20... | collective-permute-start | bytes 786440 | tf_op jit(solution)/shard_map/ppermute | solution.py:31
  155.3 0.7 copy-start.5
  158.3 6.5 %copy-start.8 = (bf16[256,128]{1,0:T(8,128)(2,1)S(1)}, bf16[256,128]{1,0:T(8,128)(2,1)}, u32[]{:S(2)}) copy-start(bf16[256,128]{1,0:T(8,128)(2,1)} %outer_ref.1) | copy-start | bytes 196612
  158.3 40.1 %all-to-all-start.4 = ((bf16[16,256,128]{2,1,0:T(8,128)(2,1)}), bf16[16,256,128]{2,1,0:T(8,128)(2,1)S(1)}, u32[]{:S(2)}, u32[]{:S(2)}) async-start(bf16[16,256,128]{2,1,0:T(8,128)(2,1)} %shard_map.175), calls=%async_computation.4 | async-start | bytes 2097152 | tf_op jit(solution)/shard_map/all_to_all | solution.py:22
  165.5 23.6 %copy-start.6 = (bf16[3,64,2048]{2,1,0:T(8,128)(2,1)S(1)}, bf16[3,64,2048]{2,1,0:T(8,128)(2,1)}, u32[]{:S(2)}) copy-start(bf16[3,64,2048]{2,1,0:T(8,128)(2,1)} %get-tuple-element.20) | copy-start | bytes 2359300
  198.4 1.0 copy-start.1
  202.6 17.7 %copy-start.14 = (bf16[256,128]{1,0:T(8,128)(2,1)S(1)}, bf16[256,128]{1,0:T(8,128)(2,1)}, u32[]{:S(2)}) copy-start(bf16[256,128]{1,0:T(8,128)(2,1)} %get-tuple-element.28) | copy-start | bytes 196612
  208.8 30.0 %all-to-all-start.6 = ((bf16[16,64,128]{2,1,0:T(8,128)(2,1)}), bf16[16,64,128]{2,1,0:T(8,128)(2,1)S(1)}, u32[]{:S(2)}, u32[]{:S(2)}) async-start(bf16[16,64,128]{2,1,0:T(8,128)(2,1)} %reduce_sum.21), calls=%async_computation.6 | async-start | bytes 524288 | tf_op jit(solution)/shard_map/all_to_all | solution.py:22
  220.3 3.1 %collective-permute-start.12 = (bf16[2,128]{1,0:T(2,128)(2,1)S(1)}, bf16[2,128]{1,0:T(2,128)(2,1)S(1)}, u32[]{:S(2)}, u32[]{:S(2)}) collective-permute-start(bf16[2,128]{1,0:T(2,128)(2,1)S(1)} %slice.55), channel_id=1, source_target_pairs={{16,0},{32,16},{48,32},{64,48},{80,64},{96,80},{112,96},{128,112},... | collective-permute-start | bytes 1544 | tf_op jit(solution)/shard_map/ppermute | solution.py:49

commit v3 on v2

--- a/solution.py
+++ b/solution.py
@@ -83,7 +83,7 @@
     place_ref[0:1, :] = ids[0:1, :] * padded + rank0
     place_ref[1:2, :] = ids[1:2, :] * padded + rank1
     slots = experts * kx
-    slot = lax.broadcasted_iota(jnp.int32, (slots, tokens), 0)
+    slot = lax.broadcasted_iota(jnp.int32, (slots, 1), 0)
     owner = slot // kx
     slot = owner * cap + xi_ref[0] * kx + (slot - owner * kx)
     hit0 = slot == ids[0:1, :] * cap + rank0
@@ -170,29 +170,31 @@
 
 
 def slot_sum_kernel(part_ref, out_ref, *, n_y, n_x, kx, padded):
-    _, slots, lanes = part_ref.shape
+    _, slots, _ = part_ref.shape
     rows = out_ref.shape[0]
     cols = n_x * slots
-    row = lax.broadcasted_iota(jnp.int32, (rows, cols), 0)
-    col = lax.broadcasted_iota(jnp.int32, (rows, cols), 1)
+    row = lax.broadcasted_iota(jnp.int32, (rows, 1), 0)
     owner = row // padded
     at = row - owner * padded
     group = at // kx
     wanted = jnp.where(group < n_x, group * slots + owner * kx + (at - group * kx), -1)
+    col = lax.broadcasted_iota(jnp.int32, (rows, cols), 1)
     pick = jnp.where(wanted == col, 1.0, 0.0).astype(BF)
-    total = jnp.zeros((rows, lanes), F32)
-    for y in range(n_y):
-        group_rows = jnp.concatenate([part_ref[y * n_x + x] for x in range(n_x)], axis=0)
-        total = total + dot(pick, group_rows, 1, 0)
-    out_ref[...] = total.astype(BF)
+    sums = []
+    for x in range(n_x):
+        total = part_ref[x].astype(F32)
+        for y in range(1, n_y):
+            total = total + part_ref[y * n_x + x].astype(F32)
+        sums.append(total.astype(BF))
+    out_ref[...] = dot(pick, jnp.concatenate(sums, axis=0), 1, 0).astype(BF)
 
 
 def combine_kernel(place_ref, back_ref, out_ref):
-    tokens = place_ref.shape[1]
-    every = lax.broadcasted_iota(jnp.int32, (back_ref.shape[0], tokens), 0)
+    tokens = place_ref.shape[0]
+    every = lax.broadcasted_iota(jnp.int32, (tokens, back_ref.shape[0]), 1)
     place = place_ref[...]
-    hit = (every == place[0:1, :]) | (every == place[1:2, :])
-    row_grads = dot(jnp.where(hit, 1.0, 0.0).astype(BF), back_ref[...], 0, 0).astype(BF)
+    hit = (every == place[:, 0:1]) | (every == place[:, 1:2])
+    row_grads = dot(jnp.where(hit, 1.0, 0.0).astype(BF), back_ref[...], 1, 0).astype(BF)
     for t in range(out_ref.shape[0]):
         out_ref[t] = row_grads
 
@@ -212,10 +214,11 @@
     cot_ref[...] = (mixed_grad * outer_ref[...].astype(F32)).astype(BF)
 
 
-def on_core(kernel, outs, *args, **static):
+def on_core(kernel, outs, *args, mib=12, **static):
     return pl.pallas_call(
         functools.partial(kernel, **static) if static else kernel,
         out_shape=[jax.ShapeDtypeStruct(s, t) for s, t in outs],
+        compiler_params=pltpu.CompilerParams(vmem_limit_bytes=mib << 20),
     )(*args)
 
 
@@ -263,10 +266,14 @@
     got = swap(got, "y")
 
     part, cots = on_core(
-        expert_kernel, [((n_tp, slots, wdev), BF), ((3, slots, n_x * hidden), BF)], got, *blocks
+        expert_kernel,
+        [((n_tp, slots, wdev), BF), ((3, slots, n_x * hidden), BF)],
+        got,
+        *blocks,
+        mib=24,
     )
     part = swap(part, TP)
-    terms = on_core(weight_grad_kernel, [((3, hidden, width), BF)] * n_x, got, cots)
+    terms = on_core(weight_grad_kernel, [((3, hidden, width), BF)] * n_x, got, cots, mib=24)
     (slot_sums,) = on_core(
         slot_sum_kernel,
         [((experts * padded, wdev), BF)],
@@ -279,13 +286,12 @@
     back = swap(slot_sums.reshape(experts, padded, wdev), SP)
     back = back.reshape(experts * padded, wdev)
 
-    total = terms[0].astype(F32)
-    for d in range(1, n_x):
-        total = total + turned(terms[d], "x", -d).astype(F32)
-    weight_grads = total.astype(BF)
-    gate_grad, lin_grad, down_grad = (weight_grads[k : k + 1] for k in range(3))
-
-    (row_grads,) = on_core(combine_kernel, [((n_tp, tokens, wdev), BF)], place, back)
+    spread = [terms[0]] + [turned(terms[d], "x", -d) for d in range(1, n_x)]
+    gate_grad, lin_grad, down_grad = (
+        sum(t[k : k + 1].astype(F32) for t in spread).astype(BF) for k in range(3)
+    )
+
+    (row_grads,) = on_core(combine_kernel, [((n_tp, tokens, wdev), BF)], place.T, back)
     full = swap(row_grads, TP)
 
     taps = conv_taps.shape[0]

time: 241 us -> 208 us (0.86)
  the two profiles are of different devices: /device:TPU:6 before, /device:TPU:10 now
where the time goes in v3:
time: 208 us; the launch traced here: 207 us
  waiting for transfers between devices  102 us (49%)
  starting transfers between devices  78.5 us (38%)
  Pallas kernels  14.8 us (7%)
  other arithmetic  5.98 us (3%)
  blocking collectives  4.27 us (2%)
    all_to_all x6, waiting for transfers between devices, swap(): return lax.all_to_all(blocks, axis, split_axis=0, concat_axis=0, tiled=True)  56.1 us
    all_to_all x6, starting transfers between devices, swap(): return lax.all_to_all(blocks, axis, split_axis=0, concat_axis=0, tiled=True)  42.5 us
    ppermute x6, waiting for transfers between devices, turned(): lax.ppermute(value, axis, [(i, (i + by) % count) for i in range(count)])  36.9 us
    ppermute x6, starting transfers between devices, turned(): lax.ppermute(value, axis, [(i, (i + by) % count) for i in range(count)])  20.9 us
    pallas_call x6, Pallas kernels, on_core(): pl.pallas_call(functools.partial(kernel, **static) if static else kernel,...  12.5 us
    ppermute x5, starting transfers between devices, mirrored(): lax.ppermute(value, axis, [(i, i ^ bit) for i in range(lax.axis_size(axis...  11.6 us
    ppermute x5, waiting for transfers between devices, mirrored(): lax.ppermute(value, axis, [(i, i ^ bit) for i in range(lax.axis_size(axis...  9.38 us
    all_to_all x1, blocking collectives, swap(): return lax.all_to_all(blocks, axis, split_axis=0, concat_axis=0, tiled=True)  4.27 us
  transfers between devices with their start and end apart: 19, of which 10 were waited for; matrix products, arithmetic and copies ran while one was open for 3% of the time, Pallas kernels for 5%

profile of v3, /device:TPU:10, one launch (start us, length us, event | category | flops | bytes accessed | tf_op | source)
XLA Modules:
  0.0 207.3 jit_solution(762241440524232549)
XLA Ops:
  0.7 2.3 %route.1 = (bf16[160,8,128]{2,1,0:T(8,128)(2,1)}, s32[2,256]{1,0:T(2,128)}) custom-call(s32[1]{0:T(128)} %bitcast.yi_ref, s32[1]{0:T(128)} %bitcast.1.xi_ref, s32[2,256]{1,0:T(2,128)} %bitcast.45, f32[2,256]{1,0:T(2,128)} %bitcast.46, bf16[256,2048]{1,0:T(8,128)(2,1)} %rows_ref.1, bf16[256,2048]{1,0:T(8,128)(2,1)} %out_grad_ref.1), custom_call_target="tpu_custom_call" | custom-call | tf_op jit(solution)/shard_map/route/pallas_call | solution.py:106
  3.0 15.5 %all-to-all-start = ((bf16[32,40,128]{2,1,0:T(8,128)(2,1)}), bf16[32,40,128]{2,1,0:T(8,128)(2,1)S(1)}, u32[]{:S(2)}, u32[]{:S(2)}) async-start(bf16[32,40,128]{2,1,0:T(8,128)(2,1)} %bitcast.43), calls=%async_computation | async-start | bytes 655360 | tf_op jit(solution)/shard_map/all_to_all | solution.py:22
  18.5 25.4 %all-to-all-done = bf16[32,40,128]{2,1,0:T(8,128)(2,1)S(1)} async-done(((bf16[32,40,128]{2,1,0:T(8,128)(2,1)}), bf16[32,40,128]{2,1,0:T(8,128)(2,1)S(1)}, u32[]{:S(2)}, u32[]{:S(2)}) %all-to-all-start) | async-done | bytes 327712 | tf_op jit(solution)/shard_map/all_to_all | solution.py:22
  43.9 1.5 shard_map.171
  45.4 5.0 %all-to-all-start.1 = ((bf16[4,8,160,128]{3,2,1,0:T(8,128)(2,1)}), bf16[4,8,160,128]{3,2,1,0:T(8,128)(2,1)S(1)}, u32[]{:S(2)}, u32[]{:S(2)}) async-start(bf16[4,8,160,128]{3,2,1,0:T(8,128)(2,1)} %shard_map.171), calls=%async_computation.1 | async-start | bytes 2621440 | tf_op jit(solution)/shard_map/all_to_all | solution.py:22
  50.5 3.4 %collective-permute-start = (bf16[3,64,2048]{2,1,0:T(8,128)(2,1)S(1)}, bf16[3,64,2048]{2,1,0:T(8,128)(2,1)S(1)}, u32[]{:S(2)}, u32[]{:S(2)}) collective-permute-start(bf16[3,64,2048]{2,1,0:T(8,128)(2,1)S(1)} %constant_dynamic-update-slice_fusion.w0_ref), channel_id=1, source_target_pairs={{0,1},{1,2},{2,3},{3,0},{4,5},{5,6},{6,7},{7,4},{8,9},{9,10},{10,1... | collective-permute-start | bytes 2359304 | tf_op jit(solution)/shard_map/ppermute | solution.py:27
  53.9 3.0 %collective-permute-start.1 = (bf16[3,64,2048]{2,1,0:T(8,128)(2,1)S(1)}, bf16[3,64,2048]{2,1,0:T(8,128)(2,1)}, u32[]{:S(2)}, u32[]{:S(2)}) collective-permute-start(bf16[3,64,2048]{2,1,0:T(8,128)(2,1)S(1)} %constant_dynamic-update-slice_fusion.w0_ref), channel_id=1, source_target_pairs={{0,2},{1,3},{2,0},{3,1},{4,6},{5,7},{6,4},{7,5},{8,10},{9,11},{10,... | collective-permute-start | bytes 2359304 | tf_op jit(solution)/shard_map/ppermute | solution.py:27
  56.9 4.1 %collective-permute-start.2 = (bf16[3,64,2048]{2,1,0:T(8,128)(2,1)S(1)}, bf16[3,64,2048]{2,1,0:T(8,128)(2,1)}, u32[]{:S(2)}, u32[]{:S(2)}) collective-permute-start(bf16[3,64,2048]{2,1,0:T(8,128)(2,1)S(1)} %constant_dynamic-update-slice_fusion.w0_ref), channel_id=1, source_target_pairs={{0,3},{1,0},{2,1},{3,2},{4,7},{5,4},{6,5},{7,6},{8,11},{9,8},{10,9... | collective-permute-start | bytes 2359304 | tf_op jit(solution)/shard_map/ppermute | solution.py:27
  61.0 2.1 %collective-permute-start.6 = (bf16[64,128]{1,0:T(8,128)(2,1)S(1)}, bf16[64,128]{1,0:T(8,128)(2,1)S(1)}, u32[]{:S(2)}, u32[]{:S(2)}) collective-permute-start(bf16[64,128]{1,0:T(8,128)(2,1)S(1)} %bitcast.44), channel_id=1, source_target_pairs={{0,256},{32,288},{64,320},{96,352},{128,384},{160,416},{192,448},{... | collective-permute-start | bytes 49160 | tf_op jit(solution)/shard_map/ppermute | solution.py:31
  63.1 9.7 %collective-permute-done.w1_ref = bf16[3,64,2048]{2,1,0:T(8,128)(2,1)S(1)} collective-permute-done((bf16[3,64,2048]{2,1,0:T(8,128)(2,1)S(1)}, bf16[3,64,2048]{2,1,0:T(8,128)(2,1)S(1)}, u32[]{:S(2)}, u32[]{:S(2)}) %collective-permute-start) | collective-permute-done | bytes 786464 | tf_op jit(solution)/shard_map/ppermute | solution.py:27
  72.8 5.1 %collective-permute-done.1.w2_ref = bf16[3,64,2048]{2,1,0:T(8,128)(2,1)} collective-permute-done((bf16[3,64,2048]{2,1,0:T(8,128)(2,1)S(1)}, bf16[3,64,2048]{2,1,0:T(8,128)(2,1)}, u32[]{:S(2)}, u32[]{:S(2)}) %collective-permute-start.1) | collective-permute-done | bytes 786464 | tf_op jit(solution)/shard_map/ppermute | solution.py:27
  77.8 14.8 %collective-permute-done.2.w3_ref = bf16[3,64,2048]{2,1,0:T(8,128)(2,1)} collective-permute-done((bf16[3,64,2048]{2,1,0:T(8,128)(2,1)S(1)}, bf16[3,64,2048]{2,1,0:T(8,128)(2,1)}, u32[]{:S(2)}, u32[]{:S(2)}) %collective-permute-start.2) | collective-permute-done | bytes 786464 | tf_op jit(solution)/shard_map/ppermute | solution.py:27
  92.6 4.5 %shard_map.172 = (bf16[16,160,128]{2,1,0:T(8,128)(2,1)}, bf16[3,160,256]{2,1,0:T(8,128)(2,1)S(1)}) custom-call(bf16[4,8,160,128]{3,2,1,0:T(8,128)(2,1)S(1)} %all-to-all-done.1.got_ref, bf16[3,64,2048]{2,1,0:T(8,128)(2,1)S(1)} %constant_dynamic-update-slice_fusion.w0_ref, bf16[3,64,2048]{2,1,0:T(8,128)(2,1)S(1)} %collective-permute-done.w1_ref, ...), custom_call_target="tpu_custom_call" | custom-call | tf_op jit(solution)/shard_map/pallas_call | solution.py:218
  97.1 6.5 %all-to-all-start.2 = ((bf16[16,160,128]{2,1,0:T(8,128)(2,1)}), bf16[16,160,128]{2,1,0:T(8,128)(2,1)S(1)}, u32[]{:S(2)}, u32[]{:S(2)}) async-start(bf16[16,160,128]{2,1,0:T(8,128)(2,1)} %get-tuple-element.25), calls=%async_computation.2 | async-start | bytes 1310720 | tf_op jit(solution)/shard_map/all_to_all | solution.py:22
  103.6 1.9 collective-permute-start.7
  105.6 8.0 %collective-permute-done.7 = bf16[2,64,128]{2,1,0:T(8,128)(2,1)S(1)} collective-permute-done((bf16[2,64,128]{2,1,0:T(8,128)(2,1)S(1)}, bf16[2,64,128]{2,1,0:T(8,128)(2,1)S(1)}, u32[]{:S(2)}, u32[]{:S(2)}) %collective-permute-start.7) | collective-permute-done | bytes 32800 | tf_op jit(solution)/shard_map/ppermute | solution.py:31
  113.6 2.1 %collective-permute-start.8 = (bf16[2,2,64,128]{3,2,0,1:T(8,128)(2,1)S(1)}, bf16[2,2,64,128]{3,2,0,1:T(8,128)(2,1)S(1)}, u32[]{:S(2)}, u32[]{:S(2)}) collective-permute-start(bf16[2,2,64,128]{3,2,0,1:T(8,128)(2,1)S(1)} %pad_maximum_fusion.3), channel_id=1, source_target_pairs={{0,64},{32,96},{64,0},{96,32},{128,192},{160,224},{192,128},{224,1... | collective-permute-start | bytes 196616 | tf_op jit(solution)/shard_map/ppermute | solution.py:31
  115.7 1.5 shard_map.174
  117.2 4.7 %all-to-all-start.3 = ((bf16[32,24,128]{2,1,0:T(8,128)(2,1)}), bf16[32,24,128]{2,1,0:T(8,128)(2,1)S(1)}, u32[]{:S(2)}, u32[]{:S(2)}) async-start(bf16[32,24,128]{2,1,0:T(8,128)(2,1)} %bitcast.7), calls=%async_computation.3 | async-start | bytes 393216 | tf_op jit(solution)/shard_map/all_to_all | solution.py:22
  122.0 2.2 %collective-permute-start.11 = (bf16[2,128]{1,0:T(2,128)(2,1)S(1)}, bf16[2,128]{1,0:T(2,128)(2,1)S(1)}, u32[]{:S(2)}, u32[]{:S(2)}) collective-permute-start(bf16[2,128]{1,0:T(2,128)(2,1)S(1)} %slice.104), channel_id=1, source_target_pairs={{0,16},{16,32},{32,48},{48,64},{64,80},{80,96},{96,112},{112,128},... | collective-permute-start | bytes 1544 | tf_op jit(solution)/shard_map/ppermute | solution.py:49
  124.2 0.1 copy.21
  124.4 3.5 %collective-permute-start.9 = (bf16[2,2,2,64,128]{4,3,0,1,2:T(8,128)(2,1)S(1)}, bf16[2,2,2,64,128]{4,3,0,1,2:T(8,128)(2,1)S(1)}, u32[]{:S(2)}, u32[]{:S(2)}) collective-permute-start(bf16[2,2,2,64,128]{4,3,0,1,2:T(8,128)(2,1)S(1)} %pad_maximum_fusion.2), channel_id=1, source_target_pairs={{0,32},{32,0},{64,96},{96,64},{128,160},{160,128},{192,224},{224,1... | collective-permute-start | bytes 393224 | tf_op jit(solution)/shard_map/ppermute | solution.py:31
  128.0 14.1 %all-to-all-done.3 = bf16[32,24,128]{2,1,0:T(8,128)(2,1)S(1)} async-done(((bf16[32,24,128]{2,1,0:T(8,128)(2,1)}), bf16[32,24,128]{2,1,0:T(8,128)(2,1)S(1)}, u32[]{:S(2)}, u32[]{:S(2)}) %all-to-all-start.3) | async-done | bytes 196640 | tf_op jit(solution)/shard_map/all_to_all | solution.py:22
  142.1 1.4 shard_map.175
  143.5 7.2 %all-to-all-start.4 = ((bf16[16,256,128]{2,1,0:T(8,128)(2,1)}), bf16[16,256,128]{2,1,0:T(8,128)(2,1)S(1)}, u32[]{:S(2)}, u32[]{:S(2)}) async-start(bf16[16,256,128]{2,1,0:T(8,128)(2,1)} %shard_map.175), calls=%async_computation.4 | async-start | bytes 2097152 | tf_op jit(solution)/shard_map/all_to_all | solution.py:22
  150.8 2.3 %shard_map.173 = (bf16[3,64,2048]{2,1,0:T(8,128)(2,1)S(1)}, bf16[3,64,2048]{2,1,0:T(8,128)(2,1)}, bf16[3,64,2048]{2,1,0:T(8,128)(2,1)}, bf16[3,64,2048]{2,1,0:T(8,128)(2,1)}) custom-call(bf16[4,8,160,128]{3,2,1,0:T(8,128)(2,1)S(1)} %all-to-all-done.1.got_ref, bf16[3,160,256]{2,1,0:T(8,128)(2,1)S(1)} %get-tuple-element.19.cots_ref), custom_call_target="tpu_custom_call" | custom-call | tf_op jit(solution)/shard_map/pallas_call | solution.py:218
  153.2 3.4 %collective-permute-start.5 = (bf16[3,64,2048]{2,1,0:T(8,128)(2,1)}, bf16[3,64,2048]{2,1,0:T(8,128)(2,1)}, u32[]{:S(2)}, u32[]{:S(2)}) collective-permute-start(bf16[3,64,2048]{2,1,0:T(8,128)(2,1)} %get-tuple-element.23), channel_id=1, source_target_pairs={{0,1},{1,2},{2,3},{3,0},{4,5},{5,6},{6,7},{7,4},{8,9},{9,10},{10,1... | collective-permute-start | bytes 2359304 | tf_op jit(solution)/shard_map/ppermute | solution.py:27
  156.5 3.1 %collective-permute-start.4 = (bf16[3,64,2048]{2,1,0:T(8,128)(2,1)}, bf16[3,64,2048]{2,1,0:T(8,128)(2,1)}, u32[]{:S(2)}, u32[]{:S(2)}) collective-permute-start(bf16[3,64,2048]{2,1,0:T(8,128)(2,1)} %get-tuple-element.22), channel_id=1, source_target_pairs={{0,2},{1,3},{2,0},{3,1},{4,6},{5,7},{6,4},{7,5},{8,10},{9,11},{10,... | collective-permute-start | bytes 2359304 | tf_op jit(solution)/shard_map/ppermute | solution.py:27
  159.6 4.0 %collective-permute-start.3 = (bf16[3,64,2048]{2,1,0:T(8,128)(2,1)}, bf16[3,64,2048]{2,1,0:T(8,128)(2,1)}, u32[]{:S(2)}, u32[]{:S(2)}) collective-permute-start(bf16[3,64,2048]{2,1,0:T(8,128)(2,1)} %get-tuple-element.21), channel_id=1, source_target_pairs={{0,3},{1,0},{2,1},{3,2},{4,7},{5,4},{6,5},{7,6},{8,11},{9,8},{10,9... | collective-permute-start | bytes 2359304 | tf_op jit(solution)/shard_map/ppermute | solution.py:27
  163.6 1.9 collective-permute-start.10
  165.6 0.1 multiply_convert_fusion
  165.7 1.4 collective-permute-done.10
  167.1 0.0 copy-start
  167.1 0.1 pad_maximum_fusion
  167.2 10.7 %all-to-all-done.4.full_ref = bf16[16,256,128]{2,1,0:T(8,128)(2,1)S(1)} async-done(((bf16[16,256,128]{2,1,0:T(8,128)(2,1)}), bf16[16,256,128]{2,1,0:T(8,128)(2,1)S(1)}, u32[]{:S(2)}, u32[]{:S(2)}) %all-to-all-start.4) | async-done | bytes 1048608 | tf_op jit(solution)/shard_map/all_to_all | solution.py:22
  178.0 1.3 shard_map.176
  179.3 4.3 %all_to_all.35 = bf16[2,16,64,128]{3,2,1,0:T(8,128)(2,1)S(1)} all-to-all(bf16[2,16,64,128]{3,2,1,0:T(8,128)(2,1)S(1)} %get-tuple-element.26), channel_id=1, replica_groups=mesh['z'=16,'c'=2,'y'=4,'x'=4] {'c'}, dimensions={0} | all-to-all | bytes 1048576 | tf_op jit(solution)/shard_map/all_to_all | solution.py:22
  183.6 0.8 reduce_sum.21
  184.4 3.5 %all-to-all-start.6 = ((bf16[16,64,128]{2,1,0:T(8,128)(2,1)}), bf16[16,64,128]{2,1,0:T(8,128)(2,1)S(1)}, u32[]{:S(2)}, u32[]{:S(2)}) async-start(bf16[16,64,128]{2,1,0:T(8,128)(2,1)} %reduce_sum.21), calls=%async_computation.6 | async-start | bytes 524288 | tf_op jit(solution)/shard_map/all_to_all | solution.py:22
  187.9 1.3 collective-permute-start.12
  189.2 0.0 collective-permute-done.5
  189.3 0.0 collective-permute-done.4
  189.3 7.3 %collective-permute-done.3 = bf16[3,64,2048]{2,1,0:T(8,128)(2,1)} collective-permute-done((bf16[3,64,2048]{2,1,0:T(8,128)(2,1)}, bf16[3,64,2048]{2,1,0:T(8,128)(2,1)}, u32[]{:S(2)}, u32[]{:S(2)}) %collective-permute-start.3) | collective-permute-done | bytes 786464 | tf_op jit(solution)/shard_map/ppermute | solution.py:27
  196.6 2.8 %add_convert_fusion = (bf16[1,64,2048]{2,1,0:T(8,128)(2,1)}, bf16[1,64,2048]{2,1,0:T(8,128)(2,1)}, bf16[1,64,2048]{2,1,0:T(8,128)(2,1)}) fusion(bf16[3,64,2048]{2,1,0:T(8,128)(2,1)} %collective-permute-done.5, bf16[3,64,2048]{2,1,0:T(8,128)(2,1)} %collective-permute-done.4, bf16[3,64,2048]{2,1,0:T(8,128)(2,1)} %collective-permute-done.3, ...), kind=kLoop, calls=%fused_computation.2 | loop fusion | flops 3145728 | bytes 3932160 | tf_op jit(solution)/shard_map/convert_element_type | solution.py:291
  199.4 0.7 fusion
  200.1 0.7 fusion.2
  200.8 5.9 %all-to-all-done.6 = bf16[16,64,128]{2,1,0:T(8,128)(2,1)S(1)} async-done(((bf16[16,64,128]{2,1,0:T(8,128)(2,1)}), bf16[16,64,128]{2,1,0:T(8,128)(2,1)S(1)}, u32[]{:S(2)}, u32[]{:S(2)}) %all-to-all-start.6) | async-done | bytes 262176 | tf_op jit(solution)/shard_map/all_to_all | solution.py:22
  206.7 0.7 convert_reduce_fusion
  (49 shorter events, 0.4 us)
Async XLA Ops:
  0.6 17.8 %copy-start.5 = (bf16[1,64,2048]{2,1,0:T(8,128)(2,1)S(1)}, bf16[1,64,2048]{2,1,0:T(8,128)(2,1)}, u32[]{:S(2)}) copy-start(bf16[1,64,2048]{2,1,0:T(8,128)(2,1)} %param.16) | copy-start | bytes 786436
  0.6 17.8 %copy-start.6 = (bf16[1,64,2048]{2,1,0:T(8,128)(2,1)S(1)}, bf16[1,64,2048]{2,1,0:T(8,128)(2,1)}, u32[]{:S(2)}) copy-start(bf16[1,64,2048]{2,1,0:T(8,128)(2,1)} %param.17) | copy-start | bytes 786436
  3.0 41.0 %all-to-all-start = ((bf16[32,40,128]{2,1,0:T(8,128)(2,1)}), bf16[32,40,128]{2,1,0:T(8,128)(2,1)S(1)}, u32[]{:S(2)}, u32[]{:S(2)}) async-start(bf16[32,40,128]{2,1,0:T(8,128)(2,1)} %bitcast.43), calls=%async_computation | async-start | bytes 655360 | tf_op jit(solution)/shard_map/all_to_all | solution.py:22
  45.4 5.1 %copy-start.7 = (bf16[1,64,2048]{2,1,0:T(8,128)(2,1)S(1)}, bf16[1,64,2048]{2,1,0:T(8,128)(2,1)}, u32[]{:S(2)}) copy-start(bf16[1,64,2048]{2,1,0:T(8,128)(2,1)} %param.18) | copy-start | bytes 786436
  45.4 15.6 %copy-start.9 = (bf16[128,64]{0,1:T(8,128)(2,1)S(1)}, bf16[128,64]{0,1:T(8,128)(2,1)}, u32[]{:S(2)}) copy-start(bf16[128,64]{0,1:T(8,128)(2,1)} %param.23) | copy-start | bytes 49156
  45.4 47.2 %all-to-all-start.1 = ((bf16[4,8,160,128]{3,2,1,0:T(8,128)(2,1)}), bf16[4,8,160,128]{3,2,1,0:T(8,128)(2,1)S(1)}, u32[]{:S(2)}, u32[]{:S(2)}) async-start(bf16[4,8,160,128]{3,2,1,0:T(8,128)(2,1)} %shard_map.171), calls=%async_computation.1 | async-start | bytes 2621440 | tf_op jit(solution)/shard_map/all_to_all | solution.py:22
  50.5 22.3 %collective-permute-start = (bf16[3,64,2048]{2,1,0:T(8,128)(2,1)S(1)}, bf16[3,64,2048]{2,1,0:T(8,128)(2,1)S(1)}, u32[]{:S(2)}, u32[]{:S(2)}) collective-permute-start(bf16[3,64,2048]{2,1,0:T(8,128)(2,1)S(1)} %constant_dynamic-update-slice_fusion.w0_ref), channel_id=1, source_target_pairs={{0,1},{1,2},{2,3},{3,0},{4,5},{5,6},{6,7},{7,4},{8,9},{9,10},{10,1... | collective-permute-start | bytes 2359304 | tf_op jit(solution)/shard_map/ppermute | solution.py:27
  53.9 24.0 %collective-permute-start.1 = (bf16[3,64,2048]{2,1,0:T(8,128)(2,1)S(1)}, bf16[3,64,2048]{2,1,0:T(8,128)(2,1)}, u32[]{:S(2)}, u32[]{:S(2)}) collective-permute-start(bf16[3,64,2048]{2,1,0:T(8,128)(2,1)S(1)} %constant_dynamic-update-slice_fusion.w0_ref), channel_id=1, source_target_pairs={{0,2},{1,3},{2,0},{3,1},{4,6},{5,7},{6,4},{7,5},{8,10},{9,11},{10,... | collective-permute-start | bytes 2359304 | tf_op jit(solution)/shard_map/ppermute | solution.py:27
  56.9 35.7 %collective-permute-start.2 = (bf16[3,64,2048]{2,1,0:T(8,128)(2,1)S(1)}, bf16[3,64,2048]{2,1,0:T(8,128)(2,1)}, u32[]{:S(2)}, u32[]{:S(2)}) collective-permute-start(bf16[3,64,2048]{2,1,0:T(8,128)(2,1)S(1)} %constant_dynamic-update-slice_fusion.w0_ref), channel_id=1, source_target_pairs={{0,3},{1,0},{2,1},{3,2},{4,7},{5,4},{6,5},{7,6},{8,11},{9,8},{10,9... | collective-permute-start | bytes 2359304 | tf_op jit(solution)/shard_map/ppermute | solution.py:27
  61.0 42.6 %collective-permute-start.6 = (bf16[64,128]{1,0:T(8,128)(2,1)S(1)}, bf16[64,128]{1,0:T(8,128)(2,1)S(1)}, u32[]{:S(2)}, u32[]{:S(2)}) collective-permute-start(bf16[64,128]{1,0:T(8,128)(2,1)S(1)} %bitcast.44), channel_id=1, source_target_pairs={{0,256},{32,288},{64,320},{96,352},{128,384},{160,416},{192,448},{... | collective-permute-start | bytes 49160 | tf_op jit(solution)/shard_map/ppermute | solution.py:31
  97.1 24.9 %copy-start.4 = (bf16[256,128]{1,0:T(8,128)(2,1)S(1)}, bf16[256,128]{1,0:T(8,128)(2,1)}, u32[]{:S(2)}) copy-start(bf16[256,128]{1,0:T(8,128)(2,1)} %param.20) | copy-start | bytes 196612
  97.1 24.9 %copy-start.8 = (bf16[256,128]{1,0:T(8,128)(2,1)S(1)}, bf16[256,128]{1,0:T(8,128)(2,1)}, u32[]{:S(2)}) copy-start(bf16[256,128]{1,0:T(8,128)(2,1)} %param.21) | copy-start | bytes 196612
  97.1 27.1 %copy-start.10 = (s32[2,256]{1,0:T(2,128)S(1)}, s32[2,256]{1,0:T(2,128)}, u32[]{:S(2)}) copy-start(s32[2,256]{1,0:T(2,128)} %get-tuple-element.24) | copy-start | bytes 6148
  97.1 18.6 %all-to-all-start.2 = ((bf16[16,160,128]{2,1,0:T(8,128)(2,1)}), bf16[16,160,128]{2,1,0:T(8,128)(2,1)S(1)}, u32[]{:S(2)}, u32[]{:S(2)}) async-start(bf16[16,160,128]{2,1,0:T(8,128)(2,1)} %get-tuple-element.25), calls=%async_computation.2 | async-start | bytes 1310720 | tf_op jit(solution)/shard_map/all_to_all | solution.py:22
  103.6 24.4 %copy-start.11 = (f32[3,128]{1,0:T(4,128)S(1)}, f32[3,128]{1,0:T(4,128)}, u32[]{:S(2)}) copy-start(f32[3,128]{1,0:T(4,128)} %param.22) | copy-start | bytes 4612
  103.6 9.9 %collective-permute-start.7 = (bf16[2,64,128]{2,1,0:T(8,128)(2,1)S(1)}, bf16[2,64,128]{2,1,0:T(8,128)(2,1)S(1)}, u32[]{:S(2)}, u32[]{:S(2)}) collective-permute-start(bf16[2,64,128]{2,1,0:T(8,128)(2,1)S(1)} %pad_maximum_fusion.4), channel_id=1, source_target_pairs={{0,128},{32,160},{64,192},{96,224},{128,0},{160,32},{192,64},{224,... | collective-permute-start | bytes 98312 | tf_op jit(solution)/shard_map/ppermute | solution.py:31
  113.6 10.8 %collective-permute-start.8 = (bf16[2,2,64,128]{3,2,0,1:T(8,128)(2,1)S(1)}, bf16[2,2,64,128]{3,2,0,1:T(8,128)(2,1)S(1)}, u32[]{:S(2)}, u32[]{:S(2)}) collective-permute-start(bf16[2,2,64,128]{3,2,0,1:T(8,128)(2,1)S(1)} %pad_maximum_fusion.3), channel_id=1, source_target_pairs={{0,64},{32,96},{64,0},{96,32},{128,192},{160,224},{192,128},{224,1... | collective-permute-start | bytes 196616 | tf_op jit(solution)/shard_map/ppermute | solution.py:31
  117.2 24.9 %all-to-all-start.3 = ((bf16[32,24,128]{2,1,0:T(8,128)(2,1)}), bf16[32,24,128]{2,1,0:T(8,128)(2,1)S(1)}, u32[]{:S(2)}, u32[]{:S(2)}) async-start(bf16[32,24,128]{2,1,0:T(8,128)(2,1)} %bitcast.7), calls=%async_computation.3 | async-start | bytes 393216 | tf_op jit(solution)/shard_map/all_to_all | solution.py:22
  122.0 43.6 %collective-permute-start.11 = (bf16[2,128]{1,0:T(2,128)(2,1)S(1)}, bf16[2,128]{1,0:T(2,128)(2,1)S(1)}, u32[]{:S(2)}, u32[]{:S(2)}) collective-permute-start(bf16[2,128]{1,0:T(2,128)(2,1)S(1)} %slice.104), channel_id=1, source_target_pairs={{0,16},{16,32},{32,48},{48,64},{64,80},{80,96},{96,112},{112,128},... | collective-permute-start | bytes 1544 | tf_op jit(solution)/shard_map/ppermute | solution.py:49
  124.4 26.3 %collective-permute-start.9 = (bf16[2,2,2,64,128]{4,3,0,1,2:T(8,128)(2,1)S(1)}, bf16[2,2,2,64,128]{4,3,0,1,2:T(8,128)(2,1)S(1)}, u32[]{:S(2)}, u32[]{:S(2)}) collective-permute-start(bf16[2,2,2,64,128]{4,3,0,1,2:T(8,128)(2,1)S(1)} %pad_maximum_fusion.2), channel_id=1, source_target_pairs={{0,32},{32,0},{64,96},{96,64},{128,160},{160,128},{192,224},{224,1... | collective-permute-start | bytes 393224 | tf_op jit(solution)/shard_map/ppermute | solution.py:31
  143.5 34.4 %all-to-all-start.4 = ((bf16[16,256,128]{2,1,0:T(8,128)(2,1)}), bf16[16,256,128]{2,1,0:T(8,128)(2,1)S(1)}, u32[]{:S(2)}, u32[]{:S(2)}) async-start(bf16[16,256,128]{2,1,0:T(8,128)(2,1)} %shard_map.175), calls=%async_computation.4 | async-start | bytes 2097152 | tf_op jit(solution)/shard_map/all_to_all | solution.py:22
  150.8 14.8 %copy-start.3 = (bf16[256,128]{1,0:T(8,128)(2,1)S(1)}, bf16[256,128]{1,0:T(8,128)(2,1)}, u32[]{:S(2)}) copy-start(bf16[256,128]{1,0:T(8,128)(2,1)} %outer_ref.1) | copy-start | bytes 196612
  153.2 14.0 %copy-start.1 = (bf16[3,64,2048]{2,1,0:T(8,128)(2,1)}, bf16[3,64,2048]{2,1,0:T(8,128)(2,1)S(1)}, u32[]{:S(2)}) copy-start(bf16[3,64,2048]{2,1,0:T(8,128)(2,1)S(1)} %get-tuple-element.20) | copy-start | bytes 2359300
  153.2 36.1 %collective-permute-start.5 = (bf16[3,64,2048]{2,1,0:T(8,128)(2,1)}, bf16[3,64,2048]{2,1,0:T(8,128)(2,1)}, u32[]{:S(2)}, u32[]{:S(2)}) collective-permute-start(bf16[3,64,2048]{2,1,0:T(8,128)(2,1)} %get-tuple-element.23), channel_id=1, source_target_pairs={{0,1},{1,2},{2,3},{3,0},{4,5},{5,6},{6,7},{7,4},{8,9},{9,10},{10,1... | collective-permute-start | bytes 2359304 | tf_op jit(solution)/shard_map/ppermute | solution.py:27
  156.5 32.7 %collective-permute-start.4 = (bf16[3,64,2048]{2,1,0:T(8,128)(2,1)}, bf16[3,64,2048]{2,1,0:T(8,128)(2,1)}, u32[]{:S(2)}, u32[]{:S(2)}) collective-permute-start(bf16[3,64,2048]{2,1,0:T(8,128)(2,1)} %get-tuple-element.22), channel_id=1, source_target_pairs={{0,2},{1,3},{2,0},{3,1},{4,6},{5,7},{6,4},{7,5},{8,10},{9,11},{10,... | collective-permute-start | bytes 2359304 | tf_op jit(solution)/shard_map/ppermute | solution.py:27
  159.6 37.0 %collective-permute-start.3 = (bf16[3,64,2048]{2,1,0:T(8,128)(2,1)}, bf16[3,64,2048]{2,1,0:T(8,128)(2,1)}, u32[]{:S(2)}, u32[]{:S(2)}) collective-permute-start(bf16[3,64,2048]{2,1,0:T(8,128)(2,1)} %get-tuple-element.21), channel_id=1, source_target_pairs={{0,3},{1,0},{2,1},{3,2},{4,7},{5,4},{6,5},{7,6},{8,11},{9,8},{10,9... | collective-permute-start | bytes 2359304 | tf_op jit(solution)/shard_map/ppermute | solution.py:27
  163.6 3.4 %collective-permute-start.10 = (bf16[2,2,2,2,64,128]{5,4,0,1,2,3:T(8,128)(2,1)S(1)}, bf16[2,2,2,2,64,128]{5,4,0,1,2,3:T(8,128)(2,1)S(1)}, u32[]{:S(2)}, u32[]{:S(2)}) collective-permute-start(bf16[2,2,2,2,64,128]{5,4,0,1,2,3:T(8,128)(2,1)S(1)} %pad_maximum_fusion.1), channel_id=1, source_target_pairs={{0,16},{16,0},{1,17},{17,1},{2,18},{18,2},{3,19},{19,3},{4,20},{20... | collective-permute-start | bytes 786440 | tf_op jit(solution)/shard_map/ppermute | solution.py:31
  167.1 10.9 %copy-start = (bf16[256,2048]{1,0:T(8,128)(2,1)S(1)}, bf16[256,2048]{1,0:T(8,128)(2,1)}, u32[]{:S(2)}) copy-start(bf16[256,2048]{1,0:T(8,128)(2,1)} %out_grad_ref.1) | copy-start | bytes 3145732
  179.3 17.3 %copy-start.2 = (bf16[3,64,2048]{2,1,0:T(8,128)(2,1)S(1)}, bf16[3,64,2048]{2,1,0:T(8,128)(2,1)}, u32[]{:S(2)}) copy-start(bf16[3,64,2048]{2,1,0:T(8,128)(2,1)} %copy-done.1) | copy-start | bytes 2359300
  184.4 22.3 %all-to-all-start.6 = ((bf16[16,64,128]{2,1,0:T(8,128)(2,1)}), bf16[16,64,128]{2,1,0:T(8,128)(2,1)S(1)}, u32[]{:S(2)}, u32[]{:S(2)}) async-start(bf16[16,64,128]{2,1,0:T(8,128)(2,1)} %reduce_sum.21), calls=%async_computation.6 | async-start | bytes 524288 | tf_op jit(solution)/shard_map/all_to_all | solution.py:22
  187.9 11.5 %collective-permute-start.12 = (bf16[2,128]{1,0:T(2,128)(2,1)S(1)}, bf16[2,128]{1,0:T(2,128)(2,1)S(1)}, u32[]{:S(2)}, u32[]{:S(2)}) collective-permute-start(bf16[2,128]{1,0:T(2,128)(2,1)S(1)} %slice.91), channel_id=1, source_target_pairs={{16,0},{32,16},{48,32},{64,48},{80,64},{96,80},{112,96},{128,112},... | collective-permute-start | bytes 1544 | tf_op jit(solution)/shard_map/ppermute | solution.py:49

commit v4 on v3

--- a/solution.py
+++ b/solution.py
@@ -199,25 +199,73 @@
         out_ref[t] = row_grads
 
 
-def mixer_kernel(full_ref, out_grad_ref, proj_ref, mixed_ref, convolved_ref, outer_ref, terms_ref, outer_grad_ref, cot_ref):
+def mixer_kernel(
+    full_ref, out_grad_ref, proj_ref, mixed_hbm, convolved_hbm, outer_hbm,
+    terms_ref, cot_ref, outer_grad_hbm,
+    mixed_ref, convolved_ref, outer_ref, outer_grad_ref, sems,
+):
     n_tp, _, _ = full_ref.shape
     n_c, n_z, per, _ = terms_ref.shape
+    fetches = [
+        pltpu.make_async_copy(src, dst, sems.at[i])
+        for i, (src, dst) in enumerate(
+            ((convolved_hbm, convolved_ref), (outer_hbm, outer_ref), (mixed_hbm, mixed_ref))
+        )
+    ]
+    for fetch in fetches:
+        fetch.start()
     full = jnp.concatenate([full_ref[t] for t in range(n_tp)], axis=1)
     stream = (out_grad_ref[...].astype(F32) + full.astype(F32)).astype(BF)
+    mixed_grad = dot(stream, proj_ref[...], 1, 0)
+    fetches[0].wait()
+    outer_grad_ref[...] = (mixed_grad * convolved_ref[...]).astype(BF)
+    keep = pltpu.make_async_copy(outer_grad_ref, outer_grad_hbm, sems.at[3])
+    keep.start()
+    fetches[1].wait()
+    cot_ref[...] = (mixed_grad * outer_ref[...].astype(F32)).astype(BF)
+    fetches[2].wait()
     terms = dot(stream, mixed_ref[...], 0, 0).astype(BF)
     for z in range(n_z):
         for c in range(n_c):
             at = (z * n_c + c) * per
             terms_ref[c, z] = terms[at : at + per]
-    mixed_grad = dot(stream, proj_ref[...], 1, 0)
-    outer_grad_ref[...] = (mixed_grad * convolved_ref[...]).astype(BF)
-    cot_ref[...] = (mixed_grad * outer_ref[...].astype(F32)).astype(BF)
+    keep.wait()
+
+
+def in_hbm(value):
+    return pltpu.with_memory_space_constraint(value, pltpu.HBM)
+
+
+def mix(full, out_grad, proj, mixed, convolved, outer_gate, n_c, n_z):
+    _, tokens, lanes = full.shape
+    small = (tokens, lanes)
+    whole = pl.BlockSpec(memory_space=pltpu.VMEM)
+    away = pl.BlockSpec(memory_space=pltpu.HBM)
+    return pl.pallas_call(
+        mixer_kernel,
+        in_specs=[whole, whole, whole, away, away, away],
+        out_specs=[whole, whole, away],
+        out_shape=[
+            pltpu.HBM((n_c, n_z, proj.shape[0] // (n_c * n_z), lanes), BF),
+            pltpu.HBM(small, BF),
+            pltpu.HBM(small, BF),
+        ],
+        scratch_shapes=[
+            pltpu.VMEM(small, BF),
+            pltpu.VMEM(small, F32),
+            pltpu.VMEM(small, BF),
+            pltpu.VMEM(small, BF),
+            pltpu.SemaphoreType.DMA((4,)),
+        ],
+        compiler_params=pltpu.CompilerParams(vmem_limit_bytes=16 << 20),
+        name="mixer",
+    )(full, out_grad, proj, *map(in_hbm, (mixed, convolved, outer_gate)))
 
 
 def on_core(kernel, outs, *args, mib=12, **static):
     return pl.pallas_call(
         functools.partial(kernel, **static) if static else kernel,
-        out_shape=[jax.ShapeDtypeStruct(s, t) for s, t in outs],
+        out_shape=[pltpu.HBM(s, t) for s, t in outs],
         compiler_params=pltpu.CompilerParams(vmem_limit_bytes=mib << 20),
     )(*args)
 
@@ -304,15 +352,8 @@
     mixed = (outer_gate.astype(F32) * convolved).astype(BF)
 
     proj = doubled(doubled(out_proj.T, "z"), "c").reshape(width, wdev)
-    pair, outer_gate_grad, conv_cot = on_core(
-        mixer_kernel,
-        [((n_c, n_z, width // n_sp, wdev), BF), ((tokens, wdev), BF), ((tokens, wdev), BF)],
-        full,
-        out_grad,
-        proj,
-        mixed,
-        convolved,
-        outer_gate,
+    pair, conv_cot, outer_gate_grad = mix(
+        full, out_grad, proj, mixed, convolved, outer_gate, n_c, n_z
     )
     terms = swap(pair, "c")
     terms = jnp.sum(terms.astype(F32), axis=0).astype(BF)

time: 208 us -> 210 us (level)
  waiting for transfers between devices: 102 us -> 91.2 us
  starting transfers between devices: 78.5 us -> 86.2 us
    all_to_all x6, waiting for transfers between devices: 56.1 us -> 46.3 us  [swap(): return lax.all_to_all(blocks, axis, split_axis=0, concat_axis=0, tiled=True)]
    all_to_all x6, starting transfers between devices: 42.5 us -> 50.2 us  [swap(): return lax.all_to_all(blocks, axis, split_axis=0, concat_axis=0, tiled=True)]
    pallas_call x0 -> x1, Pallas kernels: none -> 2.69 us  [mix(): pl.pallas_call(mixer_kernel, in_specs=[whole, whole, whole, away, away, a...]
    pallas_call x6 -> x5, Pallas kernels: 12.5 us -> 11.5 us  [on_core(): pl.pallas_call(functools.partial(kernel, **static) if static else kernel,...]
  transfers between devices with their start and end apart: 19 -> 19, of which waited for: 10 -> 9; matrix products, arithmetic and copies ran while one was open for 3% -> 3% of each run, Pallas kernels for 5% -> 6%
where the time goes in v4:
time: 210 us; the launch traced here: 208 us
  waiting for transfers between devices  91.2 us (43%)
  starting transfers between devices  86.2 us (41%)
  Pallas kernels  16.4 us (8%)
  other arithmetic  6.66 us (3%)
  blocking collectives  5.36 us (3%)
    all_to_all x6, starting transfers between devices, swap(): return lax.all_to_all(blocks, axis, split_axis=0, concat_axis=0, tiled=True)  50.2 us
    all_to_all x6, waiting for transfers between devices, swap(): return lax.all_to_all(blocks, axis, split_axis=0, concat_axis=0, tiled=True)  46.3 us
    ppermute x6, waiting for transfers between devices, turned(): lax.ppermute(value, axis, [(i, (i + by) % count) for i in range(count)])  36.2 us
    ppermute x6, starting transfers between devices, turned(): lax.ppermute(value, axis, [(i, (i + by) % count) for i in range(count)])  20.9 us
    ppermute x5, starting transfers between devices, mirrored(): lax.ppermute(value, axis, [(i, i ^ bit) for i in range(lax.axis_size(axis...  11.6 us
    pallas_call x5, Pallas kernels, on_core(): pl.pallas_call(functools.partial(kernel, **static) if static else kernel,...  11.5 us
    ppermute x5, waiting for transfers between devices, mirrored(): lax.ppermute(value, axis, [(i, i ^ bit) for i in range(lax.axis_size(axis...  8.71 us
    all_to_all x1, blocking collectives, swap(): return lax.all_to_all(blocks, axis, split_axis=0, concat_axis=0, tiled=True)  5.36 us
  transfers between devices with their start and end apart: 19, of which 9 were waited for; matrix products, arithmetic and copies ran while one was open for 3% of the time, Pallas kernels for 6%

profile of v4, /device:TPU:10, one launch (start us, length us, event | category | flops | bytes accessed | tf_op | source)
XLA Modules:
  0.0 208.3 jit_solution(12393292667690762419)
XLA Ops:
  0.7 2.3 %route.1 = (bf16[160,8,128]{2,1,0:T(8,128)(2,1)}, s32[2,256]{1,0:T(2,128)}) custom-call(s32[1]{0:T(128)} %bitcast.yi_ref, s32[1]{0:T(128)} %bitcast.1.xi_ref, s32[2,256]{1,0:T(2,128)} %bitcast.46, f32[2,256]{1,0:T(2,128)} %bitcast.47, bf16[256,2048]{1,0:T(8,128)(2,1)} %rows_ref.1, bf16[256,2048]{1,0:T(8,128)(2,1)} %out_grad_ref.1), custom_call_target="tpu_custom_call" | custom-call | tf_op jit(solution)/shard_map/route/pallas_call | solution.py:106
  3.0 15.5 %all-to-all-start = ((bf16[32,40,128]{2,1,0:T(8,128)(2,1)}), bf16[32,40,128]{2,1,0:T(8,128)(2,1)S(1)}, u32[]{:S(2)}, u32[]{:S(2)}) async-start(bf16[32,40,128]{2,1,0:T(8,128)(2,1)} %bitcast.44), calls=%async_computation | async-start | bytes 655360 | tf_op jit(solution)/shard_map/all_to_all | solution.py:22
  18.5 25.4 %all-to-all-done = bf16[32,40,128]{2,1,0:T(8,128)(2,1)S(1)} async-done(((bf16[32,40,128]{2,1,0:T(8,128)(2,1)}), bf16[32,40,128]{2,1,0:T(8,128)(2,1)S(1)}, u32[]{:S(2)}, u32[]{:S(2)}) %all-to-all-start) | async-done | bytes 327712 | tf_op jit(solution)/shard_map/all_to_all | solution.py:22
  43.9 1.5 shard_map.171
  45.4 5.0 %all-to-all-start.1 = ((bf16[4,8,160,128]{3,2,1,0:T(8,128)(2,1)}), bf16[4,8,160,128]{3,2,1,0:T(8,128)(2,1)S(1)}, u32[]{:S(2)}, u32[]{:S(2)}) async-start(bf16[4,8,160,128]{3,2,1,0:T(8,128)(2,1)} %shard_map.171), calls=%async_computation.1 | async-start | bytes 2621440 | tf_op jit(solution)/shard_map/all_to_all | solution.py:22
  50.5 3.4 %collective-permute-start = (bf16[3,64,2048]{2,1,0:T(8,128)(2,1)S(1)}, bf16[3,64,2048]{2,1,0:T(8,128)(2,1)S(1)}, u32[]{:S(2)}, u32[]{:S(2)}) collective-permute-start(bf16[3,64,2048]{2,1,0:T(8,128)(2,1)S(1)} %constant_dynamic-update-slice_fusion.w0_ref), channel_id=1, source_target_pairs={{0,1},{1,2},{2,3},{3,0},{4,5},{5,6},{6,7},{7,4},{8,9},{9,10},{10,1... | collective-permute-start | bytes 2359304 | tf_op jit(solution)/shard_map/ppermute | solution.py:27
  53.9 3.0 %collective-permute-start.1 = (bf16[3,64,2048]{2,1,0:T(8,128)(2,1)S(1)}, bf16[3,64,2048]{2,1,0:T(8,128)(2,1)}, u32[]{:S(2)}, u32[]{:S(2)}) collective-permute-start(bf16[3,64,2048]{2,1,0:T(8,128)(2,1)S(1)} %constant_dynamic-update-slice_fusion.w0_ref), channel_id=1, source_target_pairs={{0,2},{1,3},{2,0},{3,1},{4,6},{5,7},{6,4},{7,5},{8,10},{9,11},{10,... | collective-permute-start | bytes 2359304 | tf_op jit(solution)/shard_map/ppermute | solution.py:27
  56.9 4.1 %collective-permute-start.2 = (bf16[3,64,2048]{2,1,0:T(8,128)(2,1)S(1)}, bf16[3,64,2048]{2,1,0:T(8,128)(2,1)}, u32[]{:S(2)}, u32[]{:S(2)}) collective-permute-start(bf16[3,64,2048]{2,1,0:T(8,128)(2,1)S(1)} %constant_dynamic-update-slice_fusion.w0_ref), channel_id=1, source_target_pairs={{0,3},{1,0},{2,1},{3,2},{4,7},{5,4},{6,5},{7,6},{8,11},{9,8},{10,9... | collective-permute-start | bytes 2359304 | tf_op jit(solution)/shard_map/ppermute | solution.py:27
  61.0 2.1 %collective-permute-start.6 = (bf16[64,128]{1,0:T(8,128)(2,1)S(1)}, bf16[64,128]{1,0:T(8,128)(2,1)S(1)}, u32[]{:S(2)}, u32[]{:S(2)}) collective-permute-start(bf16[64,128]{1,0:T(8,128)(2,1)S(1)} %bitcast.45), channel_id=1, source_target_pairs={{0,256},{32,288},{64,320},{96,352},{128,384},{160,416},{192,448},{... | collective-permute-start | bytes 49160 | tf_op jit(solution)/shard_map/ppermute | solution.py:31
  63.1 9.7 %collective-permute-done.w1_ref = bf16[3,64,2048]{2,1,0:T(8,128)(2,1)S(1)} collective-permute-done((bf16[3,64,2048]{2,1,0:T(8,128)(2,1)S(1)}, bf16[3,64,2048]{2,1,0:T(8,128)(2,1)S(1)}, u32[]{:S(2)}, u32[]{:S(2)}) %collective-permute-start) | collective-permute-done | bytes 786464 | tf_op jit(solution)/shard_map/ppermute | solution.py:27
  72.8 5.1 %collective-permute-done.1.w2_ref = bf16[3,64,2048]{2,1,0:T(8,128)(2,1)} collective-permute-done((bf16[3,64,2048]{2,1,0:T(8,128)(2,1)S(1)}, bf16[3,64,2048]{2,1,0:T(8,128)(2,1)}, u32[]{:S(2)}, u32[]{:S(2)}) %collective-permute-start.1) | collective-permute-done | bytes 786464 | tf_op jit(solution)/shard_map/ppermute | solution.py:27
  77.8 14.8 %collective-permute-done.2.w3_ref = bf16[3,64,2048]{2,1,0:T(8,128)(2,1)} collective-permute-done((bf16[3,64,2048]{2,1,0:T(8,128)(2,1)S(1)}, bf16[3,64,2048]{2,1,0:T(8,128)(2,1)}, u32[]{:S(2)}, u32[]{:S(2)}) %collective-permute-start.2) | collective-permute-done | bytes 786464 | tf_op jit(solution)/shard_map/ppermute | solution.py:27
  92.6 0.0 all-to-all-done.1.got_ref
  92.6 4.4 %shard_map.172 = (bf16[16,160,128]{2,1,0:T(8,128)(2,1)}, bf16[3,160,256]{2,1,0:T(8,128)(2,1)}) custom-call(bf16[4,8,160,128]{3,2,1,0:T(8,128)(2,1)S(1)} %all-to-all-done.1.got_ref, bf16[3,64,2048]{2,1,0:T(8,128)(2,1)S(1)} %constant_dynamic-update-slice_fusion.w0_ref, bf16[3,64,2048]{2,1,0:T(8,128)(2,1)S(1)} %collective-permute-done.w1_ref, ...), custom_call_target="tpu_custom_call" | custom-call | tf_op jit(solution)/shard_map/pallas_call | solution.py:266
  97.1 6.5 %all-to-all-start.2 = ((bf16[16,160,128]{2,1,0:T(8,128)(2,1)}), bf16[16,160,128]{2,1,0:T(8,128)(2,1)S(1)}, u32[]{:S(2)}, u32[]{:S(2)}) async-start(bf16[16,160,128]{2,1,0:T(8,128)(2,1)} %get-tuple-element.25), calls=%async_computation.2 | async-start | bytes 1310720 | tf_op jit(solution)/shard_map/all_to_all | solution.py:22
  103.7 1.9 collective-permute-start.7
  105.6 8.0 %collective-permute-done.7 = bf16[2,64,128]{2,1,0:T(8,128)(2,1)S(1)} collective-permute-done((bf16[2,64,128]{2,1,0:T(8,128)(2,1)S(1)}, bf16[2,64,128]{2,1,0:T(8,128)(2,1)S(1)}, u32[]{:S(2)}, u32[]{:S(2)}) %collective-permute-start.7) | collective-permute-done | bytes 32800 | tf_op jit(solution)/shard_map/ppermute | solution.py:31
  113.6 2.1 %collective-permute-start.8 = (bf16[2,2,64,128]{3,2,0,1:T(8,128)(2,1)S(1)}, bf16[2,2,64,128]{3,2,0,1:T(8,128)(2,1)S(1)}, u32[]{:S(2)}, u32[]{:S(2)}) collective-permute-start(bf16[2,2,64,128]{3,2,0,1:T(8,128)(2,1)S(1)} %pad_maximum_fusion.3), channel_id=1, source_target_pairs={{0,64},{32,96},{64,0},{96,32},{128,192},{160,224},{192,128},{224,1... | collective-permute-start | bytes 196616 | tf_op jit(solution)/shard_map/ppermute | solution.py:31
  115.7 1.5 shard_map.174
  117.2 4.7 %all-to-all-start.3 = ((bf16[32,24,128]{2,1,0:T(8,128)(2,1)}), bf16[32,24,128]{2,1,0:T(8,128)(2,1)S(1)}, u32[]{:S(2)}, u32[]{:S(2)}) async-start(bf16[32,24,128]{2,1,0:T(8,128)(2,1)} %bitcast.43), calls=%async_computation.3 | async-start | bytes 393216 | tf_op jit(solution)/shard_map/all_to_all | solution.py:22
  122.0 2.2 %collective-permute-start.11 = (bf16[2,128]{1,0:T(2,128)(2,1)S(1)}, bf16[2,128]{1,0:T(2,128)(2,1)S(1)}, u32[]{:S(2)}, u32[]{:S(2)}) collective-permute-start(bf16[2,128]{1,0:T(2,128)(2,1)S(1)} %slice.104), channel_id=1, source_target_pairs={{0,16},{16,32},{32,48},{48,64},{64,80},{80,96},{96,112},{112,128},... | collective-permute-start | bytes 1544 | tf_op jit(solution)/shard_map/ppermute | solution.py:49
  124.2 0.1 copy.21
  124.4 3.5 %collective-permute-start.9 = (bf16[2,2,2,64,128]{4,3,0,1,2:T(8,128)(2,1)S(1)}, bf16[2,2,2,64,128]{4,3,0,1,2:T(8,128)(2,1)S(1)}, u32[]{:S(2)}, u32[]{:S(2)}) collective-permute-start(bf16[2,2,2,64,128]{4,3,0,1,2:T(8,128)(2,1)S(1)} %pad_maximum_fusion.2), channel_id=1, source_target_pairs={{0,32},{32,0},{64,96},{96,64},{128,160},{160,128},{192,224},{224,1... | collective-permute-start | bytes 393224 | tf_op jit(solution)/shard_map/ppermute | solution.py:31
  128.0 14.1 %all-to-all-done.3 = bf16[32,24,128]{2,1,0:T(8,128)(2,1)S(1)} async-done(((bf16[32,24,128]{2,1,0:T(8,128)(2,1)}), bf16[32,24,128]{2,1,0:T(8,128)(2,1)S(1)}, u32[]{:S(2)}, u32[]{:S(2)}) %all-to-all-start.3) | async-done | bytes 196640 | tf_op jit(solution)/shard_map/all_to_all | solution.py:22
  142.1 1.4 shard_map.175
  143.6 7.4 %all-to-all-start.4 = ((bf16[16,256,128]{2,1,0:T(8,128)(2,1)}), bf16[16,256,128]{2,1,0:T(8,128)(2,1)S(1)}, u32[]{:S(2)}, u32[]{:S(2)}) async-start(bf16[16,256,128]{2,1,0:T(8,128)(2,1)} %shard_map.175), calls=%async_computation.4 | async-start | bytes 2097152 | tf_op jit(solution)/shard_map/all_to_all | solution.py:22
  151.0 2.6 %shard_map.173 = (bf16[3,64,2048]{2,1,0:T(8,128)(2,1)}, bf16[3,64,2048]{2,1,0:T(8,128)(2,1)}, bf16[3,64,2048]{2,1,0:T(8,128)(2,1)}, bf16[3,64,2048]{2,1,0:T(8,128)(2,1)}) custom-call(bf16[4,8,160,128]{3,2,1,0:T(8,128)(2,1)S(1)} %all-to-all-done.1.got_ref, bf16[3,160,256]{2,1,0:T(8,128)(2,1)S(1)} %copy-done.1), custom_call_target="tpu_custom_call" | custom-call | tf_op jit(solution)/shard_map/pallas_call | solution.py:266
  153.6 3.4 %collective-permute-start.5 = (bf16[3,64,2048]{2,1,0:T(8,128)(2,1)}, bf16[3,64,2048]{2,1,0:T(8,128)(2,1)}, u32[]{:S(2)}, u32[]{:S(2)}) collective-permute-start(bf16[3,64,2048]{2,1,0:T(8,128)(2,1)} %get-tuple-element.23), channel_id=1, source_target_pairs={{0,1},{1,2},{2,3},{3,0},{4,5},{5,6},{6,7},{7,4},{8,9},{9,10},{10,1... | collective-permute-start | bytes 2359304 | tf_op jit(solution)/shard_map/ppermute | solution.py:27
  157.0 3.1 %collective-permute-start.4 = (bf16[3,64,2048]{2,1,0:T(8,128)(2,1)}, bf16[3,64,2048]{2,1,0:T(8,128)(2,1)}, u32[]{:S(2)}, u32[]{:S(2)}) collective-permute-start(bf16[3,64,2048]{2,1,0:T(8,128)(2,1)} %get-tuple-element.22), channel_id=1, source_target_pairs={{0,2},{1,3},{2,0},{3,1},{4,6},{5,7},{6,4},{7,5},{8,10},{9,11},{10,... | collective-permute-start | bytes 2359304 | tf_op jit(solution)/shard_map/ppermute | solution.py:27
  160.0 4.0 %collective-permute-start.3 = (bf16[3,64,2048]{2,1,0:T(8,128)(2,1)}, bf16[3,64,2048]{2,1,0:T(8,128)(2,1)}, u32[]{:S(2)}, u32[]{:S(2)}) collective-permute-start(bf16[3,64,2048]{2,1,0:T(8,128)(2,1)} %get-tuple-element.21), channel_id=1, source_target_pairs={{0,3},{1,0},{2,1},{3,2},{4,7},{5,4},{6,5},{7,6},{8,11},{9,8},{10,9... | collective-permute-start | bytes 2359304 | tf_op jit(solution)/shard_map/ppermute | solution.py:27
  164.1 1.9 collective-permute-start.10
  166.0 0.7 multiply_convert_fusion
  166.8 0.7 collective-permute-done.10
  167.5 0.0 copy-start
  167.6 0.1 pad_maximum_fusion
  167.7 1.1 copy-done
  168.8 2.7 %mixer.1 = (bf16[2,16,64,128]{3,2,1,0:T(8,128)(2,1)}, bf16[256,128]{1,0:T(8,128)(2,1)}, bf16[256,128]{1,0:T(8,128)(2,1)}) custom-call(bf16[16,256,128]{2,1,0:T(8,128)(2,1)S(1)} %all-to-all-done.4.full_ref, bf16[256,2048]{1,0:T(8,128)(2,1)S(1)} %copy-done, bf16[2048,128]{1,0:T(8,128)(2,1)S(1)} %bitcast.39, bf16[256,128]{1,0:T(8,128)(2,1)} %get-tuple-element.31.mixed_hbm, ...), custom_call_target="tpu_custom_call" | custom-call | tf_op jit(solution)/shard_map/mixer/pallas_call | solution.py:244
  171.5 0.0 copy-start.9
  171.5 5.4 %all_to_all.35 = bf16[2,16,64,128]{3,2,1,0:T(8,128)(2,1)S(1)} all-to-all(bf16[2,16,64,128]{3,2,1,0:T(8,128)(2,1)} %get-tuple-element.26), channel_id=1, replica_groups=mesh['z'=16,'c'=2,'y'=4,'x'=4] {'c'}, dimensions={0} | all-to-all | bytes 1048576 | tf_op jit(solution)/shard_map/all_to_all | solution.py:22
  176.9 0.8 reduce_sum.21
  177.7 11.1 %all-to-all-start.6 = ((bf16[16,64,128]{2,1,0:T(8,128)(2,1)}), bf16[16,64,128]{2,1,0:T(8,128)(2,1)S(1)}, u32[]{:S(2)}, u32[]{:S(2)}) async-start(bf16[16,64,128]{2,1,0:T(8,128)(2,1)} %reduce_sum.21), calls=%async_computation.6 | async-start | bytes 524288 | tf_op jit(solution)/shard_map/all_to_all | solution.py:22
  188.8 1.3 collective-permute-start.12
  190.1 6.6 %collective-permute-done.3 = bf16[3,64,2048]{2,1,0:T(8,128)(2,1)} collective-permute-done((bf16[3,64,2048]{2,1,0:T(8,128)(2,1)}, bf16[3,64,2048]{2,1,0:T(8,128)(2,1)}, u32[]{:S(2)}, u32[]{:S(2)}) %collective-permute-start.3) | collective-permute-done | bytes 786464 | tf_op jit(solution)/shard_map/ppermute | solution.py:27
  196.8 2.8 %add_convert_fusion = (bf16[1,64,2048]{2,1,0:T(8,128)(2,1)}, bf16[1,64,2048]{2,1,0:T(8,128)(2,1)}, bf16[1,64,2048]{2,1,0:T(8,128)(2,1)}) fusion(bf16[3,64,2048]{2,1,0:T(8,128)(2,1)} %collective-permute-done.5, bf16[3,64,2048]{2,1,0:T(8,128)(2,1)} %collective-permute-done.4, bf16[3,64,2048]{2,1,0:T(8,128)(2,1)} %collective-permute-done.3, ...), kind=kLoop, calls=%fused_computation.2 | loop fusion | flops 3145728 | bytes 3932160 | tf_op jit(solution)/shard_map/convert_element_type | solution.py:339
  199.6 0.7 fusion
  200.3 0.6 fusion.2
  200.9 6.7 %all-to-all-done.6 = bf16[16,64,128]{2,1,0:T(8,128)(2,1)S(1)} async-done(((bf16[16,64,128]{2,1,0:T(8,128)(2,1)}), bf16[16,64,128]{2,1,0:T(8,128)(2,1)S(1)}, u32[]{:S(2)}, u32[]{:S(2)}) %all-to-all-start.6) | async-done | bytes 262176 | tf_op jit(solution)/shard_map/all_to_all | solution.py:22
  207.7 0.7 convert_reduce_fusion
  (51 shorter events, 0.4 us)
Async XLA Ops:
  0.6 17.8 %copy-start.5 = (bf16[1,64,2048]{2,1,0:T(8,128)(2,1)S(1)}, bf16[1,64,2048]{2,1,0:T(8,128)(2,1)}, u32[]{:S(2)}) copy-start(bf16[1,64,2048]{2,1,0:T(8,128)(2,1)} %param.16) | copy-start | bytes 786436
  0.6 17.8 %copy-start.6 = (bf16[1,64,2048]{2,1,0:T(8,128)(2,1)S(1)}, bf16[1,64,2048]{2,1,0:T(8,128)(2,1)}, u32[]{:S(2)}) copy-start(bf16[1,64,2048]{2,1,0:T(8,128)(2,1)} %param.17) | copy-start | bytes 786436
  3.0 41.0 %all-to-all-start = ((bf16[32,40,128]{2,1,0:T(8,128)(2,1)}), bf16[32,40,128]{2,1,0:T(8,128)(2,1)S(1)}, u32[]{:S(2)}, u32[]{:S(2)}) async-start(bf16[32,40,128]{2,1,0:T(8,128)(2,1)} %bitcast.44), calls=%async_computation | async-start | bytes 655360 | tf_op jit(solution)/shard_map/all_to_all | solution.py:22
  45.4 5.1 %copy-start.7 = (bf16[1,64,2048]{2,1,0:T(8,128)(2,1)S(1)}, bf16[1,64,2048]{2,1,0:T(8,128)(2,1)}, u32[]{:S(2)}) copy-start(bf16[1,64,2048]{2,1,0:T(8,128)(2,1)} %param.18) | copy-start | bytes 786436
  45.4 15.6 %copy-start.10 = (bf16[128,64]{0,1:T(8,128)(2,1)S(1)}, bf16[128,64]{0,1:T(8,128)(2,1)}, u32[]{:S(2)}) copy-start(bf16[128,64]{0,1:T(8,128)(2,1)} %param.23) | copy-start | bytes 49156
  45.4 47.2 %all-to-all-start.1 = ((bf16[4,8,160,128]{3,2,1,0:T(8,128)(2,1)}), bf16[4,8,160,128]{3,2,1,0:T(8,128)(2,1)S(1)}, u32[]{:S(2)}, u32[]{:S(2)}) async-start(bf16[4,8,160,128]{3,2,1,0:T(8,128)(2,1)} %shard_map.171), calls=%async_computation.1 | async-start | bytes 2621440 | tf_op jit(solution)/shard_map/all_to_all | solution.py:22
  50.5 22.3 %collective-permute-start = (bf16[3,64,2048]{2,1,0:T(8,128)(2,1)S(1)}, bf16[3,64,2048]{2,1,0:T(8,128)(2,1)S(1)}, u32[]{:S(2)}, u32[]{:S(2)}) collective-permute-start(bf16[3,64,2048]{2,1,0:T(8,128)(2,1)S(1)} %constant_dynamic-update-slice_fusion.w0_ref), channel_id=1, source_target_pairs={{0,1},{1,2},{2,3},{3,0},{4,5},{5,6},{6,7},{7,4},{8,9},{9,10},{10,1... | collective-permute-start | bytes 2359304 | tf_op jit(solution)/shard_map/ppermute | solution.py:27
  53.9 24.0 %collective-permute-start.1 = (bf16[3,64,2048]{2,1,0:T(8,128)(2,1)S(1)}, bf16[3,64,2048]{2,1,0:T(8,128)(2,1)}, u32[]{:S(2)}, u32[]{:S(2)}) collective-permute-start(bf16[3,64,2048]{2,1,0:T(8,128)(2,1)S(1)} %constant_dynamic-update-slice_fusion.w0_ref), channel_id=1, source_target_pairs={{0,2},{1,3},{2,0},{3,1},{4,6},{5,7},{6,4},{7,5},{8,10},{9,11},{10,... | collective-permute-start | bytes 2359304 | tf_op jit(solution)/shard_map/ppermute | solution.py:27
  56.9 35.7 %collective-permute-start.2 = (bf16[3,64,2048]{2,1,0:T(8,128)(2,1)S(1)}, bf16[3,64,2048]{2,1,0:T(8,128)(2,1)}, u32[]{:S(2)}, u32[]{:S(2)}) collective-permute-start(bf16[3,64,2048]{2,1,0:T(8,128)(2,1)S(1)} %constant_dynamic-update-slice_fusion.w0_ref), channel_id=1, source_target_pairs={{0,3},{1,0},{2,1},{3,2},{4,7},{5,4},{6,5},{7,6},{8,11},{9,8},{10,9... | collective-permute-start | bytes 2359304 | tf_op jit(solution)/shard_map/ppermute | solution.py:27
  61.0 42.6 %collective-permute-start.6 = (bf16[64,128]{1,0:T(8,128)(2,1)S(1)}, bf16[64,128]{1,0:T(8,128)(2,1)S(1)}, u32[]{:S(2)}, u32[]{:S(2)}) collective-permute-start(bf16[64,128]{1,0:T(8,128)(2,1)S(1)} %bitcast.45), channel_id=1, source_target_pairs={{0,256},{32,288},{64,320},{96,352},{128,384},{160,416},{192,448},{... | collective-permute-start | bytes 49160 | tf_op jit(solution)/shard_map/ppermute | solution.py:31
  97.1 24.9 %copy-start.4 = (bf16[256,128]{1,0:T(8,128)(2,1)S(1)}, bf16[256,128]{1,0:T(8,128)(2,1)}, u32[]{:S(2)}) copy-start(bf16[256,128]{1,0:T(8,128)(2,1)} %param.20) | copy-start | bytes 196612
  97.1 24.9 %copy-start.8 = (bf16[256,128]{1,0:T(8,128)(2,1)S(1)}, bf16[256,128]{1,0:T(8,128)(2,1)}, u32[]{:S(2)}) copy-start(bf16[256,128]{1,0:T(8,128)(2,1)} %param.21) | copy-start | bytes 196612
  97.1 27.1 %copy-start.11 = (s32[2,256]{1,0:T(2,128)S(1)}, s32[2,256]{1,0:T(2,128)}, u32[]{:S(2)}) copy-start(s32[2,256]{1,0:T(2,128)} %get-tuple-element.24) | copy-start | bytes 6148
  97.1 18.6 %all-to-all-start.2 = ((bf16[16,160,128]{2,1,0:T(8,128)(2,1)}), bf16[16,160,128]{2,1,0:T(8,128)(2,1)S(1)}, u32[]{:S(2)}, u32[]{:S(2)}) async-start(bf16[16,160,128]{2,1,0:T(8,128)(2,1)} %get-tuple-element.25), calls=%async_computation.2 | async-start | bytes 1310720 | tf_op jit(solution)/shard_map/all_to_all | solution.py:22
  103.6 24.4 %copy-start.12 = (f32[3,128]{1,0:T(4,128)S(1)}, f32[3,128]{1,0:T(4,128)}, u32[]{:S(2)}) copy-start(f32[3,128]{1,0:T(4,128)} %param.22) | copy-start | bytes 4612
  103.7 9.9 %collective-permute-start.7 = (bf16[2,64,128]{2,1,0:T(8,128)(2,1)S(1)}, bf16[2,64,128]{2,1,0:T(8,128)(2,1)S(1)}, u32[]{:S(2)}, u32[]{:S(2)}) collective-permute-start(bf16[2,64,128]{2,1,0:T(8,128)(2,1)S(1)} %pad_maximum_fusion.4), channel_id=1, source_target_pairs={{0,128},{32,160},{64,192},{96,224},{128,0},{160,32},{192,64},{224,... | collective-permute-start | bytes 98312 | tf_op jit(solution)/shard_map/ppermute | solution.py:31
  113.6 10.8 %collective-permute-start.8 = (bf16[2,2,64,128]{3,2,0,1:T(8,128)(2,1)S(1)}, bf16[2,2,64,128]{3,2,0,1:T(8,128)(2,1)S(1)}, u32[]{:S(2)}, u32[]{:S(2)}) collective-permute-start(bf16[2,2,64,128]{3,2,0,1:T(8,128)(2,1)S(1)} %pad_maximum_fusion.3), channel_id=1, source_target_pairs={{0,64},{32,96},{64,0},{96,32},{128,192},{160,224},{192,128},{224,1... | collective-permute-start | bytes 196616 | tf_op jit(solution)/shard_map/ppermute | solution.py:31
  117.2 24.9 %all-to-all-start.3 = ((bf16[32,24,128]{2,1,0:T(8,128)(2,1)}), bf16[32,24,128]{2,1,0:T(8,128)(2,1)S(1)}, u32[]{:S(2)}, u32[]{:S(2)}) async-start(bf16[32,24,128]{2,1,0:T(8,128)(2,1)} %bitcast.43), calls=%async_computation.3 | async-start | bytes 393216 | tf_op jit(solution)/shard_map/all_to_all | solution.py:22
  122.0 44.0 %collective-permute-start.11 = (bf16[2,128]{1,0:T(2,128)(2,1)S(1)}, bf16[2,128]{1,0:T(2,128)(2,1)S(1)}, u32[]{:S(2)}, u32[]{:S(2)}) collective-permute-start(bf16[2,128]{1,0:T(2,128)(2,1)S(1)} %slice.104), channel_id=1, source_target_pairs={{0,16},{16,32},{32,48},{48,64},{64,80},{80,96},{96,112},{112,128},... | collective-permute-start | bytes 1544 | tf_op jit(solution)/shard_map/ppermute | solution.py:49
  124.4 26.5 %collective-permute-start.9 = (bf16[2,2,2,64,128]{4,3,0,1,2:T(8,128)(2,1)S(1)}, bf16[2,2,2,64,128]{4,3,0,1,2:T(8,128)(2,1)S(1)}, u32[]{:S(2)}, u32[]{:S(2)}) collective-permute-start(bf16[2,2,2,64,128]{4,3,0,1,2:T(8,128)(2,1)S(1)} %pad_maximum_fusion.2), channel_id=1, source_target_pairs={{0,32},{32,0},{64,96},{96,64},{128,160},{160,128},{192,224},{224,1... | collective-permute-start | bytes 393224 | tf_op jit(solution)/shard_map/ppermute | solution.py:31
  143.6 7.4 %copy-start.1 = (bf16[3,160,256]{2,1,0:T(8,128)(2,1)S(1)}, bf16[3,160,256]{2,1,0:T(8,128)(2,1)}, u32[]{:S(2)}) copy-start(bf16[3,160,256]{2,1,0:T(8,128)(2,1)} %get-tuple-element.19.cots_ref) | copy-start | bytes 737284
  143.6 24.1 %all-to-all-start.4 = ((bf16[16,256,128]{2,1,0:T(8,128)(2,1)}), bf16[16,256,128]{2,1,0:T(8,128)(2,1)S(1)}, u32[]{:S(2)}, u32[]{:S(2)}) async-start(bf16[16,256,128]{2,1,0:T(8,128)(2,1)} %shard_map.175), calls=%async_computation.4 | async-start | bytes 2097152 | tf_op jit(solution)/shard_map/all_to_all | solution.py:22
  150.9 15.1 %copy-start.3 = (bf16[256,128]{1,0:T(8,128)(2,1)S(1)}, bf16[256,128]{1,0:T(8,128)(2,1)}, u32[]{:S(2)}) copy-start(bf16[256,128]{1,0:T(8,128)(2,1)} %outer_hbm.1) | copy-start | bytes 196612
  153.6 36.5 %collective-permute-start.5 = (bf16[3,64,2048]{2,1,0:T(8,128)(2,1)}, bf16[3,64,2048]{2,1,0:T(8,128)(2,1)}, u32[]{:S(2)}, u32[]{:S(2)}) collective-permute-start(bf16[3,64,2048]{2,1,0:T(8,128)(2,1)} %get-tuple-element.23), channel_id=1, source_target_pairs={{0,1},{1,2},{2,3},{3,0},{4,5},{5,6},{6,7},{7,4},{8,9},{9,10},{10,1... | collective-permute-start | bytes 2359304 | tf_op jit(solution)/shard_map/ppermute | solution.py:27
  157.0 33.1 %collective-permute-start.4 = (bf16[3,64,2048]{2,1,0:T(8,128)(2,1)}, bf16[3,64,2048]{2,1,0:T(8,128)(2,1)}, u32[]{:S(2)}, u32[]{:S(2)}) collective-permute-start(bf16[3,64,2048]{2,1,0:T(8,128)(2,1)} %get-tuple-element.22), channel_id=1, source_target_pairs={{0,2},{1,3},{2,0},{3,1},{4,6},{5,7},{6,4},{7,5},{8,10},{9,11},{10,... | collective-permute-start | bytes 2359304 | tf_op jit(solution)/shard_map/ppermute | solution.py:27
  160.0 36.7 %collective-permute-start.3 = (bf16[3,64,2048]{2,1,0:T(8,128)(2,1)}, bf16[3,64,2048]{2,1,0:T(8,128)(2,1)}, u32[]{:S(2)}, u32[]{:S(2)}) collective-permute-start(bf16[3,64,2048]{2,1,0:T(8,128)(2,1)} %get-tuple-element.21), channel_id=1, source_target_pairs={{0,3},{1,0},{2,1},{3,2},{4,7},{5,4},{6,5},{7,6},{8,11},{9,8},{10,9... | collective-permute-start | bytes 2359304 | tf_op jit(solution)/shard_map/ppermute | solution.py:27
  164.1 3.4 %collective-permute-start.10 = (bf16[2,2,2,2,64,128]{5,4,0,1,2,3:T(8,128)(2,1)S(1)}, bf16[2,2,2,2,64,128]{5,4,0,1,2,3:T(8,128)(2,1)S(1)}, u32[]{:S(2)}, u32[]{:S(2)}) collective-permute-start(bf16[2,2,2,2,64,128]{5,4,0,1,2,3:T(8,128)(2,1)S(1)} %pad_maximum_fusion.1), channel_id=1, source_target_pairs={{0,16},{16,0},{1,17},{17,1},{2,18},{18,2},{3,19},{19,3},{4,20},{20... | collective-permute-start | bytes 786440 | tf_op jit(solution)/shard_map/ppermute | solution.py:31
  167.5 1.2 copy-start
  171.5 17.3 %copy-start.9 = (bf16[256,128]{1,0:T(8,128)(2,1)S(1)}, bf16[256,128]{1,0:T(8,128)(2,1)}, u32[]{:S(2)}) copy-start(bf16[256,128]{1,0:T(8,128)(2,1)} %get-tuple-element.28) | copy-start | bytes 196612
  171.5 25.3 %copy-start.2 = (bf16[3,64,2048]{2,1,0:T(8,128)(2,1)S(1)}, bf16[3,64,2048]{2,1,0:T(8,128)(2,1)}, u32[]{:S(2)}) copy-start(bf16[3,64,2048]{2,1,0:T(8,128)(2,1)} %get-tuple-element.20) | copy-start | bytes 2359300
  177.7 30.0 %all-to-all-start.6 = ((bf16[16,64,128]{2,1,0:T(8,128)(2,1)}), bf16[16,64,128]{2,1,0:T(8,128)(2,1)S(1)}, u32[]{:S(2)}, u32[]{:S(2)}) async-start(bf16[16,64,128]{2,1,0:T(8,128)(2,1)} %reduce_sum.21), calls=%async_computation.6 | async-start | bytes 524288 | tf_op jit(solution)/shard_map/all_to_all | solution.py:22
  188.8 10.8 %collective-permute-start.12 = (bf16[2,128]{1,0:T(2,128)(2,1)S(1)}, bf16[2,128]{1,0:T(2,128)(2,1)S(1)}, u32[]{:S(2)}, u32[]{:S(2)}) collective-permute-start(bf16[2,128]{1,0:T(2,128)(2,1)S(1)} %slice.91), channel_id=1, source_target_pairs={{16,0},{32,16},{48,32},{64,48},{80,64},{96,80},{112,96},{128,112},... | collective-permute-start | bytes 1544 | tf_op jit(solution)/shard_map/ppermute | solution.py:49

commit v5 on v4

--- a/solution.py
+++ b/solution.py
@@ -27,20 +27,20 @@
     return lax.ppermute(value, axis, [(i, (i + by) % count) for i in range(count)])
 
 
-def mirrored(value, axis, bit):
-    return lax.ppermute(value, axis, [(i, i ^ bit) for i in range(lax.axis_size(axis))])
-
-
-def doubled(value, axis):
-    index = lax.axis_index(axis)
-    bit = lax.axis_size(axis) // 2
-    while bit:
-        other = mirrored(value, axis, bit)
-        high = (index & bit) > 0
-        both = (jnp.where(high, other, value), jnp.where(high, value, other))
-        value = jnp.stack(both, axis=value.ndim - 2)
-        bit //= 2
-    return value
+def shifted(value, axis, group, stride, by):
+    count = lax.axis_size(axis)
+    size = group * stride
+
+    def source(i):
+        return i // size * size + (i + by * stride) % size
+
+    return lax.ppermute(value, axis, [(source(i), i) for i in range(count)])
+
+
+def grouped(value, axis, group, stride):
+    others = [shifted(value, axis, group, stride, by) for by in range(1, group)]
+    place = lax.rem(lax.div(lax.axis_index(axis), jnp.int32(stride)), jnp.int32(group))
+    return ordered([value, *others], place)
 
 
 def from_behind(value, axis, by):
@@ -232,6 +232,44 @@
     keep.wait()
 
 
+def order_kernel(place_ref, *refs):
+    *parts, out_ref = refs
+    for by, ref in enumerate(parts):
+        at = place_ref[0] + by
+        out_ref[jnp.where(at >= len(parts), at - len(parts), at)] = ref[...]
+
+
+def ordered(parts, place):
+    return pl.pallas_call(
+        order_kernel,
+        in_specs=[pl.BlockSpec(memory_space=pltpu.SMEM)]
+        + [pl.BlockSpec(memory_space=pltpu.VMEM)] * len(parts),
+        out_shape=jax.ShapeDtypeStruct((len(parts), *parts[0].shape), parts[0].dtype),
+        compiler_params=pltpu.CompilerParams(vmem_limit_bytes=4 << 20),
+    )(place[None], *parts)
+
+
+def twin_kernel(place_ref, own_ref, other_ref, out_ref):
+    near, far = own_ref.shape[:2]
+    mine = place_ref[0]
+    for f in range(far):
+        for n in range(near):
+            out_ref[f * near + n, mine] = own_ref[n, f]
+            out_ref[f * near + n, 1 - mine] = other_ref[n, f]
+
+
+def with_twin(own, other, place):
+    near, far, *block = own.shape
+    return pl.pallas_call(
+        twin_kernel,
+        in_specs=[pl.BlockSpec(memory_space=pltpu.SMEM)]
+        + [pl.BlockSpec(memory_space=pltpu.VMEM)] * 2,
+        out_shape=jax.ShapeDtypeStruct((far * near, 2, *block), own.dtype),
+        compiler_params=pltpu.CompilerParams(vmem_limit_bytes=4 << 20),
+        name="twins",
+    )(place[None], own, other)
+
+
 def in_hbm(value):
     return pltpu.with_memory_space_constraint(value, pltpu.HBM)
 
@@ -351,7 +389,11 @@
         convolved = convolved + conv_taps[tap][None, :] * extended[tap : tap + tokens]
     mixed = (outer_gate.astype(F32) * convolved).astype(BF)
 
-    proj = doubled(doubled(out_proj.T, "z"), "c").reshape(width, wdev)
+    inner = 4
+    proj = grouped(out_proj.T, "z", n_z // inner, inner)
+    proj = grouped(proj, "z", inner, 1)
+    twin = shifted(proj, "c", n_c, 1, 1)
+    proj = with_twin(proj, twin, lax.axis_index("c")).reshape(width, wdev)
     pair, conv_cot, outer_gate_grad = mix(
         full, out_grad, proj, mixed, convolved, outer_gate, n_c, n_z
     )

time: 210 us -> 236 us (1.12)
  the two profiles are of different devices: /device:TPU:10 before, /device:TPU:1 now
where the time goes in v5:
time: 236 us; the launch traced here: 231 us
  starting transfers between devices  91.8 us (39%)
  waiting for transfers between devices  88 us (37%)
  blocking collectives  24.6 us (10%)
  Pallas kernels  15.1 us (6%)
  other arithmetic  6.44 us (3%)
  local copies, waits for them, and re-layouts  4.33 us (2%)
    all_to_all x5, waiting for transfers between devices, swap(): return lax.all_to_all(blocks, axis, split_axis=0, concat_axis=0, tiled=True)  43.7 us
    all_to_all x5, starting transfers between devices, swap(): return lax.all_to_all(blocks, axis, split_axis=0, concat_axis=0, tiled=True)  37.6 us
    ppermute x6, waiting for transfers between devices, turned(): lax.ppermute(value, axis, [(i, (i + by) % count) for i in range(count)])  29.4 us
    all_to_all x2, blocking collectives, swap(): return lax.all_to_all(blocks, axis, split_axis=0, concat_axis=0, tiled=True)  24.6 us
    ppermute x7, starting transfers between devices, shifted(): return lax.ppermute(value, axis, [(source(i), i) for i in range(count)])  23.6 us
    ppermute x6, starting transfers between devices, turned(): lax.ppermute(value, axis, [(i, (i + by) % count) for i in range(count)])  21.2 us
    pallas_call x5, Pallas kernels, on_core(): pl.pallas_call(functools.partial(kernel, **static) if static else kernel,...  10 us
    ppermute x2, starting transfers between devices, from_behind(): return lax.ppermute(value, axis, pairs)  9.41 us
  transfers between devices with their start and end apart: 20, of which 10 were waited for; matrix products, arithmetic and copies ran while one was open for 3% of the time, Pallas kernels for 2%

profile of v5, /device:TPU:1, one launch (start us, length us, event | category | flops | bytes accessed | tf_op | source)
XLA Modules:
  0.0 231.4 jit_solution(11511342688438980183)
XLA Ops:
  0.7 2.3 route.1
  3.0 16.7 %all-to-all-start = ((bf16[32,40,128]{2,1,0:T(8,128)(2,1)}), bf16[32,40,128]{2,1,0:T(8,128)(2,1)S(1)}, u32[]{:S(2)}, u32[]{:S(2)}) async-start(bf16[32,40,128]{2,1,0:T(8,128)(2,1)} %bitcast.29), calls=%async_computation | async-start | bytes 655360 | tf_op jit(solution)/shard_map/all_to_all | solution.py:22
  19.8 24.9 %all-to-all-done = bf16[32,40,128]{2,1,0:T(8,128)(2,1)S(1)} async-done(((bf16[32,40,128]{2,1,0:T(8,128)(2,1)}), bf16[32,40,128]{2,1,0:T(8,128)(2,1)S(1)}, u32[]{:S(2)}, u32[]{:S(2)}) %all-to-all-start) | async-done | bytes 327712 | tf_op jit(solution)/shard_map/all_to_all | solution.py:22
  44.7 1.5 shard_map.171
  46.2 4.3 %all-to-all-start.1 = ((bf16[4,8,160,128]{3,2,1,0:T(8,128)(2,1)}), bf16[4,8,160,128]{3,2,1,0:T(8,128)(2,1)S(1)}, u32[]{:S(2)}, u32[]{:S(2)}) async-start(bf16[4,8,160,128]{3,2,1,0:T(8,128)(2,1)} %shard_map.171), calls=%async_computation.1 | async-start | bytes 2621440 | tf_op jit(solution)/shard_map/all_to_all | solution.py:22
  50.5 3.1 %collective-permute-start = (bf16[3,64,2048]{2,1,0:T(8,128)(2,1)S(1)}, bf16[3,64,2048]{2,1,0:T(8,128)(2,1)S(1)}, u32[]{:S(2)}, u32[]{:S(2)}) collective-permute-start(bf16[3,64,2048]{2,1,0:T(8,128)(2,1)S(1)} %constant_dynamic-update-slice_fusion.w0_ref), channel_id=1, source_target_pairs={{0,1},{1,2},{2,3},{3,0},{4,5},{5,6},{6,7},{7,4},{8,9},{9,10},{10,1... | collective-permute-start | bytes 2359304 | tf_op jit(solution)/shard_map/ppermute | solution.py:27
  53.6 4.4 %collective-permute-start.1 = (bf16[3,64,2048]{2,1,0:T(8,128)(2,1)S(1)}, bf16[3,64,2048]{2,1,0:T(8,128)(2,1)S(1)}, u32[]{:S(2)}, u32[]{:S(2)}) collective-permute-start(bf16[3,64,2048]{2,1,0:T(8,128)(2,1)S(1)} %constant_dynamic-update-slice_fusion.w0_ref), channel_id=1, source_target_pairs={{0,2},{1,3},{2,0},{3,1},{4,6},{5,7},{6,4},{7,5},{8,10},{9,11},{10,... | collective-permute-start | bytes 2359304 | tf_op jit(solution)/shard_map/ppermute | solution.py:27
  58.0 3.1 %collective-permute-start.2 = (bf16[3,64,2048]{2,1,0:T(8,128)(2,1)S(1)}, bf16[3,64,2048]{2,1,0:T(8,128)(2,1)S(1)}, u32[]{:S(2)}, u32[]{:S(2)}) collective-permute-start(bf16[3,64,2048]{2,1,0:T(8,128)(2,1)S(1)} %constant_dynamic-update-slice_fusion.w0_ref), channel_id=1, source_target_pairs={{0,3},{1,0},{2,1},{3,2},{4,7},{5,4},{6,5},{7,6},{8,11},{9,8},{10,9... | collective-permute-start | bytes 2359304 | tf_op jit(solution)/shard_map/ppermute | solution.py:27
  61.1 10.7 %collective-permute-done.w1_ref = bf16[3,64,2048]{2,1,0:T(8,128)(2,1)S(1)} collective-permute-done((bf16[3,64,2048]{2,1,0:T(8,128)(2,1)S(1)}, bf16[3,64,2048]{2,1,0:T(8,128)(2,1)S(1)}, u32[]{:S(2)}, u32[]{:S(2)}) %collective-permute-start) | collective-permute-done | bytes 786464 | tf_op jit(solution)/shard_map/ppermute | solution.py:27
  71.7 17.8 %collective-permute-done.1.w2_ref = bf16[3,64,2048]{2,1,0:T(8,128)(2,1)S(1)} collective-permute-done((bf16[3,64,2048]{2,1,0:T(8,128)(2,1)S(1)}, bf16[3,64,2048]{2,1,0:T(8,128)(2,1)S(1)}, u32[]{:S(2)}, u32[]{:S(2)}) %collective-permute-start.1) | collective-permute-done | bytes 786464 | tf_op jit(solution)/shard_map/ppermute | solution.py:27
  89.6 0.9 copy-done.1
  90.5 0.9 collective-permute-done.2.w3_ref
  91.4 0.9 copy-done.3
  92.3 1.1 copy-done.2
  93.4 1.1 copy-done.4
  94.6 3.1 %shard_map.172 = (bf16[16,160,128]{2,1,0:T(8,128)(2,1)}, bf16[3,160,256]{2,1,0:T(8,128)(2,1)}) custom-call(bf16[4,8,160,128]{3,2,1,0:T(8,128)(2,1)S(1)} %all-to-all-done.1.got_ref, bf16[3,64,2048]{2,1,0:T(8,128)(2,1)S(1)} %constant_dynamic-update-slice_fusion.w0_ref, bf16[3,64,2048]{2,1,0:T(8,128)(2,1)S(1)} %collective-permute-done.w1_ref, ...), custom_call_target="tpu_custom_call" | custom-call | tf_op jit(solution)/shard_map/pallas_call | solution.py:304
  97.7 19.2 %all_to_all.35.part_ref = bf16[16,160,128]{2,1,0:T(8,128)(2,1)S(1)} all-to-all(bf16[16,160,128]{2,1,0:T(8,128)(2,1)} %get-tuple-element.25), channel_id=1, replica_groups=mesh['z'=16,'c'=2,'y'=4,'x'=4] {'y','x'}, dimensions={0} | all-to-all | bytes 1310720 | tf_op jit(solution)/shard_map/all_to_all | solution.py:22
  116.9 1.5 shard_map.174
  118.4 5.8 %all-to-all-start.3 = ((bf16[32,24,128]{2,1,0:T(8,128)(2,1)}), bf16[32,24,128]{2,1,0:T(8,128)(2,1)S(1)}, u32[]{:S(2)}, u32[]{:S(2)}) async-start(bf16[32,24,128]{2,1,0:T(8,128)(2,1)} %bitcast.28), calls=%async_computation.3 | async-start | bytes 393216 | tf_op jit(solution)/shard_map/all_to_all | solution.py:22
  124.3 18.8 %all-to-all-done.3 = bf16[32,24,128]{2,1,0:T(8,128)(2,1)S(1)} async-done(((bf16[32,24,128]{2,1,0:T(8,128)(2,1)}), bf16[32,24,128]{2,1,0:T(8,128)(2,1)S(1)}, u32[]{:S(2)}, u32[]{:S(2)}) %all-to-all-start.3) | async-done | bytes 196640 | tf_op jit(solution)/shard_map/all_to_all | solution.py:22
  143.1 1.4 shard_map.175
  144.5 3.8 %all-to-all-start.4 = ((bf16[16,256,128]{2,1,0:T(8,128)(2,1)}), bf16[16,256,128]{2,1,0:T(8,128)(2,1)S(1)}, u32[]{:S(2)}, u32[]{:S(2)}) async-start(bf16[16,256,128]{2,1,0:T(8,128)(2,1)} %shard_map.175), calls=%async_computation.4 | async-start | bytes 2097152 | tf_op jit(solution)/shard_map/all_to_all | solution.py:22
  148.4 2.5 %collective-permute-start.6 = (bf16[64,128]{1,0:T(8,128)(2,1)S(1)}, bf16[64,128]{1,0:T(8,128)(2,1)S(1)}, u32[]{:S(2)}, u32[]{:S(2)}) collective-permute-start(bf16[64,128]{1,0:T(8,128)(2,1)S(1)} %bitcast.24), channel_id=1, source_target_pairs={{128,0},{160,32},{192,64},{224,96},{256,128},{288,160},{320,192},{... | collective-permute-start | bytes 49160 | tf_op jit(solution)/shard_map/ppermute | solution.py:37
  150.9 7.5 %collective-permute-start.7 = (bf16[64,128]{1,0:T(8,128)(2,1)S(1)}, bf16[64,128]{1,0:T(8,128)(2,1)S(1)}, u32[]{:S(2)}, u32[]{:S(2)}) collective-permute-start(bf16[64,128]{1,0:T(8,128)(2,1)S(1)} %bitcast.25), channel_id=1, source_target_pairs={{256,0},{288,32},{320,64},{352,96},{384,128},{416,160},{448,192},{... | collective-permute-start | bytes 49160 | tf_op jit(solution)/shard_map/ppermute | solution.py:37
  158.4 2.1 collective-permute-start.8
  160.6 3.7 %collective-permute-done.7.refs_2_ = bf16[64,128]{1,0:T(8,128)(2,1)S(1)} collective-permute-done((bf16[64,128]{1,0:T(8,128)(2,1)S(1)}, bf16[64,128]{1,0:T(8,128)(2,1)S(1)}, u32[]{:S(2)}, u32[]{:S(2)}) %collective-permute-start.7) | collective-permute-done | bytes 16416 | tf_op jit(solution)/shard_map/ppermute | solution.py:37
  164.3 2.5 %collective-permute-done.8.refs_3_ = bf16[64,128]{1,0:T(8,128)(2,1)S(1)} collective-permute-done((bf16[64,128]{1,0:T(8,128)(2,1)S(1)}, bf16[64,128]{1,0:T(8,128)(2,1)S(1)}, u32[]{:S(2)}, u32[]{:S(2)}) %collective-permute-start.8) | collective-permute-done | bytes 16416 | tf_op jit(solution)/shard_map/ppermute | solution.py:37
  166.8 2.4 %collective-permute-start.9 = (bf16[4,64,128]{2,1,0:T(8,128)(2,1)S(1)}, bf16[4,64,128]{2,1,0:T(8,128)(2,1)S(1)}, u32[]{:S(2)}, u32[]{:S(2)}) collective-permute-start(bf16[4,64,128]{2,1,0:T(8,128)(2,1)S(1)} %shard_map.176.refs_0_), channel_id=1, source_target_pairs={{32,0},{64,32},{96,64},{0,96},{160,128},{192,160},{224,192},{128,2... | collective-permute-start | bytes 196616 | tf_op jit(solution)/shard_map/ppermute | solution.py:37
  169.3 2.6 %shard_map.173 = (bf16[3,64,2048]{2,1,0:T(8,128)(2,1)}, bf16[3,64,2048]{2,1,0:T(8,128)(2,1)}, bf16[3,64,2048]{2,1,0:T(8,128)(2,1)}, bf16[3,64,2048]{2,1,0:T(8,128)(2,1)}) custom-call(bf16[4,8,160,128]{3,2,1,0:T(8,128)(2,1)S(1)} %all-to-all-done.1.got_ref, bf16[3,160,256]{2,1,0:T(8,128)(2,1)S(1)} %copy-done.5), custom_call_target="tpu_custom_call" | custom-call | tf_op jit(solution)/shard_map/pallas_call | solution.py:304
  171.9 3.1 %collective-permute-start.5 = (bf16[3,64,2048]{2,1,0:T(8,128)(2,1)}, bf16[3,64,2048]{2,1,0:T(8,128)(2,1)}, u32[]{:S(2)}, u32[]{:S(2)}) collective-permute-start(bf16[3,64,2048]{2,1,0:T(8,128)(2,1)} %get-tuple-element.23), channel_id=1, source_target_pairs={{0,1},{1,2},{2,3},{3,0},{4,5},{5,6},{6,7},{7,4},{8,9},{9,10},{10,1... | collective-permute-start | bytes 2359304 | tf_op jit(solution)/shard_map/ppermute | solution.py:27
  175.0 4.3 %collective-permute-start.4 = (bf16[3,64,2048]{2,1,0:T(8,128)(2,1)}, bf16[3,64,2048]{2,1,0:T(8,128)(2,1)}, u32[]{:S(2)}, u32[]{:S(2)}) collective-permute-start(bf16[3,64,2048]{2,1,0:T(8,128)(2,1)} %get-tuple-element.22), channel_id=1, source_target_pairs={{0,2},{1,3},{2,0},{3,1},{4,6},{5,7},{6,4},{7,5},{8,10},{9,11},{10,... | collective-permute-start | bytes 2359304 | tf_op jit(solution)/shard_map/ppermute | solution.py:27
  179.3 3.2 %collective-permute-start.3 = (bf16[3,64,2048]{2,1,0:T(8,128)(2,1)}, bf16[3,64,2048]{2,1,0:T(8,128)(2,1)}, u32[]{:S(2)}, u32[]{:S(2)}) collective-permute-start(bf16[3,64,2048]{2,1,0:T(8,128)(2,1)} %get-tuple-element.21), channel_id=1, source_target_pairs={{0,3},{1,0},{2,1},{3,2},{4,7},{5,4},{6,5},{7,6},{8,11},{9,8},{10,9... | collective-permute-start | bytes 2359304 | tf_op jit(solution)/shard_map/ppermute | solution.py:27
  182.6 2.8 %collective-permute-start.10 = (bf16[4,64,128]{2,1,0:T(8,128)(2,1)S(1)}, bf16[4,64,128]{2,1,0:T(8,128)(2,1)S(1)}, u32[]{:S(2)}, u32[]{:S(2)}) collective-permute-start(bf16[4,64,128]{2,1,0:T(8,128)(2,1)S(1)} %shard_map.176.refs_0_), channel_id=1, source_target_pairs={{64,0},{96,32},{0,64},{32,96},{192,128},{224,160},{128,192},{160,2... | collective-permute-start | bytes 196616 | tf_op jit(solution)/shard_map/ppermute | solution.py:37
  185.4 2.6 %collective-permute-start.11 = (bf16[4,64,128]{2,1,0:T(8,128)(2,1)S(1)}, bf16[4,64,128]{2,1,0:T(8,128)(2,1)S(1)}, u32[]{:S(2)}, u32[]{:S(2)}) collective-permute-start(bf16[4,64,128]{2,1,0:T(8,128)(2,1)S(1)} %shard_map.176.refs_0_), channel_id=1, source_target_pairs={{96,0},{0,32},{32,64},{64,96},{224,128},{128,160},{160,192},{192,2... | collective-permute-start | bytes 196616 | tf_op jit(solution)/shard_map/ppermute | solution.py:37
  188.1 0.9 collective-permute-done.10.refs_2_
  188.9 6.9 %collective-permute-start.13 = (bf16[2,128]{1,0:T(2,128)(2,1)S(1)}, bf16[2,128]{1,0:T(2,128)(2,1)S(1)}, u32[]{:S(2)}, u32[]{:S(2)}) collective-permute-start(bf16[2,128]{1,0:T(2,128)(2,1)S(1)} %slice.104), channel_id=1, source_target_pairs={{0,16},{16,32},{32,48},{48,64},{64,80},{80,96},{96,112},{112,128},... | collective-permute-start | bytes 1544 | tf_op jit(solution)/shard_map/ppermute | solution.py:49
  195.8 3.6 %collective-permute-start.12 = (bf16[4,4,64,128]{3,2,1,0:T(8,128)(2,1)S(1)}, bf16[4,4,64,128]{3,2,1,0:T(8,128)(2,1)S(1)}, u32[]{:S(2)}, u32[]{:S(2)}) collective-permute-start(bf16[4,4,64,128]{3,2,1,0:T(8,128)(2,1)S(1)} %shard_map.177.own_ref), channel_id=1, source_target_pairs={{16,0},{0,16},{17,1},{1,17},{18,2},{2,18},{19,3},{3,19},{20,4},{4,... | collective-permute-start | bytes 786440 | tf_op jit(solution)/shard_map/ppermute | solution.py:37
  199.5 0.7 multiply_convert_fusion
  200.6 2.7 %mixer.1 = (bf16[2,16,64,128]{3,2,1,0:T(8,128)(2,1)}, bf16[256,128]{1,0:T(8,128)(2,1)}, bf16[256,128]{1,0:T(8,128)(2,1)}) custom-call(bf16[16,256,128]{2,1,0:T(8,128)(2,1)S(1)} %all-to-all-done.4.full_ref, bf16[256,2048]{1,0:T(8,128)(2,1)S(1)} %copy-done, bf16[2048,128]{1,0:T(8,128)(2,1)S(1)} %bitcast.20, bf16[256,128]{1,0:T(8,128)(2,1)} %get-tuple-element.31.mixed_hbm, ...), custom_call_target="tpu_custom_call" | custom-call | tf_op jit(solution)/shard_map/mixer/pallas_call | solution.py:282
  203.4 5.4 %all_to_all.36 = bf16[2,16,64,128]{3,2,1,0:T(8,128)(2,1)S(1)} all-to-all(bf16[2,16,64,128]{3,2,1,0:T(8,128)(2,1)} %get-tuple-element.26), channel_id=1, replica_groups=mesh['z'=16,'c'=2,'y'=4,'x'=4] {'c'}, dimensions={0} | all-to-all | bytes 1048576 | tf_op jit(solution)/shard_map/all_to_all | solution.py:22
  208.7 0.8 reduce_sum.21
  209.6 7.0 %all-to-all-start.6 = ((bf16[16,64,128]{2,1,0:T(8,128)(2,1)}), bf16[16,64,128]{2,1,0:T(8,128)(2,1)S(1)}, u32[]{:S(2)}, u32[]{:S(2)}) async-start(bf16[16,64,128]{2,1,0:T(8,128)(2,1)} %reduce_sum.21), calls=%async_computation.6 | async-start | bytes 524288 | tf_op jit(solution)/shard_map/all_to_all | solution.py:22
  216.6 2.6 %collective-permute-start.14 = (bf16[2,128]{1,0:T(2,128)(2,1)S(1)}, bf16[2,128]{1,0:T(2,128)(2,1)S(1)}, u32[]{:S(2)}, u32[]{:S(2)}) collective-permute-start(bf16[2,128]{1,0:T(2,128)(2,1)S(1)} %slice.91), channel_id=1, source_target_pairs={{16,0},{32,16},{48,32},{64,48},{80,64},{96,80},{112,96},{128,112},... | collective-permute-start | bytes 1544 | tf_op jit(solution)/shard_map/ppermute | solution.py:49
  219.2 2.8 %add_convert_fusion = (bf16[1,64,2048]{2,1,0:T(8,128)(2,1)}, bf16[1,64,2048]{2,1,0:T(8,128)(2,1)}, bf16[1,64,2048]{2,1,0:T(8,128)(2,1)}) fusion(bf16[3,64,2048]{2,1,0:T(8,128)(2,1)} %collective-permute-done.5, bf16[3,64,2048]{2,1,0:T(8,128)(2,1)} %collective-permute-done.4, bf16[3,64,2048]{2,1,0:T(8,128)(2,1)} %collective-permute-done.3, ...), kind=kLoop, calls=%fused_computation.1 | loop fusion | flops 3145728 | bytes 3932160 | tf_op jit(solution)/shard_map/convert_element_type | solution.py:377
  222.0 7.4 %collective-permute-done.14 = bf16[2,128]{1,0:T(2,128)(2,1)S(1)} collective-permute-done((bf16[2,128]{1,0:T(2,128)(2,1)S(1)}, bf16[2,128]{1,0:T(2,128)(2,1)S(1)}, u32[]{:S(2)}, u32[]{:S(2)}) %collective-permute-start.14) | collective-permute-done | bytes 544 | tf_op jit(solution)/shard_map/ppermute | solution.py:49
  229.4 0.7 fusion
  230.1 0.7 fusion.2
  230.8 0.7 convert_reduce_fusion
  (54 shorter events, 0.8 us)
Async XLA Ops:
  0.6 19.1 %copy-start.10 = (bf16[1,64,2048]{2,1,0:T(8,128)(2,1)S(1)}, bf16[1,64,2048]{2,1,0:T(8,128)(2,1)}, u32[]{:S(2)}) copy-start(bf16[1,64,2048]{2,1,0:T(8,128)(2,1)} %param.16) | copy-start | bytes 786436
  0.6 19.1 %copy-start.11 = (bf16[1,64,2048]{2,1,0:T(8,128)(2,1)S(1)}, bf16[1,64,2048]{2,1,0:T(8,128)(2,1)}, u32[]{:S(2)}) copy-start(bf16[1,64,2048]{2,1,0:T(8,128)(2,1)} %param.17) | copy-start | bytes 786436
  3.0 41.7 %all-to-all-start = ((bf16[32,40,128]{2,1,0:T(8,128)(2,1)}), bf16[32,40,128]{2,1,0:T(8,128)(2,1)S(1)}, u32[]{:S(2)}, u32[]{:S(2)}) async-start(bf16[32,40,128]{2,1,0:T(8,128)(2,1)} %bitcast.29), calls=%async_computation | async-start | bytes 655360 | tf_op jit(solution)/shard_map/all_to_all | solution.py:22
  46.2 4.3 %copy-start.12 = (bf16[1,64,2048]{2,1,0:T(8,128)(2,1)S(1)}, bf16[1,64,2048]{2,1,0:T(8,128)(2,1)}, u32[]{:S(2)}) copy-start(bf16[1,64,2048]{2,1,0:T(8,128)(2,1)} %param.18) | copy-start | bytes 786436
  46.2 46.1 %all-to-all-start.1 = ((bf16[4,8,160,128]{3,2,1,0:T(8,128)(2,1)}), bf16[4,8,160,128]{3,2,1,0:T(8,128)(2,1)S(1)}, u32[]{:S(2)}, u32[]{:S(2)}) async-start(bf16[4,8,160,128]{3,2,1,0:T(8,128)(2,1)} %shard_map.171), calls=%async_computation.1 | async-start | bytes 2621440 | tf_op jit(solution)/shard_map/all_to_all | solution.py:22
  50.5 21.2 %collective-permute-start = (bf16[3,64,2048]{2,1,0:T(8,128)(2,1)S(1)}, bf16[3,64,2048]{2,1,0:T(8,128)(2,1)S(1)}, u32[]{:S(2)}, u32[]{:S(2)}) collective-permute-start(bf16[3,64,2048]{2,1,0:T(8,128)(2,1)S(1)} %constant_dynamic-update-slice_fusion.w0_ref), channel_id=1, source_target_pairs={{0,1},{1,2},{2,3},{3,0},{4,5},{5,6},{6,7},{7,4},{8,9},{9,10},{10,1... | collective-permute-start | bytes 2359304 | tf_op jit(solution)/shard_map/ppermute | solution.py:27
  53.6 35.9 %collective-permute-start.1 = (bf16[3,64,2048]{2,1,0:T(8,128)(2,1)S(1)}, bf16[3,64,2048]{2,1,0:T(8,128)(2,1)S(1)}, u32[]{:S(2)}, u32[]{:S(2)}) collective-permute-start(bf16[3,64,2048]{2,1,0:T(8,128)(2,1)S(1)} %constant_dynamic-update-slice_fusion.w0_ref), channel_id=1, source_target_pairs={{0,2},{1,3},{2,0},{3,1},{4,6},{5,7},{6,4},{7,5},{8,10},{9,11},{10,... | collective-permute-start | bytes 2359304 | tf_op jit(solution)/shard_map/ppermute | solution.py:27
  58.0 33.4 %collective-permute-start.2 = (bf16[3,64,2048]{2,1,0:T(8,128)(2,1)S(1)}, bf16[3,64,2048]{2,1,0:T(8,128)(2,1)S(1)}, u32[]{:S(2)}, u32[]{:S(2)}) collective-permute-start(bf16[3,64,2048]{2,1,0:T(8,128)(2,1)S(1)} %constant_dynamic-update-slice_fusion.w0_ref), channel_id=1, source_target_pairs={{0,3},{1,0},{2,1},{3,2},{4,7},{5,4},{6,5},{7,6},{8,11},{9,8},{10,9... | collective-permute-start | bytes 2359304 | tf_op jit(solution)/shard_map/ppermute | solution.py:27
  89.6 0.9 copy-start.1
  91.4 0.9 copy-start.3
  92.3 1.1 copy-start.2
  93.4 1.1 copy-start.4
  97.7 26.5 %copy-start.15 = (s32[2,256]{1,0:T(2,128)S(1)}, s32[2,256]{1,0:T(2,128)}, u32[]{:S(2)}) copy-start(s32[2,256]{1,0:T(2,128)} %get-tuple-element.24) | copy-start | bytes 6148
  118.4 24.8 %all-to-all-start.3 = ((bf16[32,24,128]{2,1,0:T(8,128)(2,1)}), bf16[32,24,128]{2,1,0:T(8,128)(2,1)S(1)}, u32[]{:S(2)}, u32[]{:S(2)}) async-start(bf16[32,24,128]{2,1,0:T(8,128)(2,1)} %bitcast.28), calls=%async_computation.3 | async-start | bytes 393216 | tf_op jit(solution)/shard_map/all_to_all | solution.py:22
  144.5 3.8 %copy-start.6 = (bf16[128,64]{0,1:T(8,128)(2,1)S(1)}, bf16[128,64]{0,1:T(8,128)(2,1)}, u32[]{:S(2)}) copy-start(bf16[128,64]{0,1:T(8,128)(2,1)} %param.23) | copy-start | bytes 49156
  144.5 24.7 %copy-start.5 = (bf16[3,160,256]{2,1,0:T(8,128)(2,1)S(1)}, bf16[3,160,256]{2,1,0:T(8,128)(2,1)}, u32[]{:S(2)}) copy-start(bf16[3,160,256]{2,1,0:T(8,128)(2,1)} %get-tuple-element.19.cots_ref) | copy-start | bytes 737284
  144.5 56.1 %all-to-all-start.4 = ((bf16[16,256,128]{2,1,0:T(8,128)(2,1)}), bf16[16,256,128]{2,1,0:T(8,128)(2,1)S(1)}, u32[]{:S(2)}, u32[]{:S(2)}) async-start(bf16[16,256,128]{2,1,0:T(8,128)(2,1)} %shard_map.175), calls=%async_computation.4 | async-start | bytes 2097152 | tf_op jit(solution)/shard_map/all_to_all | solution.py:22
  148.3 34.2 %copy-start.9 = (bf16[256,128]{1,0:T(8,128)(2,1)S(1)}, bf16[256,128]{1,0:T(8,128)(2,1)}, u32[]{:S(2)}) copy-start(bf16[256,128]{1,0:T(8,128)(2,1)} %param.20) | copy-start | bytes 196612
  148.4 34.2 %copy-start.13 = (bf16[256,128]{1,0:T(8,128)(2,1)S(1)}, bf16[256,128]{1,0:T(8,128)(2,1)}, u32[]{:S(2)}) copy-start(bf16[256,128]{1,0:T(8,128)(2,1)} %param.21) | copy-start | bytes 196612
  148.4 39.7 %copy-start.16 = (f32[3,128]{1,0:T(4,128)S(1)}, f32[3,128]{1,0:T(4,128)}, u32[]{:S(2)}) copy-start(f32[3,128]{1,0:T(4,128)} %param.22) | copy-start | bytes 4612
  148.4 12.2 %collective-permute-start.6 = (bf16[64,128]{1,0:T(8,128)(2,1)S(1)}, bf16[64,128]{1,0:T(8,128)(2,1)S(1)}, u32[]{:S(2)}, u32[]{:S(2)}) collective-permute-start(bf16[64,128]{1,0:T(8,128)(2,1)S(1)} %bitcast.24), channel_id=1, source_target_pairs={{128,0},{160,32},{192,64},{224,96},{256,128},{288,160},{320,192},{... | collective-permute-start | bytes 49160 | tf_op jit(solution)/shard_map/ppermute | solution.py:37
  150.9 13.4 %collective-permute-start.7 = (bf16[64,128]{1,0:T(8,128)(2,1)S(1)}, bf16[64,128]{1,0:T(8,128)(2,1)S(1)}, u32[]{:S(2)}, u32[]{:S(2)}) collective-permute-start(bf16[64,128]{1,0:T(8,128)(2,1)S(1)} %bitcast.25), channel_id=1, source_target_pairs={{256,0},{288,32},{320,64},{352,96},{384,128},{416,160},{448,192},{... | collective-permute-start | bytes 49160 | tf_op jit(solution)/shard_map/ppermute | solution.py:37
  158.4 8.4 %collective-permute-start.8 = (bf16[64,128]{1,0:T(8,128)(2,1)S(1)}, bf16[64,128]{1,0:T(8,128)(2,1)S(1)}, u32[]{:S(2)}, u32[]{:S(2)}) collective-permute-start(bf16[64,128]{1,0:T(8,128)(2,1)S(1)} %bitcast.26), channel_id=1, source_target_pairs={{384,0},{416,32},{448,64},{480,96},{0,128},{32,160},{64,192},{96,2... | collective-permute-start | bytes 49160 | tf_op jit(solution)/shard_map/ppermute | solution.py:37
  166.8 32.7 %copy-start.8 = (bf16[256,128]{1,0:T(8,128)(2,1)S(1)}, bf16[256,128]{1,0:T(8,128)(2,1)}, u32[]{:S(2)}) copy-start(bf16[256,128]{1,0:T(8,128)(2,1)} %outer_hbm.1) | copy-start | bytes 196612
  166.8 18.6 %collective-permute-start.9 = (bf16[4,64,128]{2,1,0:T(8,128)(2,1)S(1)}, bf16[4,64,128]{2,1,0:T(8,128)(2,1)S(1)}, u32[]{:S(2)}, u32[]{:S(2)}) collective-permute-start(bf16[4,64,128]{2,1,0:T(8,128)(2,1)S(1)} %shard_map.176.refs_0_), channel_id=1, source_target_pairs={{32,0},{64,32},{96,64},{0,96},{160,128},{192,160},{224,192},{128,2... | collective-permute-start | bytes 196616 | tf_op jit(solution)/shard_map/ppermute | solution.py:37
  171.9 47.3 %collective-permute-start.5 = (bf16[3,64,2048]{2,1,0:T(8,128)(2,1)}, bf16[3,64,2048]{2,1,0:T(8,128)(2,1)}, u32[]{:S(2)}, u32[]{:S(2)}) collective-permute-start(bf16[3,64,2048]{2,1,0:T(8,128)(2,1)} %get-tuple-element.23), channel_id=1, source_target_pairs={{0,1},{1,2},{2,3},{3,0},{4,5},{5,6},{6,7},{7,4},{8,9},{9,10},{10,1... | collective-permute-start | bytes 2359304 | tf_op jit(solution)/shard_map/ppermute | solution.py:27
  175.0 44.2 %collective-permute-start.4 = (bf16[3,64,2048]{2,1,0:T(8,128)(2,1)}, bf16[3,64,2048]{2,1,0:T(8,128)(2,1)}, u32[]{:S(2)}, u32[]{:S(2)}) collective-permute-start(bf16[3,64,2048]{2,1,0:T(8,128)(2,1)} %get-tuple-element.22), channel_id=1, source_target_pairs={{0,2},{1,3},{2,0},{3,1},{4,6},{5,7},{6,4},{7,5},{8,10},{9,11},{10,... | collective-permute-start | bytes 2359304 | tf_op jit(solution)/shard_map/ppermute | solution.py:27
  179.3 21.3 %copy-start = (bf16[256,2048]{1,0:T(8,128)(2,1)S(1)}, bf16[256,2048]{1,0:T(8,128)(2,1)}, u32[]{:S(2)}) copy-start(bf16[256,2048]{1,0:T(8,128)(2,1)} %out_grad_ref.1) | copy-start | bytes 3145732
  179.3 39.8 %collective-permute-start.3 = (bf16[3,64,2048]{2,1,0:T(8,128)(2,1)}, bf16[3,64,2048]{2,1,0:T(8,128)(2,1)}, u32[]{:S(2)}, u32[]{:S(2)}) collective-permute-start(bf16[3,64,2048]{2,1,0:T(8,128)(2,1)} %get-tuple-element.21), channel_id=1, source_target_pairs={{0,3},{1,0},{2,1},{3,2},{4,7},{5,4},{6,5},{7,6},{8,11},{9,8},{10,9... | collective-permute-start | bytes 2359304 | tf_op jit(solution)/shard_map/ppermute | solution.py:27
  182.6 6.3 %collective-permute-start.10 = (bf16[4,64,128]{2,1,0:T(8,128)(2,1)S(1)}, bf16[4,64,128]{2,1,0:T(8,128)(2,1)S(1)}, u32[]{:S(2)}, u32[]{:S(2)}) collective-permute-start(bf16[4,64,128]{2,1,0:T(8,128)(2,1)S(1)} %shard_map.176.refs_0_), channel_id=1, source_target_pairs={{64,0},{96,32},{0,64},{32,96},{192,128},{224,160},{128,192},{160,2... | collective-permute-start | bytes 196616 | tf_op jit(solution)/shard_map/ppermute | solution.py:37
  185.4 10.4 %collective-permute-start.11 = (bf16[4,64,128]{2,1,0:T(8,128)(2,1)S(1)}, bf16[4,64,128]{2,1,0:T(8,128)(2,1)S(1)}, u32[]{:S(2)}, u32[]{:S(2)}) collective-permute-start(bf16[4,64,128]{2,1,0:T(8,128)(2,1)S(1)} %shard_map.176.refs_0_), channel_id=1, source_target_pairs={{96,0},{0,32},{32,64},{64,96},{224,128},{128,160},{160,192},{192,2... | collective-permute-start | bytes 196616 | tf_op jit(solution)/shard_map/ppermute | solution.py:37
  188.9 10.5 %collective-permute-start.13 = (bf16[2,128]{1,0:T(2,128)(2,1)S(1)}, bf16[2,128]{1,0:T(2,128)(2,1)S(1)}, u32[]{:S(2)}, u32[]{:S(2)}) collective-permute-start(bf16[2,128]{1,0:T(2,128)(2,1)S(1)} %slice.104), channel_id=1, source_target_pairs={{0,16},{16,32},{32,48},{48,64},{64,80},{80,96},{96,112},{112,128},... | collective-permute-start | bytes 1544 | tf_op jit(solution)/shard_map/ppermute | solution.py:49
  195.8 4.7 %collective-permute-start.12 = (bf16[4,4,64,128]{3,2,1,0:T(8,128)(2,1)S(1)}, bf16[4,4,64,128]{3,2,1,0:T(8,128)(2,1)S(1)}, u32[]{:S(2)}, u32[]{:S(2)}) collective-permute-start(bf16[4,4,64,128]{3,2,1,0:T(8,128)(2,1)S(1)} %shard_map.177.own_ref), channel_id=1, source_target_pairs={{16,0},{0,16},{17,1},{1,17},{18,2},{2,18},{19,3},{3,19},{20,4},{4,... | collective-permute-start | bytes 786440 | tf_op jit(solution)/shard_map/ppermute | solution.py:37
  203.3 13.2 %copy-start.14 = (bf16[256,128]{1,0:T(8,128)(2,1)S(1)}, bf16[256,128]{1,0:T(8,128)(2,1)}, u32[]{:S(2)}) copy-start(bf16[256,128]{1,0:T(8,128)(2,1)} %get-tuple-element.28) | copy-start | bytes 196612
  203.4 15.8 %copy-start.7 = (bf16[3,64,2048]{2,1,0:T(8,128)(2,1)S(1)}, bf16[3,64,2048]{2,1,0:T(8,128)(2,1)}, u32[]{:S(2)}) copy-start(bf16[3,64,2048]{2,1,0:T(8,128)(2,1)} %get-tuple-element.20) | copy-start | bytes 2359300
  209.6 21.2 %all-to-all-start.6 = ((bf16[16,64,128]{2,1,0:T(8,128)(2,1)}), bf16[16,64,128]{2,1,0:T(8,128)(2,1)S(1)}, u32[]{:S(2)}, u32[]{:S(2)}) async-start(bf16[16,64,128]{2,1,0:T(8,128)(2,1)} %reduce_sum.21), calls=%async_computation.6 | async-start | bytes 524288 | tf_op jit(solution)/shard_map/all_to_all | solution.py:22
  216.6 12.8 %collective-permute-start.14 = (bf16[2,128]{1,0:T(2,128)(2,1)S(1)}, bf16[2,128]{1,0:T(2,128)(2,1)S(1)}, u32[]{:S(2)}, u32[]{:S(2)}) collective-permute-start(bf16[2,128]{1,0:T(2,128)(2,1)S(1)} %slice.91), channel_id=1, source_target_pairs={{16,0},{32,16},{48,32},{64,48},{80,64},{96,80},{112,96},{128,112},... | collective-permute-start | bytes 1544 | tf_op jit(solution)/shard_map/ppermute | solution.py:49

commit v6 on v5

--- a/solution.py
+++ b/solution.py
@@ -67,7 +67,7 @@
     return act, gate_cot, lin_cot
 
 
-def routing_kernel(yi_ref, xi_ref, ids_ref, weights_ref, rows_ref, grads_ref, send_ref, place_ref, *, kx, cap, padded):
+def routing_kernel(yi_ref, xi_ref, core_ref, ids_ref, weights_ref, rows_ref, grads_ref, send_ref, place_ref, *, kx, cap):
     tokens = ids_ref.shape[1]
     experts = send_ref.shape[0] // kx
     ids = ids_ref[...]
@@ -80,8 +80,9 @@
     before = dot(one, jnp.where(early < late, 1.0, 0.0).astype(BF), 1, 0)
     rank0 = jnp.sum(jnp.where(first, before, 0.0), axis=0, keepdims=True).astype(jnp.int32)
     rank1 = jnp.sum(jnp.where(second, before, 0.0), axis=0, keepdims=True).astype(jnp.int32)
-    place_ref[0:1, :] = ids[0:1, :] * padded + rank0
-    place_ref[1:2, :] = ids[1:2, :] * padded + rank1
+    turn = jnp.where((ids & 1) == core_ref[0], 0, cap) - (ids & 1) * cap
+    place_ref[0:1, :] = ids[0:1, :] * cap + turn[0:1, :] + rank0
+    place_ref[1:2, :] = ids[1:2, :] * cap + turn[1:2, :] + rank1
     slots = experts * kx
     slot = lax.broadcasted_iota(jnp.int32, (slots, 1), 0)
     owner = slot // kx
@@ -99,24 +100,24 @@
     send_ref[...] = both.reshape(slots, both.shape[1] // LANES, LANES).astype(BF)
 
 
-def route(route_ids, route_weights, moe_input, out_grad, yi, xi, n_y, kx, experts, cap, padded):
+def route(route_ids, route_weights, moe_input, out_grad, yi, xi, core, n_y, kx, experts, cap):
     tokens, width = moe_input.shape
     wy = width // n_y
     slots = experts * kx
     return pl.pallas_call(
-        functools.partial(routing_kernel, kx=kx, cap=cap, padded=padded),
+        functools.partial(routing_kernel, kx=kx, cap=cap),
         grid_spec=pltpu.PrefetchScalarGridSpec(
-            num_scalar_prefetch=2,
+            num_scalar_prefetch=3,
             grid=(1,),
             in_specs=[
-                pl.BlockSpec((2, tokens), lambda i, y, x: (0, 0)),
-                pl.BlockSpec((2, tokens), lambda i, y, x: (0, 0)),
-                pl.BlockSpec((tokens, wy), lambda i, y, x: (0, y[0])),
-                pl.BlockSpec((tokens, wy), lambda i, y, x: (0, y[0])),
+                pl.BlockSpec((2, tokens), lambda i, y, x, c: (0, 0)),
+                pl.BlockSpec((2, tokens), lambda i, y, x, c: (0, 0)),
+                pl.BlockSpec((tokens, wy), lambda i, y, x, c: (0, y[0])),
+                pl.BlockSpec((tokens, wy), lambda i, y, x, c: (0, y[0])),
             ],
             out_specs=[
-                pl.BlockSpec((slots, 2 * wy // LANES, LANES), lambda i, y, x: (0, 0, 0)),
-                pl.BlockSpec((2, tokens), lambda i, y, x: (0, 0)),
+                pl.BlockSpec((slots, 2 * wy // LANES, LANES), lambda i, y, x, c: (0, 0, 0)),
+                pl.BlockSpec((2, tokens), lambda i, y, x, c: (0, 0)),
             ],
         ),
         out_shape=[
@@ -124,7 +125,7 @@
             jax.ShapeDtypeStruct((2, tokens), jnp.int32),
         ],
         name="route",
-    )(yi[None], xi[None], route_ids.T, route_weights.T, moe_input, out_grad)
+    )(yi[None], xi[None], core[None], route_ids.T, route_weights.T, moe_input, out_grad)
 
 
 def regroup_kernel(got_ref, out_ref):
@@ -169,24 +170,36 @@
             ref[k] = terms[d * hidden : (d + 1) * hidden].astype(ref.dtype)
 
 
-def slot_sum_kernel(part_ref, out_ref, *, n_y, n_x, kx, padded):
+def slot_sum_kernel(core_ref, part_ref, keep_ref, give_ref, *, n_y, n_x, kx):
     _, slots, _ = part_ref.shape
-    rows = out_ref.shape[0]
-    cols = n_x * slots
+    rows = keep_ref.shape[0]
+    cap = n_x * kx
     row = lax.broadcasted_iota(jnp.int32, (rows, 1), 0)
-    owner = row // padded
-    at = row - owner * padded
+    ring = row // cap
+    at = row - ring * cap
     group = at // kx
-    wanted = jnp.where(group < n_x, group * slots + owner * kx + (at - group * kx), -1)
-    col = lax.broadcasted_iota(jnp.int32, (rows, cols), 1)
-    pick = jnp.where(wanted == col, 1.0, 0.0).astype(BF)
+    wanted = group * slots + 2 * ring * kx + (at - group * kx)
+    col = lax.broadcasted_iota(jnp.int32, (rows, n_x * slots), 1)
     sums = []
     for x in range(n_x):
         total = part_ref[x].astype(F32)
         for y in range(1, n_y):
             total = total + part_ref[y * n_x + x].astype(F32)
         sums.append(total.astype(BF))
-    out_ref[...] = dot(pick, jnp.concatenate(sums, axis=0), 1, 0).astype(BF)
+    sums = jnp.concatenate(sums, axis=0)
+    for ref, core in ((keep_ref, core_ref[0]), (give_ref, 1 - core_ref[0])):
+        pick = jnp.where(wanted + core * kx == col, 1.0, 0.0).astype(BF)
+        ref[...] = dot(pick, sums, 1, 0).astype(BF)
+
+
+def join_kernel(own_ref, other_ref, out_ref):
+    rings, both, _ = out_ref.shape
+    cap = both // 2
+    own = own_ref[...].astype(F32)
+    other = other_ref[...].astype(F32)
+    for z in range(rings):
+        at = slice(z * cap, (z + 1) * cap)
+        out_ref[z] = jnp.concatenate([own[at], other[at]], axis=0).astype(BF)
 
 
 def combine_kernel(place_ref, back_ref, out_ref):
@@ -200,12 +213,12 @@
 
 
 def mixer_kernel(
-    full_ref, out_grad_ref, proj_ref, mixed_hbm, convolved_hbm, outer_hbm,
-    terms_ref, cot_ref, outer_grad_hbm,
+    core_ref, full_ref, out_grad_ref, proj_ref, mixed_hbm, convolved_hbm, outer_hbm,
+    keep_ref, give_ref, cot_ref, outer_grad_hbm,
     mixed_ref, convolved_ref, outer_ref, outer_grad_ref, sems,
 ):
     n_tp, _, _ = full_ref.shape
-    n_c, n_z, per, _ = terms_ref.shape
+    n_z, per, _ = keep_ref.shape
     fetches = [
         pltpu.make_async_copy(src, dst, sems.at[i])
         for i, (src, dst) in enumerate(
@@ -225,10 +238,12 @@
     cot_ref[...] = (mixed_grad * outer_ref[...].astype(F32)).astype(BF)
     fetches[2].wait()
     terms = dot(stream, mixed_ref[...], 0, 0).astype(BF)
+    lower = core_ref[0] == 0
     for z in range(n_z):
-        for c in range(n_c):
-            at = (z * n_c + c) * per
-            terms_ref[c, z] = terms[at : at + per]
+        low = terms[2 * z * per : (2 * z + 1) * per]
+        high = terms[(2 * z + 1) * per : (2 * z + 2) * per]
+        keep_ref[z] = jnp.where(lower, low, high)
+        give_ref[z] = jnp.where(lower, high, low)
     keep.wait()
 
 
@@ -274,17 +289,19 @@
     return pltpu.with_memory_space_constraint(value, pltpu.HBM)
 
 
-def mix(full, out_grad, proj, mixed, convolved, outer_gate, n_c, n_z):
+def mix(core, full, out_grad, proj, mixed, convolved, outer_gate, n_c, n_z):
     _, tokens, lanes = full.shape
     small = (tokens, lanes)
     whole = pl.BlockSpec(memory_space=pltpu.VMEM)
     away = pl.BlockSpec(memory_space=pltpu.HBM)
+    half = (n_z, proj.shape[0] // (n_c * n_z), lanes)
     return pl.pallas_call(
         mixer_kernel,
-        in_specs=[whole, whole, whole, away, away, away],
-        out_specs=[whole, whole, away],
+        in_specs=[pl.BlockSpec(memory_space=pltpu.SMEM)] + [whole] * 3 + [away] * 3,
+        out_specs=[whole, whole, whole, away],
         out_shape=[
-            pltpu.HBM((n_c, n_z, proj.shape[0] // (n_c * n_z), lanes), BF),
+            jax.ShapeDtypeStruct(half, BF),
+            pltpu.HBM(half, BF),
             pltpu.HBM(small, BF),
             pltpu.HBM(small, BF),
         ],
@@ -297,12 +314,16 @@
         ],
         compiler_params=pltpu.CompilerParams(vmem_limit_bytes=16 << 20),
         name="mixer",
-    )(full, out_grad, proj, *map(in_hbm, (mixed, convolved, outer_gate)))
-
-
-def on_core(kernel, outs, *args, mib=12, **static):
+    )(core[None], full, out_grad, proj, *map(in_hbm, (mixed, convolved, outer_gate)))
+
+
+def on_core(kernel, outs, *args, mib=12, scalars=0, **static):
     return pl.pallas_call(
         functools.partial(kernel, **static) if static else kernel,
+        in_specs=[
+            pl.BlockSpec(memory_space=pltpu.SMEM if i < scalars else pltpu.VMEM)
+            for i in range(len(args))
+        ],
         out_shape=[pltpu.HBM(s, t) for s, t in outs],
         compiler_params=pltpu.CompilerParams(vmem_limit_bytes=mib << 20),
     )(*args)
@@ -335,15 +356,15 @@
     cap = 5 * tokens // (2 * experts)
     kx = cap // n_x
     slots = experts * kx
-    padded = -(-cap // 8) * 8
     yi = lax.axis_index("y")
     xi = lax.axis_index("x")
 
     weights = jnp.concatenate([gate_weight, lin_weight, down_weight], axis=0)
     blocks = [weights] + [turned(weights, "x", d) for d in range(1, n_x)]
 
+    core = lax.axis_index("c")
     send, place = route(
-        route_ids, route_weights, moe_input, out_grad, yi, xi, n_y, kx, experts, cap, padded
+        route_ids, route_weights, moe_input, out_grad, yi, xi, core, n_y, kx, experts, cap
     )
     got = swap(send.reshape(experts, kx * 2 * chunks, wdev), SP)
     (got,) = on_core(
@@ -360,17 +381,19 @@
     )
     part = swap(part, TP)
     terms = on_core(weight_grad_kernel, [((3, hidden, width), BF)] * n_x, got, cots, mib=24)
-    (slot_sums,) = on_core(
+    held, given = on_core(
         slot_sum_kernel,
-        [((experts * padded, wdev), BF)],
+        [((n_z * cap, wdev), BF)] * 2,
+        core[None],
         part,
         n_y=n_y,
         n_x=n_x,
         kx=kx,
-        padded=padded,
-    )
-    back = swap(slot_sums.reshape(experts, padded, wdev), SP)
-    back = back.reshape(experts * padded, wdev)
+        scalars=1,
+    )
+    given = shifted(given, "c", n_c, 1, 1)
+    (joined,) = on_core(join_kernel, [((n_z, 2 * cap, wdev), BF)], held, given)
+    back = swap(joined, "z").reshape(experts * cap, wdev)
 
     spread = [terms[0]] + [turned(terms[d], "x", -d) for d in range(1, n_x)]
     gate_grad, lin_grad, down_grad = (
@@ -393,12 +416,12 @@
     proj = grouped(out_proj.T, "z", n_z // inner, inner)
     proj = grouped(proj, "z", inner, 1)
     twin = shifted(proj, "c", n_c, 1, 1)
-    proj = with_twin(proj, twin, lax.axis_index("c")).reshape(width, wdev)
-    pair, conv_cot, outer_gate_grad = mix(
-        full, out_grad, proj, mixed, convolved, outer_gate, n_c, n_z
-    )
-    terms = swap(pair, "c")
-    terms = jnp.sum(terms.astype(F32), axis=0).astype(BF)
+    proj = with_twin(proj, twin, core).reshape(width, wdev)
+    keep, give, conv_cot, outer_gate_grad = mix(
+        core, full, out_grad, proj, mixed, convolved, outer_gate, n_c, n_z
+    )
+    given = shifted(give, "c", n_c, 1, 1)
+    terms = (keep.astype(F32) + given.astype(F32)).astype(BF)
     out_proj_grad = jnp.sum(swap(terms, "z").astype(F32), axis=0)
 
     later_rows = from_behind(conv_cot[: taps - 1], SP, -1)

time: 236 us -> 239 us (1.013); the launches traced: 231 us -> 237 us
  starting transfers between devices: 91.8 us -> 103 us
  blocking collectives: 24.6 us -> 19.2 us
    ppermute x7 -> x9, starting transfers between devices: 23.6 us -> 39.3 us  [shifted(): return lax.ppermute(value, axis, [(source(i), i) for i in range(count)])]
    ppermute x6, waiting for transfers between devices: 29.4 us -> 43 us  [turned(): lax.ppermute(value, axis, [(i, (i + by) % count) for i in range(count)])]
    ppermute x2, waiting for transfers between devices: 7.4 us -> 0.01 us  [from_behind(): return lax.ppermute(value, axis, pairs)]
    all_to_all x5, waiting for transfers between devices: 43.7 us -> 37.4 us  [swap(): return lax.all_to_all(blocks, axis, split_axis=0, concat_axis=0, tiled=True)]
    all_to_all x2 -> x1, blocking collectives: 24.6 us -> 19.2 us  [swap(): return lax.all_to_all(blocks, axis, split_axis=0, concat_axis=0, tiled=True)]
    ppermute x2, starting transfers between devices: 9.41 us -> 6.2 us  [from_behind(): return lax.ppermute(value, axis, pairs)]
    ppermute x7 -> x9, waiting for transfers between devices: 7.45 us -> 5.71 us  [shifted(): return lax.ppermute(value, axis, [(source(i), i) for i in range(count)])]
    unnamed x36 -> x38, local copies, waits for them, and re-layouts: 4.17 us -> 5.03 us
  transfers between devices with their start and end apart: 20 -> 22, of which waited for: 10 -> 10; matrix products, arithmetic and copies ran while one was open for 3% -> 3% of each run, Pallas kernels for 2% -> 2%
where the time goes in v6:
time: 239 us; the launch traced here: 237 us
  starting transfers between devices  103 us (43%)
  waiting for transfers between devices  86.1 us (36%)
  blocking collectives  19.2 us (8%)
  Pallas kernels  15.5 us (6%)
  other arithmetic  6.4 us (3%)
  local copies, waits for them, and re-layouts  5.88 us (2%)
    ppermute x6, waiting for transfers between devices, turned(): lax.ppermute(value, axis, [(i, (i + by) % count) for i in range(count)])  43 us
    ppermute x9, starting transfers between devices, shifted(): return lax.ppermute(value, axis, [(source(i), i) for i in range(count)])  39.3 us
    all_to_all x5, waiting for transfers between devices, swap(): return lax.all_to_all(blocks, axis, split_axis=0, concat_axis=0, tiled=True)  37.4 us
    all_to_all x5, starting transfers between devices, swap(): return lax.all_to_all(blocks, axis, split_axis=0, concat_axis=0, tiled=True)  36 us
    ppermute x6, starting transfers between devices, turned(): lax.ppermute(value, axis, [(i, (i + by) % count) for i in range(count)])  21.3 us
    all_to_all x1, blocking collectives, swap(): return lax.all_to_all(blocks, axis, split_axis=0, concat_axis=0, tiled=True)  19.2 us
    pallas_call x6, Pallas kernels, on_core(): pl.pallas_call(functools.partial(kernel, **static) if static else kernel,...  10.5 us
    ppermute x2, starting transfers between devices, from_behind(): return lax.ppermute(value, axis, pairs)  6.2 us
  transfers between devices with their start and end apart: 22, of which 10 were waited for; matrix products, arithmetic and copies ran while one was open for 3% of the time, Pallas kernels for 2%

profile of v6, /device:TPU:1, one launch (start us, length us, event | category | flops | bytes accessed | tf_op | source)
XLA Modules:
  0.0 237.0 jit_solution(1090506438184814545)
XLA Ops:
  0.7 2.3 route.1
  2.9 16.7 %all-to-all-start = ((bf16[32,40,128]{2,1,0:T(8,128)(2,1)}), bf16[32,40,128]{2,1,0:T(8,128)(2,1)S(1)}, u32[]{:S(2)}, u32[]{:S(2)}) async-start(bf16[32,40,128]{2,1,0:T(8,128)(2,1)} %bitcast.27), calls=%async_computation | async-start | bytes 655360 | tf_op jit(solution)/shard_map/all_to_all | solution.py:22
  19.8 24.9 %all-to-all-done = bf16[32,40,128]{2,1,0:T(8,128)(2,1)S(1)} async-done(((bf16[32,40,128]{2,1,0:T(8,128)(2,1)}), bf16[32,40,128]{2,1,0:T(8,128)(2,1)S(1)}, u32[]{:S(2)}, u32[]{:S(2)}) %all-to-all-start) | async-done | bytes 327712 | tf_op jit(solution)/shard_map/all_to_all | solution.py:22
  44.7 1.5 shard_map.171
  46.2 4.3 %all-to-all-start.1 = ((bf16[4,8,160,128]{3,2,1,0:T(8,128)(2,1)}), bf16[4,8,160,128]{3,2,1,0:T(8,128)(2,1)S(1)}, u32[]{:S(2)}, u32[]{:S(2)}) async-start(bf16[4,8,160,128]{3,2,1,0:T(8,128)(2,1)} %shard_map.171), calls=%async_computation.1 | async-start | bytes 2621440 | tf_op jit(solution)/shard_map/all_to_all | solution.py:22
  50.5 3.1 %collective-permute-start = (bf16[3,64,2048]{2,1,0:T(8,128)(2,1)S(1)}, bf16[3,64,2048]{2,1,0:T(8,128)(2,1)S(1)}, u32[]{:S(2)}, u32[]{:S(2)}) collective-permute-start(bf16[3,64,2048]{2,1,0:T(8,128)(2,1)S(1)} %constant_dynamic-update-slice_fusion.w0_ref), channel_id=1, source_target_pairs={{0,1},{1,2},{2,3},{3,0},{4,5},{5,6},{6,7},{7,4},{8,9},{9,10},{10,1... | collective-permute-start | bytes 2359304 | tf_op jit(solution)/shard_map/ppermute | solution.py:27
  53.6 4.4 %collective-permute-start.1 = (bf16[3,64,2048]{2,1,0:T(8,128)(2,1)S(1)}, bf16[3,64,2048]{2,1,0:T(8,128)(2,1)S(1)}, u32[]{:S(2)}, u32[]{:S(2)}) collective-permute-start(bf16[3,64,2048]{2,1,0:T(8,128)(2,1)S(1)} %constant_dynamic-update-slice_fusion.w0_ref), channel_id=1, source_target_pairs={{0,2},{1,3},{2,0},{3,1},{4,6},{5,7},{6,4},{7,5},{8,10},{9,11},{10,... | collective-permute-start | bytes 2359304 | tf_op jit(solution)/shard_map/ppermute | solution.py:27
  58.0 3.1 %collective-permute-start.2 = (bf16[3,64,2048]{2,1,0:T(8,128)(2,1)S(1)}, bf16[3,64,2048]{2,1,0:T(8,128)(2,1)S(1)}, u32[]{:S(2)}, u32[]{:S(2)}) collective-permute-start(bf16[3,64,2048]{2,1,0:T(8,128)(2,1)S(1)} %constant_dynamic-update-slice_fusion.w0_ref), channel_id=1, source_target_pairs={{0,3},{1,0},{2,1},{3,2},{4,7},{5,4},{6,5},{7,6},{8,11},{9,8},{10,9... | collective-permute-start | bytes 2359304 | tf_op jit(solution)/shard_map/ppermute | solution.py:27
  61.1 10.6 %collective-permute-done.w1_ref = bf16[3,64,2048]{2,1,0:T(8,128)(2,1)S(1)} collective-permute-done((bf16[3,64,2048]{2,1,0:T(8,128)(2,1)S(1)}, bf16[3,64,2048]{2,1,0:T(8,128)(2,1)S(1)}, u32[]{:S(2)}, u32[]{:S(2)}) %collective-permute-start) | collective-permute-done | bytes 786464 | tf_op jit(solution)/shard_map/ppermute | solution.py:27
  71.7 17.8 %collective-permute-done.1.w2_ref = bf16[3,64,2048]{2,1,0:T(8,128)(2,1)S(1)} collective-permute-done((bf16[3,64,2048]{2,1,0:T(8,128)(2,1)S(1)}, bf16[3,64,2048]{2,1,0:T(8,128)(2,1)S(1)}, u32[]{:S(2)}, u32[]{:S(2)}) %collective-permute-start.1) | collective-permute-done | bytes 786464 | tf_op jit(solution)/shard_map/ppermute | solution.py:27
  89.5 0.9 copy-done.1
  90.4 0.9 collective-permute-done.2.w3_ref
  91.4 0.9 copy-done.3
  92.3 1.1 copy-done.2
  93.4 1.1 copy-done.4
  94.5 3.1 %shard_map.172 = (bf16[16,160,128]{2,1,0:T(8,128)(2,1)}, bf16[3,160,256]{2,1,0:T(8,128)(2,1)}) custom-call(bf16[4,8,160,128]{3,2,1,0:T(8,128)(2,1)S(1)} %all-to-all-done.1.got_ref, bf16[3,64,2048]{2,1,0:T(8,128)(2,1)S(1)} %constant_dynamic-update-slice_fusion.w0_ref, bf16[3,64,2048]{2,1,0:T(8,128)(2,1)S(1)} %collective-permute-done.w1_ref, ...), custom_call_target="tpu_custom_call" | custom-call | tf_op jit(solution)/shard_map/pallas_call | solution.py:321
  97.7 19.2 %all_to_all.30.part_ref = bf16[16,160,128]{2,1,0:T(8,128)(2,1)S(1)} all-to-all(bf16[16,160,128]{2,1,0:T(8,128)(2,1)} %get-tuple-element.28), channel_id=1, replica_groups=mesh['z'=16,'c'=2,'y'=4,'x'=4] {'y','x'}, dimensions={0} | all-to-all | bytes 1310720 | tf_op jit(solution)/shard_map/all_to_all | solution.py:22
  116.9 1.2 shard_map.174
  118.1 4.2 %collective-permute-start.6 = (bf16[320,128]{1,0:T(8,128)(2,1)}, bf16[320,128]{1,0:T(8,128)(2,1)S(1)}, u32[]{:S(2)}, u32[]{:S(2)}) collective-permute-start(bf16[320,128]{1,0:T(8,128)(2,1)} %get-tuple-element.30), channel_id=1, source_target_pairs={{16,0},{0,16},{17,1},{1,17},{18,2},{2,18},{19,3},{3,19},{20,4},{4,... | collective-permute-start | bytes 245768 | tf_op jit(solution)/shard_map/ppermute | solution.py:37
  122.3 1.1 collective-permute-done.6.other_ref
  123.4 0.9 copy-done.6
  125.0 3.5 %all-to-all-start.3 = ((bf16[16,40,128]{2,1,0:T(8,128)(2,1)}), bf16[16,40,128]{2,1,0:T(8,128)(2,1)S(1)}, u32[]{:S(2)}, u32[]{:S(2)}) async-start(bf16[16,40,128]{2,1,0:T(8,128)(2,1)} %shard_map.175), calls=%async_computation.3 | async-start | bytes 327680 | tf_op jit(solution)/shard_map/all_to_all | solution.py:22
  128.6 12.5 %all-to-all-done.3 = bf16[16,40,128]{2,1,0:T(8,128)(2,1)S(1)} async-done(((bf16[16,40,128]{2,1,0:T(8,128)(2,1)}), bf16[16,40,128]{2,1,0:T(8,128)(2,1)S(1)}, u32[]{:S(2)}, u32[]{:S(2)}) %all-to-all-start.3) | async-done | bytes 163872 | tf_op jit(solution)/shard_map/all_to_all | solution.py:22
  141.2 1.4 shard_map.176
  142.6 3.8 %all-to-all-start.4 = ((bf16[16,256,128]{2,1,0:T(8,128)(2,1)}), bf16[16,256,128]{2,1,0:T(8,128)(2,1)S(1)}, u32[]{:S(2)}, u32[]{:S(2)}) async-start(bf16[16,256,128]{2,1,0:T(8,128)(2,1)} %shard_map.176), calls=%async_computation.4 | async-start | bytes 2097152 | tf_op jit(solution)/shard_map/all_to_all | solution.py:22
  146.4 5.6 %collective-permute-start.7 = (bf16[64,128]{1,0:T(8,128)(2,1)S(1)}, bf16[64,128]{1,0:T(8,128)(2,1)S(1)}, u32[]{:S(2)}, u32[]{:S(2)}) collective-permute-start(bf16[64,128]{1,0:T(8,128)(2,1)S(1)} %bitcast.23), channel_id=1, source_target_pairs={{128,0},{160,32},{192,64},{224,96},{256,128},{288,160},{320,192},{... | collective-permute-start | bytes 49160 | tf_op jit(solution)/shard_map/ppermute | solution.py:37
  152.0 7.2 %collective-permute-start.8 = (bf16[64,128]{1,0:T(8,128)(2,1)S(1)}, bf16[64,128]{1,0:T(8,128)(2,1)S(1)}, u32[]{:S(2)}, u32[]{:S(2)}) collective-permute-start(bf16[64,128]{1,0:T(8,128)(2,1)S(1)} %bitcast.24), channel_id=1, source_target_pairs={{256,0},{288,32},{320,64},{352,96},{384,128},{416,160},{448,192},{... | collective-permute-start | bytes 49160 | tf_op jit(solution)/shard_map/ppermute | solution.py:37
  159.3 4.3 %collective-permute-start.9 = (bf16[64,128]{1,0:T(8,128)(2,1)S(1)}, bf16[64,128]{1,0:T(8,128)(2,1)S(1)}, u32[]{:S(2)}, u32[]{:S(2)}) collective-permute-start(bf16[64,128]{1,0:T(8,128)(2,1)S(1)} %bitcast.25), channel_id=1, source_target_pairs={{384,0},{416,32},{448,64},{480,96},{0,128},{32,160},{64,192},{96,2... | collective-permute-start | bytes 49160 | tf_op jit(solution)/shard_map/ppermute | solution.py:37
  163.6 4.3 %collective-permute-start.14 = (bf16[2,128]{1,0:T(2,128)(2,1)S(1)}, bf16[2,128]{1,0:T(2,128)(2,1)S(1)}, u32[]{:S(2)}, u32[]{:S(2)}) collective-permute-start(bf16[2,128]{1,0:T(2,128)(2,1)S(1)} %slice.104), channel_id=1, source_target_pairs={{0,16},{16,32},{32,48},{48,64},{64,80},{80,96},{96,112},{112,128},... | collective-permute-start | bytes 1544 | tf_op jit(solution)/shard_map/ppermute | solution.py:49
  168.0 5.7 %collective-permute-start.10 = (bf16[4,64,128]{2,1,0:T(8,128)(2,1)S(1)}, bf16[4,64,128]{2,1,0:T(8,128)(2,1)S(1)}, u32[]{:S(2)}, u32[]{:S(2)}) collective-permute-start(bf16[4,64,128]{2,1,0:T(8,128)(2,1)S(1)} %shard_map.177.refs_0_), channel_id=1, source_target_pairs={{32,0},{64,32},{96,64},{0,96},{160,128},{192,160},{224,192},{128,2... | collective-permute-start | bytes 196616 | tf_op jit(solution)/shard_map/ppermute | solution.py:37
  173.7 1.9 collective-permute-start.11
  175.6 2.2 collective-permute-start.12
  177.8 1.7 collective-permute-done.11.refs_2_
  179.6 2.8 %collective-permute-done.12.refs_3_ = bf16[4,64,128]{2,1,0:T(8,128)(2,1)S(1)} collective-permute-done((bf16[4,64,128]{2,1,0:T(8,128)(2,1)S(1)}, bf16[4,64,128]{2,1,0:T(8,128)(2,1)S(1)}, u32[]{:S(2)}, u32[]{:S(2)}) %collective-permute-start.12) | collective-permute-done | bytes 65568 | tf_op jit(solution)/shard_map/ppermute | solution.py:37
  182.4 5.3 %collective-permute-start.13 = (bf16[4,4,64,128]{3,2,1,0:T(8,128)(2,1)S(1)}, bf16[4,4,64,128]{3,2,1,0:T(8,128)(2,1)S(1)}, u32[]{:S(2)}, u32[]{:S(2)}) collective-permute-start(bf16[4,4,64,128]{3,2,1,0:T(8,128)(2,1)S(1)} %shard_map.178.own_ref), channel_id=1, source_target_pairs={{16,0},{0,16},{17,1},{1,17},{18,2},{2,18},{19,3},{3,19},{20,4},{4,... | collective-permute-start | bytes 786440 | tf_op jit(solution)/shard_map/ppermute | solution.py:37
  187.8 2.6 %shard_map.173 = (bf16[3,64,2048]{2,1,0:T(8,128)(2,1)}, bf16[3,64,2048]{2,1,0:T(8,128)(2,1)}, bf16[3,64,2048]{2,1,0:T(8,128)(2,1)}, bf16[3,64,2048]{2,1,0:T(8,128)(2,1)}) custom-call(bf16[4,8,160,128]{3,2,1,0:T(8,128)(2,1)S(1)} %all-to-all-done.1.got_ref, bf16[3,160,256]{2,1,0:T(8,128)(2,1)S(1)} %copy-done.5), custom_call_target="tpu_custom_call" | custom-call | tf_op jit(solution)/shard_map/pallas_call | solution.py:321
  190.4 3.4 %collective-permute-start.5 = (bf16[3,64,2048]{2,1,0:T(8,128)(2,1)}, bf16[3,64,2048]{2,1,0:T(8,128)(2,1)}, u32[]{:S(2)}, u32[]{:S(2)}) collective-permute-start(bf16[3,64,2048]{2,1,0:T(8,128)(2,1)} %get-tuple-element.26), channel_id=1, source_target_pairs={{0,1},{1,2},{2,3},{3,0},{4,5},{5,6},{6,7},{7,4},{8,9},{9,10},{10,1... | collective-permute-start | bytes 2359304 | tf_op jit(solution)/shard_map/ppermute | solution.py:27
  193.8 4.3 %collective-permute-start.4 = (bf16[3,64,2048]{2,1,0:T(8,128)(2,1)}, bf16[3,64,2048]{2,1,0:T(8,128)(2,1)}, u32[]{:S(2)}, u32[]{:S(2)}) collective-permute-start(bf16[3,64,2048]{2,1,0:T(8,128)(2,1)} %get-tuple-element.25), channel_id=1, source_target_pairs={{0,2},{1,3},{2,0},{3,1},{4,6},{5,7},{6,4},{7,5},{8,10},{9,11},{10,... | collective-permute-start | bytes 2359304 | tf_op jit(solution)/shard_map/ppermute | solution.py:27
  198.1 3.1 %collective-permute-start.3 = (bf16[3,64,2048]{2,1,0:T(8,128)(2,1)}, bf16[3,64,2048]{2,1,0:T(8,128)(2,1)}, u32[]{:S(2)}, u32[]{:S(2)}) collective-permute-start(bf16[3,64,2048]{2,1,0:T(8,128)(2,1)} %get-tuple-element.24), channel_id=1, source_target_pairs={{0,3},{1,0},{2,1},{3,2},{4,7},{5,4},{6,5},{7,6},{8,11},{9,8},{10,9... | collective-permute-start | bytes 2359304 | tf_op jit(solution)/shard_map/ppermute | solution.py:27
  201.3 0.7 multiply_convert_fusion
  202.0 2.6 %mixer.1 = (bf16[16,64,128]{2,1,0:T(8,128)(2,1)S(1)}, bf16[16,64,128]{2,1,0:T(8,128)(2,1)}, bf16[256,128]{1,0:T(8,128)(2,1)}, bf16[256,128]{1,0:T(8,128)(2,1)}) custom-call(s32[1]{0:T(128)} %bitcast.2.core_ref.place_ref, bf16[16,256,128]{2,1,0:T(8,128)(2,1)S(1)} %all-to-all-done.4.full_ref, bf16[256,2048]{1,0:T(8,128)(2,1)S(1)} %copy-done, ...), custom_call_target="tpu_custom_call" | custom-call | tf_op jit(solution)/shard_map/mixer/pallas_call | solution.py:298
  204.7 2.9 %collective-permute-start.15 = (bf16[16,64,128]{2,1,0:T(8,128)(2,1)}, bf16[16,64,128]{2,1,0:T(8,128)(2,1)S(1)}, u32[]{:S(2)}, u32[]{:S(2)}) collective-permute-start(bf16[16,64,128]{2,1,0:T(8,128)(2,1)} %get-tuple-element.32), channel_id=1, source_target_pairs={{16,0},{0,16},{17,1},{1,17},{18,2},{2,18},{19,3},{3,19},{20,4},{4,... | collective-permute-start | bytes 786440 | tf_op jit(solution)/shard_map/ppermute | solution.py:37
  208.3 1.9 collective-permute-start.16
  210.2 0.8 add_convert_fusion
  211.0 7.6 %all-to-all-start.5 = ((bf16[16,64,128]{2,1,0:T(8,128)(2,1)}), bf16[16,64,128]{2,1,0:T(8,128)(2,1)S(1)}, u32[]{:S(2)}, u32[]{:S(2)}) async-start(bf16[16,64,128]{2,1,0:T(8,128)(2,1)} %add_convert_fusion), calls=%async_computation.5 | async-start | bytes 524288 | tf_op jit(solution)/shard_map/all_to_all | solution.py:22
  218.6 12.3 %collective-permute-done.4 = bf16[3,64,2048]{2,1,0:T(8,128)(2,1)} collective-permute-done((bf16[3,64,2048]{2,1,0:T(8,128)(2,1)}, bf16[3,64,2048]{2,1,0:T(8,128)(2,1)}, u32[]{:S(2)}, u32[]{:S(2)}) %collective-permute-start.4) | collective-permute-done | bytes 786464 | tf_op jit(solution)/shard_map/ppermute | solution.py:27
  231.0 1.2 collective-permute-done.3
  232.1 2.9 %add_convert_fusion.1 = (bf16[1,64,2048]{2,1,0:T(8,128)(2,1)}, bf16[1,64,2048]{2,1,0:T(8,128)(2,1)}, bf16[1,64,2048]{2,1,0:T(8,128)(2,1)}) fusion(bf16[3,64,2048]{2,1,0:T(8,128)(2,1)} %collective-permute-done.5, bf16[3,64,2048]{2,1,0:T(8,128)(2,1)} %collective-permute-done.4, bf16[3,64,2048]{2,1,0:T(8,128)(2,1)} %collective-permute-done.3, ...), kind=kLoop, calls=%fused_computation.2 | loop fusion | flops 3145728 | bytes 3932160 | tf_op jit(solution)/shard_map/convert_element_type | solution.py:400
  (60 shorter events, 3.8 us)
Async XLA Ops:
  0.6 19.1 %copy-start.11 = (bf16[1,64,2048]{2,1,0:T(8,128)(2,1)S(1)}, bf16[1,64,2048]{2,1,0:T(8,128)(2,1)}, u32[]{:S(2)}) copy-start(bf16[1,64,2048]{2,1,0:T(8,128)(2,1)} %param.16) | copy-start | bytes 786436
  0.7 19.1 %copy-start.12 = (bf16[1,64,2048]{2,1,0:T(8,128)(2,1)S(1)}, bf16[1,64,2048]{2,1,0:T(8,128)(2,1)}, u32[]{:S(2)}) copy-start(bf16[1,64,2048]{2,1,0:T(8,128)(2,1)} %param.17) | copy-start | bytes 786436
  2.9 41.7 %all-to-all-start = ((bf16[32,40,128]{2,1,0:T(8,128)(2,1)}), bf16[32,40,128]{2,1,0:T(8,128)(2,1)S(1)}, u32[]{:S(2)}, u32[]{:S(2)}) async-start(bf16[32,40,128]{2,1,0:T(8,128)(2,1)} %bitcast.27), calls=%async_computation | async-start | bytes 655360 | tf_op jit(solution)/shard_map/all_to_all | solution.py:22
  46.2 4.3 %copy-start.13 = (bf16[1,64,2048]{2,1,0:T(8,128)(2,1)S(1)}, bf16[1,64,2048]{2,1,0:T(8,128)(2,1)}, u32[]{:S(2)}) copy-start(bf16[1,64,2048]{2,1,0:T(8,128)(2,1)} %param.18) | copy-start | bytes 786436
  46.2 46.1 %all-to-all-start.1 = ((bf16[4,8,160,128]{3,2,1,0:T(8,128)(2,1)}), bf16[4,8,160,128]{3,2,1,0:T(8,128)(2,1)S(1)}, u32[]{:S(2)}, u32[]{:S(2)}) async-start(bf16[4,8,160,128]{3,2,1,0:T(8,128)(2,1)} %shard_map.171), calls=%async_computation.1 | async-start | bytes 2621440 | tf_op jit(solution)/shard_map/all_to_all | solution.py:22
  50.5 21.2 %collective-permute-start = (bf16[3,64,2048]{2,1,0:T(8,128)(2,1)S(1)}, bf16[3,64,2048]{2,1,0:T(8,128)(2,1)S(1)}, u32[]{:S(2)}, u32[]{:S(2)}) collective-permute-start(bf16[3,64,2048]{2,1,0:T(8,128)(2,1)S(1)} %constant_dynamic-update-slice_fusion.w0_ref), channel_id=1, source_target_pairs={{0,1},{1,2},{2,3},{3,0},{4,5},{5,6},{6,7},{7,4},{8,9},{9,10},{10,1... | collective-permute-start | bytes 2359304 | tf_op jit(solution)/shard_map/ppermute | solution.py:27
  53.6 35.9 %collective-permute-start.1 = (bf16[3,64,2048]{2,1,0:T(8,128)(2,1)S(1)}, bf16[3,64,2048]{2,1,0:T(8,128)(2,1)S(1)}, u32[]{:S(2)}, u32[]{:S(2)}) collective-permute-start(bf16[3,64,2048]{2,1,0:T(8,128)(2,1)S(1)} %constant_dynamic-update-slice_fusion.w0_ref), channel_id=1, source_target_pairs={{0,2},{1,3},{2,0},{3,1},{4,6},{5,7},{6,4},{7,5},{8,10},{9,11},{10,... | collective-permute-start | bytes 2359304 | tf_op jit(solution)/shard_map/ppermute | solution.py:27
  58.0 33.4 %collective-permute-start.2 = (bf16[3,64,2048]{2,1,0:T(8,128)(2,1)S(1)}, bf16[3,64,2048]{2,1,0:T(8,128)(2,1)S(1)}, u32[]{:S(2)}, u32[]{:S(2)}) collective-permute-start(bf16[3,64,2048]{2,1,0:T(8,128)(2,1)S(1)} %constant_dynamic-update-slice_fusion.w0_ref), channel_id=1, source_target_pairs={{0,3},{1,0},{2,1},{3,2},{4,7},{5,4},{6,5},{7,6},{8,11},{9,8},{10,9... | collective-permute-start | bytes 2359304 | tf_op jit(solution)/shard_map/ppermute | solution.py:27
  89.5 0.9 copy-start.1
  91.4 0.9 copy-start.3
  92.3 1.1 copy-start.2
  93.4 1.1 copy-start.4
  97.6 30.9 %copy-start.16 = (s32[2,256]{1,0:T(2,128)S(1)}, s32[2,256]{1,0:T(2,128)}, u32[]{:S(2)}) copy-start(s32[2,256]{1,0:T(2,128)} %get-tuple-element.27) | copy-start | bytes 6148
  118.1 5.3 %collective-permute-start.6 = (bf16[320,128]{1,0:T(8,128)(2,1)}, bf16[320,128]{1,0:T(8,128)(2,1)S(1)}, u32[]{:S(2)}, u32[]{:S(2)}) collective-permute-start(bf16[320,128]{1,0:T(8,128)(2,1)} %get-tuple-element.30), channel_id=1, source_target_pairs={{16,0},{0,16},{17,1},{1,17},{18,2},{2,18},{19,3},{3,19},{20,4},{4,... | collective-permute-start | bytes 245768 | tf_op jit(solution)/shard_map/ppermute | solution.py:37
  123.4 0.9 copy-start.6
  125.0 16.2 %all-to-all-start.3 = ((bf16[16,40,128]{2,1,0:T(8,128)(2,1)}), bf16[16,40,128]{2,1,0:T(8,128)(2,1)S(1)}, u32[]{:S(2)}, u32[]{:S(2)}) async-start(bf16[16,40,128]{2,1,0:T(8,128)(2,1)} %shard_map.175), calls=%async_computation.3 | async-start | bytes 327680 | tf_op jit(solution)/shard_map/all_to_all | solution.py:22
  142.6 3.8 %copy-start.7 = (bf16[128,64]{0,1:T(8,128)(2,1)S(1)}, bf16[128,64]{0,1:T(8,128)(2,1)}, u32[]{:S(2)}) copy-start(bf16[128,64]{0,1:T(8,128)(2,1)} %param.23) | copy-start | bytes 49156
  142.6 21.0 %copy-start.10 = (bf16[256,128]{1,0:T(8,128)(2,1)S(1)}, bf16[256,128]{1,0:T(8,128)(2,1)}, u32[]{:S(2)}) copy-start(bf16[256,128]{1,0:T(8,128)(2,1)} %param.20) | copy-start | bytes 196612
  142.6 21.0 %copy-start.14 = (bf16[256,128]{1,0:T(8,128)(2,1)S(1)}, bf16[256,128]{1,0:T(8,128)(2,1)}, u32[]{:S(2)}) copy-start(bf16[256,128]{1,0:T(8,128)(2,1)} %param.21) | copy-start | bytes 196612
  142.6 35.2 %copy-start.17 = (f32[3,128]{1,0:T(4,128)S(1)}, f32[3,128]{1,0:T(4,128)}, u32[]{:S(2)}) copy-start(f32[3,128]{1,0:T(4,128)} %param.22) | copy-start | bytes 4612
  142.6 45.2 %copy-start.5 = (bf16[3,160,256]{2,1,0:T(8,128)(2,1)S(1)}, bf16[3,160,256]{2,1,0:T(8,128)(2,1)}, u32[]{:S(2)}) copy-start(bf16[3,160,256]{2,1,0:T(8,128)(2,1)} %get-tuple-element.22.cots_ref) | copy-start | bytes 737284
  142.6 59.4 %all-to-all-start.4 = ((bf16[16,256,128]{2,1,0:T(8,128)(2,1)}), bf16[16,256,128]{2,1,0:T(8,128)(2,1)S(1)}, u32[]{:S(2)}, u32[]{:S(2)}) async-start(bf16[16,256,128]{2,1,0:T(8,128)(2,1)} %shard_map.176), calls=%async_computation.4 | async-start | bytes 2097152 | tf_op jit(solution)/shard_map/all_to_all | solution.py:22
  146.4 54.8 %copy-start.9 = (bf16[256,128]{1,0:T(8,128)(2,1)S(1)}, bf16[256,128]{1,0:T(8,128)(2,1)}, u32[]{:S(2)}) copy-start(bf16[256,128]{1,0:T(8,128)(2,1)} %outer_hbm.1) | copy-start | bytes 196612
  146.4 21.5 %collective-permute-start.7 = (bf16[64,128]{1,0:T(8,128)(2,1)S(1)}, bf16[64,128]{1,0:T(8,128)(2,1)S(1)}, u32[]{:S(2)}, u32[]{:S(2)}) collective-permute-start(bf16[64,128]{1,0:T(8,128)(2,1)S(1)} %bitcast.23), channel_id=1, source_target_pairs={{128,0},{160,32},{192,64},{224,96},{256,128},{288,160},{320,192},{... | collective-permute-start | bytes 49160 | tf_op jit(solution)/shard_map/ppermute | solution.py:37
  152.0 15.9 %collective-permute-start.8 = (bf16[64,128]{1,0:T(8,128)(2,1)S(1)}, bf16[64,128]{1,0:T(8,128)(2,1)S(1)}, u32[]{:S(2)}, u32[]{:S(2)}) collective-permute-start(bf16[64,128]{1,0:T(8,128)(2,1)S(1)} %bitcast.24), channel_id=1, source_target_pairs={{256,0},{288,32},{320,64},{352,96},{384,128},{416,160},{448,192},{... | collective-permute-start | bytes 49160 | tf_op jit(solution)/shard_map/ppermute | solution.py:37
  159.3 8.7 %collective-permute-start.9 = (bf16[64,128]{1,0:T(8,128)(2,1)S(1)}, bf16[64,128]{1,0:T(8,128)(2,1)S(1)}, u32[]{:S(2)}, u32[]{:S(2)}) collective-permute-start(bf16[64,128]{1,0:T(8,128)(2,1)S(1)} %bitcast.25), channel_id=1, source_target_pairs={{384,0},{416,32},{448,64},{480,96},{0,128},{32,160},{64,192},{96,2... | collective-permute-start | bytes 49160 | tf_op jit(solution)/shard_map/ppermute | solution.py:37
  163.6 37.6 %collective-permute-start.14 = (bf16[2,128]{1,0:T(2,128)(2,1)S(1)}, bf16[2,128]{1,0:T(2,128)(2,1)S(1)}, u32[]{:S(2)}, u32[]{:S(2)}) collective-permute-start(bf16[2,128]{1,0:T(2,128)(2,1)S(1)} %slice.104), channel_id=1, source_target_pairs={{0,16},{16,32},{32,48},{48,64},{64,80},{80,96},{96,112},{112,128},... | collective-permute-start | bytes 1544 | tf_op jit(solution)/shard_map/ppermute | solution.py:49
  168.0 9.9 %collective-permute-start.10 = (bf16[4,64,128]{2,1,0:T(8,128)(2,1)S(1)}, bf16[4,64,128]{2,1,0:T(8,128)(2,1)S(1)}, u32[]{:S(2)}, u32[]{:S(2)}) collective-permute-start(bf16[4,64,128]{2,1,0:T(8,128)(2,1)S(1)} %shard_map.177.refs_0_), channel_id=1, source_target_pairs={{32,0},{64,32},{96,64},{0,96},{160,128},{192,160},{224,192},{128,2... | collective-permute-start | bytes 196616 | tf_op jit(solution)/shard_map/ppermute | solution.py:37
  173.7 5.9 %collective-permute-start.11 = (bf16[4,64,128]{2,1,0:T(8,128)(2,1)S(1)}, bf16[4,64,128]{2,1,0:T(8,128)(2,1)S(1)}, u32[]{:S(2)}, u32[]{:S(2)}) collective-permute-start(bf16[4,64,128]{2,1,0:T(8,128)(2,1)S(1)} %shard_map.177.refs_0_), channel_id=1, source_target_pairs={{64,0},{96,32},{0,64},{32,96},{192,128},{224,160},{128,192},{160,2... | collective-permute-start | bytes 196616 | tf_op jit(solution)/shard_map/ppermute | solution.py:37
  175.6 6.8 %collective-permute-start.12 = (bf16[4,64,128]{2,1,0:T(8,128)(2,1)S(1)}, bf16[4,64,128]{2,1,0:T(8,128)(2,1)S(1)}, u32[]{:S(2)}, u32[]{:S(2)}) collective-permute-start(bf16[4,64,128]{2,1,0:T(8,128)(2,1)S(1)} %shard_map.177.refs_0_), channel_id=1, source_target_pairs={{96,0},{0,32},{32,64},{64,96},{224,128},{128,160},{160,192},{192,2... | collective-permute-start | bytes 196616 | tf_op jit(solution)/shard_map/ppermute | solution.py:37
  182.4 19.5 %collective-permute-start.13 = (bf16[4,4,64,128]{3,2,1,0:T(8,128)(2,1)S(1)}, bf16[4,4,64,128]{3,2,1,0:T(8,128)(2,1)S(1)}, u32[]{:S(2)}, u32[]{:S(2)}) collective-permute-start(bf16[4,4,64,128]{3,2,1,0:T(8,128)(2,1)S(1)} %shard_map.178.own_ref), channel_id=1, source_target_pairs={{16,0},{0,16},{17,1},{1,17},{18,2},{2,18},{19,3},{3,19},{20,4},{4,... | collective-permute-start | bytes 786440 | tf_op jit(solution)/shard_map/ppermute | solution.py:37
  190.4 11.6 %copy-start = (bf16[256,2048]{1,0:T(8,128)(2,1)S(1)}, bf16[256,2048]{1,0:T(8,128)(2,1)}, u32[]{:S(2)}) copy-start(bf16[256,2048]{1,0:T(8,128)(2,1)} %out_grad_ref.1) | copy-start | bytes 3145732
  190.4 28.2 %collective-permute-start.5 = (bf16[3,64,2048]{2,1,0:T(8,128)(2,1)}, bf16[3,64,2048]{2,1,0:T(8,128)(2,1)}, u32[]{:S(2)}, u32[]{:S(2)}) collective-permute-start(bf16[3,64,2048]{2,1,0:T(8,128)(2,1)} %get-tuple-element.26), channel_id=1, source_target_pairs={{0,1},{1,2},{2,3},{3,0},{4,5},{5,6},{6,7},{7,4},{8,9},{9,10},{10,1... | collective-permute-start | bytes 2359304 | tf_op jit(solution)/shard_map/ppermute | solution.py:27
  193.8 37.2 %collective-permute-start.4 = (bf16[3,64,2048]{2,1,0:T(8,128)(2,1)}, bf16[3,64,2048]{2,1,0:T(8,128)(2,1)}, u32[]{:S(2)}, u32[]{:S(2)}) collective-permute-start(bf16[3,64,2048]{2,1,0:T(8,128)(2,1)} %get-tuple-element.25), channel_id=1, source_target_pairs={{0,2},{1,3},{2,0},{3,1},{4,6},{5,7},{6,4},{7,5},{8,10},{9,11},{10,... | collective-permute-start | bytes 2359304 | tf_op jit(solution)/shard_map/ppermute | solution.py:27
  198.1 34.0 %collective-permute-start.3 = (bf16[3,64,2048]{2,1,0:T(8,128)(2,1)}, bf16[3,64,2048]{2,1,0:T(8,128)(2,1)}, u32[]{:S(2)}, u32[]{:S(2)}) collective-permute-start(bf16[3,64,2048]{2,1,0:T(8,128)(2,1)} %get-tuple-element.24), channel_id=1, source_target_pairs={{0,3},{1,0},{2,1},{3,2},{4,7},{5,4},{6,5},{7,6},{8,11},{9,8},{10,9... | collective-permute-start | bytes 2359304 | tf_op jit(solution)/shard_map/ppermute | solution.py:27
  204.7 27.5 %copy-start.8 = (bf16[3,64,2048]{2,1,0:T(8,128)(2,1)S(1)}, bf16[3,64,2048]{2,1,0:T(8,128)(2,1)}, u32[]{:S(2)}) copy-start(bf16[3,64,2048]{2,1,0:T(8,128)(2,1)} %get-tuple-element.23) | copy-start | bytes 2359300
  204.7 5.5 %collective-permute-start.15 = (bf16[16,64,128]{2,1,0:T(8,128)(2,1)}, bf16[16,64,128]{2,1,0:T(8,128)(2,1)S(1)}, u32[]{:S(2)}, u32[]{:S(2)}) collective-permute-start(bf16[16,64,128]{2,1,0:T(8,128)(2,1)} %get-tuple-element.32), channel_id=1, source_target_pairs={{16,0},{0,16},{17,1},{1,17},{18,2},{2,18},{19,3},{3,19},{20,4},{4,... | collective-permute-start | bytes 786440 | tf_op jit(solution)/shard_map/ppermute | solution.py:37
  208.3 26.7 %collective-permute-start.16 = (bf16[2,128]{1,0:T(2,128)(2,1)S(1)}, bf16[2,128]{1,0:T(2,128)(2,1)S(1)}, u32[]{:S(2)}, u32[]{:S(2)}) collective-permute-start(bf16[2,128]{1,0:T(2,128)(2,1)S(1)} %slice.91), channel_id=1, source_target_pairs={{16,0},{32,16},{48,32},{64,48},{80,64},{96,80},{112,96},{128,112},... | collective-permute-start | bytes 1544 | tf_op jit(solution)/shard_map/ppermute | solution.py:49
  211.0 25.4 %all-to-all-start.5 = ((bf16[16,64,128]{2,1,0:T(8,128)(2,1)}), bf16[16,64,128]{2,1,0:T(8,128)(2,1)S(1)}, u32[]{:S(2)}, u32[]{:S(2)}) async-start(bf16[16,64,128]{2,1,0:T(8,128)(2,1)} %add_convert_fusion), calls=%async_computation.5 | async-start | bytes 524288 | tf_op jit(solution)/shard_map/all_to_all | solution.py:22
  232.1 2.9 %copy-start.15 = (bf16[256,128]{1,0:T(8,128)(2,1)S(1)}, bf16[256,128]{1,0:T(8,128)(2,1)}, u32[]{:S(2)}) copy-start(bf16[256,128]{1,0:T(8,128)(2,1)} %get-tuple-element.34) | copy-start | bytes 196612

commit v7 on v5

--- a/solution.py
+++ b/solution.py
@@ -200,12 +200,12 @@
 
 
 def mixer_kernel(
-    full_ref, out_grad_ref, proj_ref, mixed_hbm, convolved_hbm, outer_hbm,
-    terms_ref, cot_ref, outer_grad_hbm,
+    core_ref, full_ref, out_grad_ref, proj_ref, mixed_hbm, convolved_hbm, outer_hbm,
+    keep_ref, give_ref, cot_ref, outer_grad_hbm,
     mixed_ref, convolved_ref, outer_ref, outer_grad_ref, sems,
 ):
     n_tp, _, _ = full_ref.shape
-    n_c, n_z, per, _ = terms_ref.shape
+    n_z, per, _ = keep_ref.shape
     fetches = [
         pltpu.make_async_copy(src, dst, sems.at[i])
         for i, (src, dst) in enumerate(
@@ -225,10 +225,12 @@
     cot_ref[...] = (mixed_grad * outer_ref[...].astype(F32)).astype(BF)
     fetches[2].wait()
     terms = dot(stream, mixed_ref[...], 0, 0).astype(BF)
+    lower = core_ref[0] == 0
     for z in range(n_z):
-        for c in range(n_c):
-            at = (z * n_c + c) * per
-            terms_ref[c, z] = terms[at : at + per]
+        low = terms[2 * z * per : (2 * z + 1) * per]
+        high = terms[(2 * z + 1) * per : (2 * z + 2) * per]
+        keep_ref[z] = jnp.where(lower, low, high)
+        give_ref[z] = jnp.where(lower, high, low)
     keep.wait()
 
 
@@ -274,17 +276,19 @@
     return pltpu.with_memory_space_constraint(value, pltpu.HBM)
 
 
-def mix(full, out_grad, proj, mixed, convolved, outer_gate, n_c, n_z):
+def mix(core, full, out_grad, proj, mixed, convolved, outer_gate, n_c, n_z):
     _, tokens, lanes = full.shape
     small = (tokens, lanes)
     whole = pl.BlockSpec(memory_space=pltpu.VMEM)
     away = pl.BlockSpec(memory_space=pltpu.HBM)
+    half = (n_z, proj.shape[0] // (n_c * n_z), lanes)
     return pl.pallas_call(
         mixer_kernel,
-        in_specs=[whole, whole, whole, away, away, away],
-        out_specs=[whole, whole, away],
+        in_specs=[pl.BlockSpec(memory_space=pltpu.SMEM)] + [whole] * 3 + [away] * 3,
+        out_specs=[whole, whole, whole, away],
         out_shape=[
-            pltpu.HBM((n_c, n_z, proj.shape[0] // (n_c * n_z), lanes), BF),
+            jax.ShapeDtypeStruct(half, BF),
+            pltpu.HBM(half, BF),
             pltpu.HBM(small, BF),
             pltpu.HBM(small, BF),
         ],
@@ -297,7 +301,7 @@
         ],
         compiler_params=pltpu.CompilerParams(vmem_limit_bytes=16 << 20),
         name="mixer",
-    )(full, out_grad, proj, *map(in_hbm, (mixed, convolved, outer_gate)))
+    )(core[None], full, out_grad, proj, *map(in_hbm, (mixed, convolved, outer_gate)))
 
 
 def on_core(kernel, outs, *args, mib=12, **static):
@@ -393,12 +397,13 @@
     proj = grouped(out_proj.T, "z", n_z // inner, inner)
     proj = grouped(proj, "z", inner, 1)
     twin = shifted(proj, "c", n_c, 1, 1)
-    proj = with_twin(proj, twin, lax.axis_index("c")).reshape(width, wdev)
-    pair, conv_cot, outer_gate_grad = mix(
-        full, out_grad, proj, mixed, convolved, outer_gate, n_c, n_z
-    )
-    terms = swap(pair, "c")
-    terms = jnp.sum(terms.astype(F32), axis=0).astype(BF)
+    core = lax.axis_index("c")
+    proj = with_twin(proj, twin, core).reshape(width, wdev)
+    keep, give, conv_cot, outer_gate_grad = mix(
+        core, full, out_grad, proj, mixed, convolved, outer_gate, n_c, n_z
+    )
+    given = shifted(give, "c", n_c, 1, 1)
+    terms = (keep.astype(F32) + given.astype(F32)).astype(BF)
     out_proj_grad = jnp.sum(swap(terms, "z").astype(F32), axis=0)
 
     later_rows = from_behind(conv_cot[: taps - 1], SP, -1)

time: 236 us -> 236 us (level); the launches traced: 231 us -> 234 us
  waiting for transfers between devices: 88 us -> 93.8 us
  blocking collectives: 24.6 us -> 19.2 us
    ppermute x6, waiting for transfers between devices: 29.4 us -> 43.5 us  [turned(): lax.ppermute(value, axis, [(i, (i + by) % count) for i in range(count)])]
    ppermute x2, waiting for transfers between devices: 7.4 us -> 0.01 us  [from_behind(): return lax.ppermute(value, axis, pairs)]
    all_to_all x2 -> x1, blocking collectives: 24.6 us -> 19.2 us  [swap(): return lax.all_to_all(blocks, axis, split_axis=0, concat_axis=0, tiled=True)]
    ppermute x7 -> x8, starting transfers between devices: 23.6 us -> 28.4 us  [shifted(): return lax.ppermute(value, axis, [(source(i), i) for i in range(count)])]
    ppermute x2, starting transfers between devices: 9.41 us -> 6.13 us  [from_behind(): return lax.ppermute(value, axis, pairs)]
    ppermute x7 -> x8, waiting for transfers between devices: 7.45 us -> 6.49 us  [shifted(): return lax.ppermute(value, axis, [(source(i), i) for i in range(count)])]
  transfers between devices with their start and end apart: 20 -> 21, of which waited for: 10 -> 10; matrix products, arithmetic and copies ran while one was open for 3% -> 3% of each run, Pallas kernels for 2% -> 2%
where the time goes in v7:
time: 236 us; the launch traced here: 234 us
  waiting for transfers between devices  93.8 us (40%)
  starting transfers between devices  93.7 us (40%)
  blocking collectives  19.2 us (8%)
  Pallas kernels  15.1 us (6%)
  other arithmetic  6.41 us (3%)
  local copies, waits for them, and re-layouts  5.01 us (2%)
    all_to_all x5, waiting for transfers between devices, swap(): return lax.all_to_all(blocks, axis, split_axis=0, concat_axis=0, tiled=True)  43.7 us
    ppermute x6, waiting for transfers between devices, turned(): lax.ppermute(value, axis, [(i, (i + by) % count) for i in range(count)])  43.5 us
    all_to_all x5, starting transfers between devices, swap(): return lax.all_to_all(blocks, axis, split_axis=0, concat_axis=0, tiled=True)  37.7 us
    ppermute x8, starting transfers between devices, shifted(): return lax.ppermute(value, axis, [(source(i), i) for i in range(count)])  28.4 us
    ppermute x6, starting transfers between devices, turned(): lax.ppermute(value, axis, [(i, (i + by) % count) for i in range(count)])  21.5 us
    all_to_all x1, blocking collectives, swap(): return lax.all_to_all(blocks, axis, split_axis=0, concat_axis=0, tiled=True)  19.2 us
    pallas_call x5, Pallas kernels, on_core(): pl.pallas_call(functools.partial(kernel, **static) if static else kernel,...  10.1 us
    ppermute x8, waiting for transfers between devices, shifted(): return lax.ppermute(value, axis, [(source(i), i) for i in range(count)])  6.49 us
  transfers between devices with their start and end apart: 21, of which 10 were waited for; matrix products, arithmetic and copies ran while one was open for 3% of the time, Pallas kernels for 2%

profile of v7, /device:TPU:1, one launch (start us, length us, event | category | flops | bytes accessed | tf_op | source)
XLA Modules:
  0.0 234.3 jit_solution(10022990519876035986)
XLA Ops:
  0.7 2.3 route.1
  3.0 16.7 %all-to-all-start = ((bf16[32,40,128]{2,1,0:T(8,128)(2,1)}), bf16[32,40,128]{2,1,0:T(8,128)(2,1)S(1)}, u32[]{:S(2)}, u32[]{:S(2)}) async-start(bf16[32,40,128]{2,1,0:T(8,128)(2,1)} %bitcast.29), calls=%async_computation | async-start | bytes 655360 | tf_op jit(solution)/shard_map/all_to_all | solution.py:22
  19.8 24.9 %all-to-all-done = bf16[32,40,128]{2,1,0:T(8,128)(2,1)S(1)} async-done(((bf16[32,40,128]{2,1,0:T(8,128)(2,1)}), bf16[32,40,128]{2,1,0:T(8,128)(2,1)S(1)}, u32[]{:S(2)}, u32[]{:S(2)}) %all-to-all-start) | async-done | bytes 327712 | tf_op jit(solution)/shard_map/all_to_all | solution.py:22
  44.7 1.5 shard_map.171
  46.2 4.3 %all-to-all-start.1 = ((bf16[4,8,160,128]{3,2,1,0:T(8,128)(2,1)}), bf16[4,8,160,128]{3,2,1,0:T(8,128)(2,1)S(1)}, u32[]{:S(2)}, u32[]{:S(2)}) async-start(bf16[4,8,160,128]{3,2,1,0:T(8,128)(2,1)} %shard_map.171), calls=%async_computation.1 | async-start | bytes 2621440 | tf_op jit(solution)/shard_map/all_to_all | solution.py:22
  50.5 3.1 %collective-permute-start = (bf16[3,64,2048]{2,1,0:T(8,128)(2,1)S(1)}, bf16[3,64,2048]{2,1,0:T(8,128)(2,1)S(1)}, u32[]{:S(2)}, u32[]{:S(2)}) collective-permute-start(bf16[3,64,2048]{2,1,0:T(8,128)(2,1)S(1)} %constant_dynamic-update-slice_fusion.w0_ref), channel_id=1, source_target_pairs={{0,1},{1,2},{2,3},{3,0},{4,5},{5,6},{6,7},{7,4},{8,9},{9,10},{10,1... | collective-permute-start | bytes 2359304 | tf_op jit(solution)/shard_map/ppermute | solution.py:27
  53.6 4.4 %collective-permute-start.1 = (bf16[3,64,2048]{2,1,0:T(8,128)(2,1)S(1)}, bf16[3,64,2048]{2,1,0:T(8,128)(2,1)S(1)}, u32[]{:S(2)}, u32[]{:S(2)}) collective-permute-start(bf16[3,64,2048]{2,1,0:T(8,128)(2,1)S(1)} %constant_dynamic-update-slice_fusion.w0_ref), channel_id=1, source_target_pairs={{0,2},{1,3},{2,0},{3,1},{4,6},{5,7},{6,4},{7,5},{8,10},{9,11},{10,... | collective-permute-start | bytes 2359304 | tf_op jit(solution)/shard_map/ppermute | solution.py:27
  58.0 3.1 %collective-permute-start.2 = (bf16[3,64,2048]{2,1,0:T(8,128)(2,1)S(1)}, bf16[3,64,2048]{2,1,0:T(8,128)(2,1)S(1)}, u32[]{:S(2)}, u32[]{:S(2)}) collective-permute-start(bf16[3,64,2048]{2,1,0:T(8,128)(2,1)S(1)} %constant_dynamic-update-slice_fusion.w0_ref), channel_id=1, source_target_pairs={{0,3},{1,0},{2,1},{3,2},{4,7},{5,4},{6,5},{7,6},{8,11},{9,8},{10,9... | collective-permute-start | bytes 2359304 | tf_op jit(solution)/shard_map/ppermute | solution.py:27
  61.1 10.7 %collective-permute-done.w1_ref = bf16[3,64,2048]{2,1,0:T(8,128)(2,1)S(1)} collective-permute-done((bf16[3,64,2048]{2,1,0:T(8,128)(2,1)S(1)}, bf16[3,64,2048]{2,1,0:T(8,128)(2,1)S(1)}, u32[]{:S(2)}, u32[]{:S(2)}) %collective-permute-start) | collective-permute-done | bytes 786464 | tf_op jit(solution)/shard_map/ppermute | solution.py:27
  71.7 17.8 %collective-permute-done.1.w2_ref = bf16[3,64,2048]{2,1,0:T(8,128)(2,1)S(1)} collective-permute-done((bf16[3,64,2048]{2,1,0:T(8,128)(2,1)S(1)}, bf16[3,64,2048]{2,1,0:T(8,128)(2,1)S(1)}, u32[]{:S(2)}, u32[]{:S(2)}) %collective-permute-start.1) | collective-permute-done | bytes 786464 | tf_op jit(solution)/shard_map/ppermute | solution.py:27
  89.6 0.9 copy-done.1
  90.5 0.9 collective-permute-done.2.w3_ref
  91.4 0.9 copy-done.3
  92.3 1.1 copy-done.2
  93.4 1.1 copy-done.4
  94.6 3.1 %shard_map.172 = (bf16[16,160,128]{2,1,0:T(8,128)(2,1)}, bf16[3,160,256]{2,1,0:T(8,128)(2,1)}) custom-call(bf16[4,8,160,128]{3,2,1,0:T(8,128)(2,1)S(1)} %all-to-all-done.1.got_ref, bf16[3,64,2048]{2,1,0:T(8,128)(2,1)S(1)} %constant_dynamic-update-slice_fusion.w0_ref, bf16[3,64,2048]{2,1,0:T(8,128)(2,1)S(1)} %collective-permute-done.w1_ref, ...), custom_call_target="tpu_custom_call" | custom-call | tf_op jit(solution)/shard_map/pallas_call | solution.py:308
  97.7 19.2 %all_to_all.30.part_ref = bf16[16,160,128]{2,1,0:T(8,128)(2,1)S(1)} all-to-all(bf16[16,160,128]{2,1,0:T(8,128)(2,1)} %get-tuple-element.26), channel_id=1, replica_groups=mesh['z'=16,'c'=2,'y'=4,'x'=4] {'y','x'}, dimensions={0} | all-to-all | bytes 1310720 | tf_op jit(solution)/shard_map/all_to_all | solution.py:22
  116.9 1.5 shard_map.174
  118.4 5.8 %all-to-all-start.3 = ((bf16[32,24,128]{2,1,0:T(8,128)(2,1)}), bf16[32,24,128]{2,1,0:T(8,128)(2,1)S(1)}, u32[]{:S(2)}, u32[]{:S(2)}) async-start(bf16[32,24,128]{2,1,0:T(8,128)(2,1)} %bitcast.28), calls=%async_computation.3 | async-start | bytes 393216 | tf_op jit(solution)/shard_map/all_to_all | solution.py:22
  124.3 18.8 %all-to-all-done.3 = bf16[32,24,128]{2,1,0:T(8,128)(2,1)S(1)} async-done(((bf16[32,24,128]{2,1,0:T(8,128)(2,1)}), bf16[32,24,128]{2,1,0:T(8,128)(2,1)S(1)}, u32[]{:S(2)}, u32[]{:S(2)}) %all-to-all-start.3) | async-done | bytes 196640 | tf_op jit(solution)/shard_map/all_to_all | solution.py:22
  143.2 1.4 shard_map.175
  144.6 3.8 %all-to-all-start.4 = ((bf16[16,256,128]{2,1,0:T(8,128)(2,1)}), bf16[16,256,128]{2,1,0:T(8,128)(2,1)S(1)}, u32[]{:S(2)}, u32[]{:S(2)}) async-start(bf16[16,256,128]{2,1,0:T(8,128)(2,1)} %shard_map.175), calls=%async_computation.4 | async-start | bytes 2097152 | tf_op jit(solution)/shard_map/all_to_all | solution.py:22
  148.4 2.5 %collective-permute-start.6 = (bf16[64,128]{1,0:T(8,128)(2,1)S(1)}, bf16[64,128]{1,0:T(8,128)(2,1)S(1)}, u32[]{:S(2)}, u32[]{:S(2)}) collective-permute-start(bf16[64,128]{1,0:T(8,128)(2,1)S(1)} %bitcast.24), channel_id=1, source_target_pairs={{128,0},{160,32},{192,64},{224,96},{256,128},{288,160},{320,192},{... | collective-permute-start | bytes 49160 | tf_op jit(solution)/shard_map/ppermute | solution.py:37
  150.9 7.5 %collective-permute-start.7 = (bf16[64,128]{1,0:T(8,128)(2,1)S(1)}, bf16[64,128]{1,0:T(8,128)(2,1)S(1)}, u32[]{:S(2)}, u32[]{:S(2)}) collective-permute-start(bf16[64,128]{1,0:T(8,128)(2,1)S(1)} %bitcast.25), channel_id=1, source_target_pairs={{256,0},{288,32},{320,64},{352,96},{384,128},{416,160},{448,192},{... | collective-permute-start | bytes 49160 | tf_op jit(solution)/shard_map/ppermute | solution.py:37
  158.5 2.1 collective-permute-start.8
  160.7 4.2 %collective-permute-start.13 = (bf16[2,128]{1,0:T(2,128)(2,1)S(1)}, bf16[2,128]{1,0:T(2,128)(2,1)S(1)}, u32[]{:S(2)}, u32[]{:S(2)}) collective-permute-start(bf16[2,128]{1,0:T(2,128)(2,1)S(1)} %slice.104), channel_id=1, source_target_pairs={{0,16},{16,32},{32,48},{48,64},{64,80},{80,96},{96,112},{112,128},... | collective-permute-start | bytes 1544 | tf_op jit(solution)/shard_map/ppermute | solution.py:49
  164.9 1.9 collective-permute-done.8.refs_3_
  166.9 4.1 %collective-permute-start.9 = (bf16[4,64,128]{2,1,0:T(8,128)(2,1)S(1)}, bf16[4,64,128]{2,1,0:T(8,128)(2,1)S(1)}, u32[]{:S(2)}, u32[]{:S(2)}) collective-permute-start(bf16[4,64,128]{2,1,0:T(8,128)(2,1)S(1)} %shard_map.176.refs_0_), channel_id=1, source_target_pairs={{32,0},{64,32},{96,64},{0,96},{160,128},{192,160},{224,192},{128,2... | collective-permute-start | bytes 196616 | tf_op jit(solution)/shard_map/ppermute | solution.py:37
  171.0 1.9 collective-permute-start.10
  172.9 2.2 collective-permute-start.11
  175.2 1.7 collective-permute-done.10.refs_2_
  176.9 2.8 %collective-permute-done.11.refs_3_ = bf16[4,64,128]{2,1,0:T(8,128)(2,1)S(1)} collective-permute-done((bf16[4,64,128]{2,1,0:T(8,128)(2,1)S(1)}, bf16[4,64,128]{2,1,0:T(8,128)(2,1)S(1)}, u32[]{:S(2)}, u32[]{:S(2)}) %collective-permute-start.11) | collective-permute-done | bytes 65568 | tf_op jit(solution)/shard_map/ppermute | solution.py:37
  179.8 5.1 %collective-permute-start.12 = (bf16[4,4,64,128]{3,2,1,0:T(8,128)(2,1)S(1)}, bf16[4,4,64,128]{3,2,1,0:T(8,128)(2,1)S(1)}, u32[]{:S(2)}, u32[]{:S(2)}) collective-permute-start(bf16[4,4,64,128]{3,2,1,0:T(8,128)(2,1)S(1)} %shard_map.177.own_ref), channel_id=1, source_target_pairs={{16,0},{0,16},{17,1},{1,17},{18,2},{2,18},{19,3},{3,19},{20,4},{4,... | collective-permute-start | bytes 786440 | tf_op jit(solution)/shard_map/ppermute | solution.py:37
  184.9 2.6 %shard_map.173 = (bf16[3,64,2048]{2,1,0:T(8,128)(2,1)}, bf16[3,64,2048]{2,1,0:T(8,128)(2,1)}, bf16[3,64,2048]{2,1,0:T(8,128)(2,1)}, bf16[3,64,2048]{2,1,0:T(8,128)(2,1)}) custom-call(bf16[4,8,160,128]{3,2,1,0:T(8,128)(2,1)S(1)} %all-to-all-done.1.got_ref, bf16[3,160,256]{2,1,0:T(8,128)(2,1)S(1)} %copy-done.5), custom_call_target="tpu_custom_call" | custom-call | tf_op jit(solution)/shard_map/pallas_call | solution.py:308
  187.5 3.5 %collective-permute-start.5 = (bf16[3,64,2048]{2,1,0:T(8,128)(2,1)}, bf16[3,64,2048]{2,1,0:T(8,128)(2,1)}, u32[]{:S(2)}, u32[]{:S(2)}) collective-permute-start(bf16[3,64,2048]{2,1,0:T(8,128)(2,1)} %get-tuple-element.24), channel_id=1, source_target_pairs={{0,1},{1,2},{2,3},{3,0},{4,5},{5,6},{6,7},{7,4},{8,9},{9,10},{10,1... | collective-permute-start | bytes 2359304 | tf_op jit(solution)/shard_map/ppermute | solution.py:27
  191.0 4.3 %collective-permute-start.4 = (bf16[3,64,2048]{2,1,0:T(8,128)(2,1)}, bf16[3,64,2048]{2,1,0:T(8,128)(2,1)}, u32[]{:S(2)}, u32[]{:S(2)}) collective-permute-start(bf16[3,64,2048]{2,1,0:T(8,128)(2,1)} %get-tuple-element.23), channel_id=1, source_target_pairs={{0,2},{1,3},{2,0},{3,1},{4,6},{5,7},{6,4},{7,5},{8,10},{9,11},{10,... | collective-permute-start | bytes 2359304 | tf_op jit(solution)/shard_map/ppermute | solution.py:27
  195.4 3.1 %collective-permute-start.3 = (bf16[3,64,2048]{2,1,0:T(8,128)(2,1)}, bf16[3,64,2048]{2,1,0:T(8,128)(2,1)}, u32[]{:S(2)}, u32[]{:S(2)}) collective-permute-start(bf16[3,64,2048]{2,1,0:T(8,128)(2,1)} %get-tuple-element.22), channel_id=1, source_target_pairs={{0,3},{1,0},{2,1},{3,2},{4,7},{5,4},{6,5},{7,6},{8,11},{9,8},{10,9... | collective-permute-start | bytes 2359304 | tf_op jit(solution)/shard_map/ppermute | solution.py:27
  198.5 0.7 multiply_convert_fusion
  199.3 2.6 %mixer.1 = (bf16[16,64,128]{2,1,0:T(8,128)(2,1)S(1)}, bf16[16,64,128]{2,1,0:T(8,128)(2,1)}, bf16[256,128]{1,0:T(8,128)(2,1)}, bf16[256,128]{1,0:T(8,128)(2,1)}) custom-call(s32[1]{0:T(128)} %bitcast.6.place_ref.core_ref, bf16[16,256,128]{2,1,0:T(8,128)(2,1)S(1)} %all-to-all-done.4.full_ref, bf16[256,2048]{1,0:T(8,128)(2,1)S(1)} %copy-done, ...), custom_call_target="tpu_custom_call" | custom-call | tf_op jit(solution)/shard_map/mixer/pallas_call | solution.py:285
  201.9 2.9 %collective-permute-start.14 = (bf16[16,64,128]{2,1,0:T(8,128)(2,1)}, bf16[16,64,128]{2,1,0:T(8,128)(2,1)S(1)}, u32[]{:S(2)}, u32[]{:S(2)}) collective-permute-start(bf16[16,64,128]{2,1,0:T(8,128)(2,1)} %get-tuple-element.28), channel_id=1, source_target_pairs={{16,0},{0,16},{17,1},{1,17},{18,2},{2,18},{19,3},{3,19},{20,4},{4,... | collective-permute-start | bytes 786440 | tf_op jit(solution)/shard_map/ppermute | solution.py:37
  204.8 0.7 slice.91
  205.5 1.9 collective-permute-start.15
  207.4 0.8 add_convert_fusion
  208.2 7.0 %all-to-all-start.5 = ((bf16[16,64,128]{2,1,0:T(8,128)(2,1)}), bf16[16,64,128]{2,1,0:T(8,128)(2,1)S(1)}, u32[]{:S(2)}, u32[]{:S(2)}) async-start(bf16[16,64,128]{2,1,0:T(8,128)(2,1)} %add_convert_fusion), calls=%async_computation.5 | async-start | bytes 524288 | tf_op jit(solution)/shard_map/all_to_all | solution.py:22
  215.3 13.0 %collective-permute-done.4 = bf16[3,64,2048]{2,1,0:T(8,128)(2,1)} collective-permute-done((bf16[3,64,2048]{2,1,0:T(8,128)(2,1)}, bf16[3,64,2048]{2,1,0:T(8,128)(2,1)}, u32[]{:S(2)}, u32[]{:S(2)}) %collective-permute-start.4) | collective-permute-done | bytes 786464 | tf_op jit(solution)/shard_map/ppermute | solution.py:27
  228.2 1.2 collective-permute-done.3
  229.4 2.9 %add_convert_fusion.1 = (bf16[1,64,2048]{2,1,0:T(8,128)(2,1)}, bf16[1,64,2048]{2,1,0:T(8,128)(2,1)}, bf16[1,64,2048]{2,1,0:T(8,128)(2,1)}) fusion(bf16[3,64,2048]{2,1,0:T(8,128)(2,1)} %collective-permute-done.5, bf16[3,64,2048]{2,1,0:T(8,128)(2,1)} %collective-permute-done.4, bf16[3,64,2048]{2,1,0:T(8,128)(2,1)} %collective-permute-done.3, ...), kind=kLoop, calls=%fused_computation.2 | loop fusion | flops 3145728 | bytes 3932160 | tf_op jit(solution)/shard_map/convert_element_type | solution.py:381
  232.3 0.7 fusion
  (55 shorter events, 1.7 us)
Async XLA Ops:
  0.6 19.1 %copy-start.10 = (bf16[1,64,2048]{2,1,0:T(8,128)(2,1)S(1)}, bf16[1,64,2048]{2,1,0:T(8,128)(2,1)}, u32[]{:S(2)}) copy-start(bf16[1,64,2048]{2,1,0:T(8,128)(2,1)} %param.16) | copy-start | bytes 786436
  0.6 19.1 %copy-start.11 = (bf16[1,64,2048]{2,1,0:T(8,128)(2,1)S(1)}, bf16[1,64,2048]{2,1,0:T(8,128)(2,1)}, u32[]{:S(2)}) copy-start(bf16[1,64,2048]{2,1,0:T(8,128)(2,1)} %param.17) | copy-start | bytes 786436
  3.0 41.7 %all-to-all-start = ((bf16[32,40,128]{2,1,0:T(8,128)(2,1)}), bf16[32,40,128]{2,1,0:T(8,128)(2,1)S(1)}, u32[]{:S(2)}, u32[]{:S(2)}) async-start(bf16[32,40,128]{2,1,0:T(8,128)(2,1)} %bitcast.29), calls=%async_computation | async-start | bytes 655360 | tf_op jit(solution)/shard_map/all_to_all | solution.py:22
  46.2 4.3 %copy-start.12 = (bf16[1,64,2048]{2,1,0:T(8,128)(2,1)S(1)}, bf16[1,64,2048]{2,1,0:T(8,128)(2,1)}, u32[]{:S(2)}) copy-start(bf16[1,64,2048]{2,1,0:T(8,128)(2,1)} %param.18) | copy-start | bytes 786436
  46.2 46.1 %all-to-all-start.1 = ((bf16[4,8,160,128]{3,2,1,0:T(8,128)(2,1)}), bf16[4,8,160,128]{3,2,1,0:T(8,128)(2,1)S(1)}, u32[]{:S(2)}, u32[]{:S(2)}) async-start(bf16[4,8,160,128]{3,2,1,0:T(8,128)(2,1)} %shard_map.171), calls=%async_computation.1 | async-start | bytes 2621440 | tf_op jit(solution)/shard_map/all_to_all | solution.py:22
  50.5 21.2 %collective-permute-start = (bf16[3,64,2048]{2,1,0:T(8,128)(2,1)S(1)}, bf16[3,64,2048]{2,1,0:T(8,128)(2,1)S(1)}, u32[]{:S(2)}, u32[]{:S(2)}) collective-permute-start(bf16[3,64,2048]{2,1,0:T(8,128)(2,1)S(1)} %constant_dynamic-update-slice_fusion.w0_ref), channel_id=1, source_target_pairs={{0,1},{1,2},{2,3},{3,0},{4,5},{5,6},{6,7},{7,4},{8,9},{9,10},{10,1... | collective-permute-start | bytes 2359304 | tf_op jit(solution)/shard_map/ppermute | solution.py:27
  53.6 35.9 %collective-permute-start.1 = (bf16[3,64,2048]{2,1,0:T(8,128)(2,1)S(1)}, bf16[3,64,2048]{2,1,0:T(8,128)(2,1)S(1)}, u32[]{:S(2)}, u32[]{:S(2)}) collective-permute-start(bf16[3,64,2048]{2,1,0:T(8,128)(2,1)S(1)} %constant_dynamic-update-slice_fusion.w0_ref), channel_id=1, source_target_pairs={{0,2},{1,3},{2,0},{3,1},{4,6},{5,7},{6,4},{7,5},{8,10},{9,11},{10,... | collective-permute-start | bytes 2359304 | tf_op jit(solution)/shard_map/ppermute | solution.py:27
  58.0 33.4 %collective-permute-start.2 = (bf16[3,64,2048]{2,1,0:T(8,128)(2,1)S(1)}, bf16[3,64,2048]{2,1,0:T(8,128)(2,1)S(1)}, u32[]{:S(2)}, u32[]{:S(2)}) collective-permute-start(bf16[3,64,2048]{2,1,0:T(8,128)(2,1)S(1)} %constant_dynamic-update-slice_fusion.w0_ref), channel_id=1, source_target_pairs={{0,3},{1,0},{2,1},{3,2},{4,7},{5,4},{6,5},{7,6},{8,11},{9,8},{10,9... | collective-permute-start | bytes 2359304 | tf_op jit(solution)/shard_map/ppermute | solution.py:27
  89.6 0.9 copy-start.1
  91.4 0.9 copy-start.3
  92.3 1.1 copy-start.2
  93.4 1.1 copy-start.4
  97.7 26.5 %copy-start.15 = (s32[2,256]{1,0:T(2,128)S(1)}, s32[2,256]{1,0:T(2,128)}, u32[]{:S(2)}) copy-start(s32[2,256]{1,0:T(2,128)} %get-tuple-element.25) | copy-start | bytes 6148
  118.4 24.8 %all-to-all-start.3 = ((bf16[32,24,128]{2,1,0:T(8,128)(2,1)}), bf16[32,24,128]{2,1,0:T(8,128)(2,1)S(1)}, u32[]{:S(2)}, u32[]{:S(2)}) async-start(bf16[32,24,128]{2,1,0:T(8,128)(2,1)} %bitcast.28), calls=%async_computation.3 | async-start | bytes 393216 | tf_op jit(solution)/shard_map/all_to_all | solution.py:22
  144.6 3.8 %copy-start.6 = (bf16[128,64]{0,1:T(8,128)(2,1)S(1)}, bf16[128,64]{0,1:T(8,128)(2,1)}, u32[]{:S(2)}) copy-start(bf16[128,64]{0,1:T(8,128)(2,1)} %param.23) | copy-start | bytes 49156
  144.6 16.1 %copy-start.9 = (bf16[256,128]{1,0:T(8,128)(2,1)S(1)}, bf16[256,128]{1,0:T(8,128)(2,1)}, u32[]{:S(2)}) copy-start(bf16[256,128]{1,0:T(8,128)(2,1)} %param.20) | copy-start | bytes 196612
  144.6 16.1 %copy-start.13 = (bf16[256,128]{1,0:T(8,128)(2,1)S(1)}, bf16[256,128]{1,0:T(8,128)(2,1)}, u32[]{:S(2)}) copy-start(bf16[256,128]{1,0:T(8,128)(2,1)} %param.21) | copy-start | bytes 196612
  144.6 30.6 %copy-start.16 = (f32[3,128]{1,0:T(4,128)S(1)}, f32[3,128]{1,0:T(4,128)}, u32[]{:S(2)}) copy-start(f32[3,128]{1,0:T(4,128)} %param.22) | copy-start | bytes 4612
  144.6 40.3 %copy-start.5 = (bf16[3,160,256]{2,1,0:T(8,128)(2,1)S(1)}, bf16[3,160,256]{2,1,0:T(8,128)(2,1)}, u32[]{:S(2)}) copy-start(bf16[3,160,256]{2,1,0:T(8,128)(2,1)} %get-tuple-element.20.cots_ref) | copy-start | bytes 737284
  144.6 54.7 %all-to-all-start.4 = ((bf16[16,256,128]{2,1,0:T(8,128)(2,1)}), bf16[16,256,128]{2,1,0:T(8,128)(2,1)S(1)}, u32[]{:S(2)}, u32[]{:S(2)}) async-start(bf16[16,256,128]{2,1,0:T(8,128)(2,1)} %shard_map.175), calls=%async_computation.4 | async-start | bytes 2097152 | tf_op jit(solution)/shard_map/all_to_all | solution.py:22
  148.4 50.1 %copy-start.8 = (bf16[256,128]{1,0:T(8,128)(2,1)S(1)}, bf16[256,128]{1,0:T(8,128)(2,1)}, u32[]{:S(2)}) copy-start(bf16[256,128]{1,0:T(8,128)(2,1)} %outer_hbm.1) | copy-start | bytes 196612
  148.4 16.5 %collective-permute-start.6 = (bf16[64,128]{1,0:T(8,128)(2,1)S(1)}, bf16[64,128]{1,0:T(8,128)(2,1)S(1)}, u32[]{:S(2)}, u32[]{:S(2)}) collective-permute-start(bf16[64,128]{1,0:T(8,128)(2,1)S(1)} %bitcast.24), channel_id=1, source_target_pairs={{128,0},{160,32},{192,64},{224,96},{256,128},{288,160},{320,192},{... | collective-permute-start | bytes 49160 | tf_op jit(solution)/shard_map/ppermute | solution.py:37
  150.9 14.0 %collective-permute-start.7 = (bf16[64,128]{1,0:T(8,128)(2,1)S(1)}, bf16[64,128]{1,0:T(8,128)(2,1)S(1)}, u32[]{:S(2)}, u32[]{:S(2)}) collective-permute-start(bf16[64,128]{1,0:T(8,128)(2,1)S(1)} %bitcast.25), channel_id=1, source_target_pairs={{256,0},{288,32},{320,64},{352,96},{384,128},{416,160},{448,192},{... | collective-permute-start | bytes 49160 | tf_op jit(solution)/shard_map/ppermute | solution.py:37
  158.5 8.4 %collective-permute-start.8 = (bf16[64,128]{1,0:T(8,128)(2,1)S(1)}, bf16[64,128]{1,0:T(8,128)(2,1)S(1)}, u32[]{:S(2)}, u32[]{:S(2)}) collective-permute-start(bf16[64,128]{1,0:T(8,128)(2,1)S(1)} %bitcast.26), channel_id=1, source_target_pairs={{384,0},{416,32},{448,64},{480,96},{0,128},{32,160},{64,192},{96,2... | collective-permute-start | bytes 49160 | tf_op jit(solution)/shard_map/ppermute | solution.py:37
  160.7 37.8 %collective-permute-start.13 = (bf16[2,128]{1,0:T(2,128)(2,1)S(1)}, bf16[2,128]{1,0:T(2,128)(2,1)S(1)}, u32[]{:S(2)}, u32[]{:S(2)}) collective-permute-start(bf16[2,128]{1,0:T(2,128)(2,1)S(1)} %slice.104), channel_id=1, source_target_pairs={{0,16},{16,32},{32,48},{48,64},{64,80},{80,96},{96,112},{112,128},... | collective-permute-start | bytes 1544 | tf_op jit(solution)/shard_map/ppermute | solution.py:49
  166.9 8.3 %collective-permute-start.9 = (bf16[4,64,128]{2,1,0:T(8,128)(2,1)S(1)}, bf16[4,64,128]{2,1,0:T(8,128)(2,1)S(1)}, u32[]{:S(2)}, u32[]{:S(2)}) collective-permute-start(bf16[4,64,128]{2,1,0:T(8,128)(2,1)S(1)} %shard_map.176.refs_0_), channel_id=1, source_target_pairs={{32,0},{64,32},{96,64},{0,96},{160,128},{192,160},{224,192},{128,2... | collective-permute-start | bytes 196616 | tf_op jit(solution)/shard_map/ppermute | solution.py:37
  171.0 5.9 %collective-permute-start.10 = (bf16[4,64,128]{2,1,0:T(8,128)(2,1)S(1)}, bf16[4,64,128]{2,1,0:T(8,128)(2,1)S(1)}, u32[]{:S(2)}, u32[]{:S(2)}) collective-permute-start(bf16[4,64,128]{2,1,0:T(8,128)(2,1)S(1)} %shard_map.176.refs_0_), channel_id=1, source_target_pairs={{64,0},{96,32},{0,64},{32,96},{192,128},{224,160},{128,192},{160,2... | collective-permute-start | bytes 196616 | tf_op jit(solution)/shard_map/ppermute | solution.py:37
  172.9 6.8 %collective-permute-start.11 = (bf16[4,64,128]{2,1,0:T(8,128)(2,1)S(1)}, bf16[4,64,128]{2,1,0:T(8,128)(2,1)S(1)}, u32[]{:S(2)}, u32[]{:S(2)}) collective-permute-start(bf16[4,64,128]{2,1,0:T(8,128)(2,1)S(1)} %shard_map.176.refs_0_), channel_id=1, source_target_pairs={{96,0},{0,32},{32,64},{64,96},{224,128},{128,160},{160,192},{192,2... | collective-permute-start | bytes 196616 | tf_op jit(solution)/shard_map/ppermute | solution.py:37
  179.8 19.5 %collective-permute-start.12 = (bf16[4,4,64,128]{3,2,1,0:T(8,128)(2,1)S(1)}, bf16[4,4,64,128]{3,2,1,0:T(8,128)(2,1)S(1)}, u32[]{:S(2)}, u32[]{:S(2)}) collective-permute-start(bf16[4,4,64,128]{3,2,1,0:T(8,128)(2,1)S(1)} %shard_map.177.own_ref), channel_id=1, source_target_pairs={{16,0},{0,16},{17,1},{1,17},{18,2},{2,18},{19,3},{3,19},{20,4},{4,... | collective-permute-start | bytes 786440 | tf_op jit(solution)/shard_map/ppermute | solution.py:37
  187.5 11.8 %copy-start = (bf16[256,2048]{1,0:T(8,128)(2,1)S(1)}, bf16[256,2048]{1,0:T(8,128)(2,1)}, u32[]{:S(2)}) copy-start(bf16[256,2048]{1,0:T(8,128)(2,1)} %out_grad_ref.1) | copy-start | bytes 3145732
  187.5 27.8 %collective-permute-start.5 = (bf16[3,64,2048]{2,1,0:T(8,128)(2,1)}, bf16[3,64,2048]{2,1,0:T(8,128)(2,1)}, u32[]{:S(2)}, u32[]{:S(2)}) collective-permute-start(bf16[3,64,2048]{2,1,0:T(8,128)(2,1)} %get-tuple-element.24), channel_id=1, source_target_pairs={{0,1},{1,2},{2,3},{3,0},{4,5},{5,6},{6,7},{7,4},{8,9},{9,10},{10,1... | collective-permute-start | bytes 2359304 | tf_op jit(solution)/shard_map/ppermute | solution.py:27
  191.0 37.2 %collective-permute-start.4 = (bf16[3,64,2048]{2,1,0:T(8,128)(2,1)}, bf16[3,64,2048]{2,1,0:T(8,128)(2,1)}, u32[]{:S(2)}, u32[]{:S(2)}) collective-permute-start(bf16[3,64,2048]{2,1,0:T(8,128)(2,1)} %get-tuple-element.23), channel_id=1, source_target_pairs={{0,2},{1,3},{2,0},{3,1},{4,6},{5,7},{6,4},{7,5},{8,10},{9,11},{10,... | collective-permute-start | bytes 2359304 | tf_op jit(solution)/shard_map/ppermute | solution.py:27
  195.4 34.0 %collective-permute-start.3 = (bf16[3,64,2048]{2,1,0:T(8,128)(2,1)}, bf16[3,64,2048]{2,1,0:T(8,128)(2,1)}, u32[]{:S(2)}, u32[]{:S(2)}) collective-permute-start(bf16[3,64,2048]{2,1,0:T(8,128)(2,1)} %get-tuple-element.22), channel_id=1, source_target_pairs={{0,3},{1,0},{2,1},{3,2},{4,7},{5,4},{6,5},{7,6},{8,11},{9,8},{10,9... | collective-permute-start | bytes 2359304 | tf_op jit(solution)/shard_map/ppermute | solution.py:27
  201.9 27.5 %copy-start.7 = (bf16[3,64,2048]{2,1,0:T(8,128)(2,1)S(1)}, bf16[3,64,2048]{2,1,0:T(8,128)(2,1)}, u32[]{:S(2)}) copy-start(bf16[3,64,2048]{2,1,0:T(8,128)(2,1)} %get-tuple-element.21) | copy-start | bytes 2359300
  201.9 5.5 %collective-permute-start.14 = (bf16[16,64,128]{2,1,0:T(8,128)(2,1)}, bf16[16,64,128]{2,1,0:T(8,128)(2,1)S(1)}, u32[]{:S(2)}, u32[]{:S(2)}) collective-permute-start(bf16[16,64,128]{2,1,0:T(8,128)(2,1)} %get-tuple-element.28), channel_id=1, source_target_pairs={{16,0},{0,16},{17,1},{1,17},{18,2},{2,18},{19,3},{3,19},{20,4},{4,... | collective-permute-start | bytes 786440 | tf_op jit(solution)/shard_map/ppermute | solution.py:37
  205.5 26.7 %collective-permute-start.15 = (bf16[2,128]{1,0:T(2,128)(2,1)S(1)}, bf16[2,128]{1,0:T(2,128)(2,1)S(1)}, u32[]{:S(2)}, u32[]{:S(2)}) collective-permute-start(bf16[2,128]{1,0:T(2,128)(2,1)S(1)} %slice.91), channel_id=1, source_target_pairs={{16,0},{32,16},{48,32},{64,48},{80,64},{96,80},{112,96},{128,112},... | collective-permute-start | bytes 1544 | tf_op jit(solution)/shard_map/ppermute | solution.py:49
  208.2 25.4 %all-to-all-start.5 = ((bf16[16,64,128]{2,1,0:T(8,128)(2,1)}), bf16[16,64,128]{2,1,0:T(8,128)(2,1)S(1)}, u32[]{:S(2)}, u32[]{:S(2)}) async-start(bf16[16,64,128]{2,1,0:T(8,128)(2,1)} %add_convert_fusion), calls=%async_computation.5 | async-start | bytes 524288 | tf_op jit(solution)/shard_map/all_to_all | solution.py:22
  229.4 2.9 %copy-start.14 = (bf16[256,128]{1,0:T(8,128)(2,1)S(1)}, bf16[256,128]{1,0:T(8,128)(2,1)}, u32[]{:S(2)}) copy-start(bf16[256,128]{1,0:T(8,128)(2,1)} %get-tuple-element.30) | copy-start | bytes 196612
